TPU v7x, 512 devices: a whole 4x4x16 slice. The times are simulated.
512 devices in a mesh: fs: 64 (over z, y), tp: 8 (over x, core).
Axes of the slice: x: 4, y: 4, z: 16, core: 2. Of those that a mesh axis runs over, the one named last changes fastest.
Arguments:
- fwd_tokens: bfloat16 [8192, 2048], P('fs'), may hold values from -6 to 6
- back_tokens: bfloat16 [8192, 2048], P('fs'), may hold values from -16 to 16
- out_grad: bfloat16 [8192, 2048], P('fs'), may hold values from -16 to 16
- norm_gain: float32 [2048], replicated, may hold values from 0.1 to 1.9
- gate_weight: bfloat16 [2048, 2816], P('fs', 'tp'), may hold values from -0.125 to 0.125
- up_weight: bfloat16 [2048, 2816], P('fs', 'tp'), may hold values from -0.125 to 0.125
- down_weight: bfloat16 [2048, 2816], P('fs', 'tp'), may hold values from -0.109375 to 0.109375
- gate_grad_sum: float32 [2048, 2816], P('fs', 'tp'), may hold values from -96 to 96
Outputs:
- fwd_out: bfloat16 [8192, 2048], P('fs')
- back_grad: bfloat16 [8192, 2048], P('fs')
- gate_grad_out: float32 [2048, 2816], P('fs', 'tp')
All inputs are finite; a program needn't handle non-finite values.
Results may differ from a plain program's by a relative error of at most 0.014.
Values may be sent and summed in bfloat16 or wider, within the bound.
No kernel may reach another device: no remote copies, remote signals or barrier semaphores. Data moves between devices by JAX's collectives and lax.ppermute only.
A program may use at most 64 MiB of HBM per device.

v0:
```python
import jax
import jax.numpy as jnp
from jax import lax
from jax.experimental import pallas as pl
from jax.experimental.pallas import tpu as pltpu
from jax.sharding import Mesh
from jax.sharding import PartitionSpec as P

Z = ("za", "zb")
FS = ("za", "zb", "y")
TP = ("x", "c")
norm_eps = 0.25
F32 = jnp.float32
BF = jnp.bfloat16


def shift(array, axis, by):
    n = lax.axis_size(axis)
    return lax.ppermute(array, axis, [(k, (k + by) % n) for k in range(n)])


def copies_to_all(array, axis):
    copies = jnp.broadcast_to(array, (lax.axis_size(axis), *array.shape))
    return lax.all_to_all(copies, axis, split_axis=0, concat_axis=0, tiled=True)


def normalize(tokens, gain):
    values = tokens.astype(F32)
    factor = lax.rsqrt(jnp.mean(values * values, axis=-1, keepdims=True) + norm_eps)
    return (values * factor * gain).astype(BF)


def dot(a, b, ca, cb):
    return lax.dot_general(a, b, (((ca,), (cb,)), ((), ())), preferred_element_type=F32)


def assemble(at, pieces, wholes):
    zb, y = at[0], at[1]
    near, a1, a3, far, z1, z3 = pieces
    todo = []
    for yy in range(4):
        for za in range(4):
            todo.append((near, (yy, za), za * 512 + zb * 128 + yy * 32))
            todo.append((far, (yy, za), za * 512 + (zb + 2) % 4 * 128 + yy * 32))
    for r, mine, other in ((1, a1, z1), (3, a3, z3)):
        base = (zb + r) % 4 * 128
        for za in range(4):
            todo.append((mine, (za,), za * 512 + base + y * 32))
            for dy in range(1, 4):
                todo.append((other, (dy - 1, za), za * 512 + base + (y + dy) % 4 * 32))
    for piece, spot, row in todo:
        rows = pl.ds(pl.multiple_of(row, 32), 32)
        for m, whole in enumerate(wholes):
            whole[rows, :] = piece[(*spot, slice(m * 32, (m + 1) * 32))]


def prepare(at, bt, ft, og, gain, bn, fn, oc):
    bn[...] = normalize(bt[...], gain[...])
    fn[...] = normalize(ft[...], gain[...])
    oc[...] = og[...]


def backward(at, bn, og, *refs):
    pieces, (grads, gd_out, ud_out, wg, wu, wd) = refs[:6], refs[6:]
    assemble(at, pieces, (wg, wu, wd))
    gate = dot(bn[...], wg[...], 1, 0)
    up = dot(bn[...], wu[...], 1, 0)
    hid = 0.5 * dot(og[...], wd[...], 1, 0)
    s = jax.nn.sigmoid(gate)
    gd = (hid * up * s * (1.0 + gate * (1.0 - s))).astype(BF)
    gd_out[...] = gd
    ud_out[...] = (hid * gate * s).astype(BF)
    part = dot(bn[...], gd, 0, 0).astype(BF)
    for yy in range(4):
        for z in range(16):
            row = (z * 4 + yy) * 32
            grads[yy, z, :, :] = part[row : row + 32, :]


def rest(at, fn, gd, ud, *refs):
    pieces, (keep, give, wg, wu, wd, parts) = refs[:6], refs[6:]
    assemble(at, pieces, (wg, wu, wd))
    diff = dot(gd[...], wg[...], 1, 1) + dot(ud[...], wu[...], 1, 1)
    parts[:, 2048:4096] = diff.astype(BF)
    gate = dot(fn[...], wg[...], 1, 0)
    up = dot(fn[...], wu[...], 1, 0)
    hidden = (gate * jax.nn.sigmoid(gate) * up).astype(BF)
    parts[:, 0:2048] = dot(hidden, wd[...], 1, 1).astype(BF)
    c = at[2]
    keep[...] = parts[pl.ds(pl.multiple_of(c * 64, 64), 64), :]
    give[...] = parts[pl.ds(pl.multiple_of((1 - c) * 64, 64), 64), :]


def pair(at, keep, other, *outs):
    for k, out in enumerate(outs):
        rows = pl.ds(pl.multiple_of((at[3] + k) % 4 * 16, 16), 16)
        out[...] = (keep[rows, :].astype(F32) + other[rows, :].astype(F32)).astype(BF)


def finish(at, p0, p1, p2, p3, bt, gain, out):
    rows = pl.ds(pl.multiple_of((at[2] * 4 + at[3]) * 16, 16), 16)
    total = p0[...].astype(F32) + p1[...].astype(F32) + p2[...].astype(F32) + p3[...].astype(F32)
    out[:, 0:2048] = (0.5 * total[:, 0:2048]).astype(BF)
    values = bt[rows, :].astype(F32)
    factor = lax.rsqrt(jnp.mean(values * values, axis=-1, keepdims=True) + norm_eps)
    scaled = total[:, 2048:4096] * gain[...]
    cubed = factor * factor * factor
    mean = jnp.mean(scaled * values, axis=-1, keepdims=True)
    out[:, 2048:4096] = (factor * scaled - values * cubed * mean).astype(BF)


VM = pl.BlockSpec(memory_space=pltpu.VMEM)
SM = pl.BlockSpec(memory_space=pltpu.SMEM)


def call(body, outs, scratch, *args):
    return pl.pallas_call(
        body,
        out_shape=tuple(jax.ShapeDtypeStruct(o, BF) for o in outs),
        in_specs=[SM] + [VM] * (len(args) - 1),
        out_specs=(VM,) * len(outs),
        scratch_shapes=[pltpu.VMEM(o, BF) for o in scratch],
        compiler_params=pltpu.CompilerParams(vmem_limit_bytes=LIMIT),
    )(*args)


LIMIT = 24 * 1024 * 1024
W = (2048, 352)
TOK = (128, 2048)
HID = (128, 352)


def exchange(array, axis):
    return lax.all_to_all(array, axis, split_axis=0, concat_axis=0, tiled=True)


def shards(ft, bt, og, gain, gw, uw, dw, gsum):
    spots = [lax.axis_index(n) for n in ("zb", "y", "c", "x")]
    y, c = spots[1], spots[2]
    at = jnp.stack(spots).astype(jnp.int32)
    gain = gain.reshape(1, 2048)
    own = jnp.concatenate([gw, uw, dw], axis=0)
    a = copies_to_all(own, "za")
    near = copies_to_all(a, "y")
    a1 = shift(a, Z, -1)
    a3 = shift(a, Z, 1)
    a2 = jnp.concatenate([shift(a[:2], Z, -2), shift(a[2:], Z, 2)])
    others = lax.dynamic_slice_in_dim(jnp.concatenate([near, near]), y + 1, 3)
    z1 = shift(others, Z, -1)
    z3 = shift(others, Z, 1)
    far = copies_to_all(a2, "y")
    pieces = (near, a1, a3, far, z1, z3)
    bn, fn, oc = call(prepare, (TOK,) * 3, (), at, bt, ft, og, gain)
    grads, gd, ud = call(backward, ((4, 16, 32, 352), HID, HID), (W,) * 3, at, bn, oc, *pieces)
    gy = exchange(grads, "y")
    keep, give = call(rest, ((64, 4096),) * 2, (W, W, W, (128, 4096)), at, fn, gd, ud, *pieces)
    other = shift(give, "c", 1)
    p0, p1, p2, p3 = call(pair, ((16, 4096),) * 4, (), at, keep, other)
    p1, p2, p3 = shift(p1, "x", 1), shift(p2, "x", 2), shift(p3, "x", -1)
    gy = gy.astype(F32).sum(axis=0).astype(BF)
    gz = exchange(gy, Z)
    (done,) = call(finish, ((16, 4096),), (), at, p0, p1, p2, p3, bt, gain)
    half = lax.all_gather(done, "x", axis=0, tiled=True)
    other = shift(half, "c", 1)
    first = jnp.where(c == 0, half, other)
    second = jnp.where(c == 0, other, half)
    whole = jnp.concatenate([first, second], axis=0)
    grad = gsum + gz.astype(F32).sum(axis=0)
    return whole[:, :2048], whole[:, 2048:], grad


def solution(mesh):
    split = Mesh(mesh.devices.reshape(4, 4, 4, 4, 2), ("za", "zb", "y", "x", "c"))
    tok = P(FS, None)
    w = P(FS, TP)
    return jax.shard_map(
        shards,
        mesh=split,
        in_specs=(tok, tok, tok, P(), w, w, w, w),
        out_specs=(tok, tok, w),
        check_vma=False,
    )
```

profile of v0, /device:TPU:16, one launch (start us, length us, event | category | flops | bytes accessed | tf_op | source)
XLA Modules:
  0.0 182.4 jit_solution(11032637768188151865)
XLA Ops:
  0.6 0.8 pad_maximum_fusion.2
  1.5 34.3 %all_to_all.25 = bf16[4,96,352]{2,1,0:T(8,128)(2,1)} all-to-all(bf16[4,96,352]{2,1,0:T(8,128)(2,1)S(1)} %broadcast_in_dim.9), channel_id=1, replica_groups=mesh['za'=4,'zb'=4,'y'=4,'x'=4,'c'=2] {'za'}, dimensions={0} | all-to-all | bytes 540672 | tf_op jit(solution)/shard_map/all_to_all | solution.py:24
  35.8 2.1 %broadcast_in_dim.10 = bf16[4,4,96,352]{3,2,1,0:T(8,128)(2,1)} broadcast(bf16[4,96,352]{2,1,0:T(8,128)(2,1)} %all_to_all.25), dimensions={1,2,3} | broadcast | bytes 1351680 | tf_op jit(solution)/shard_map/broadcast_in_dim | solution.py:23
  37.9 4.8 %all-to-all-start.1 = ((bf16[4,4,96,352]{3,2,1,0:T(8,128)(2,1)}), bf16[4,4,96,352]{3,2,1,0:T(8,128)(2,1)S(1)}, u32[]{:S(2)}, u32[]{:S(2)}) async-start(bf16[4,4,96,352]{3,2,1,0:T(8,128)(2,1)} %broadcast_in_dim.10), calls=%async_computation.1 | async-start | bytes 2359296 | tf_op jit(solution)/shard_map/all_to_all | solution.py:24
  42.7 1.0 fusion.2
  43.7 5.5 %collective-permute-start.2 = (bf16[2,96,352]{2,1,0:T(8,128)(2,1)S(1)}, bf16[2,96,352]{2,1,0:T(8,128)(2,1)S(1)}, u32[]{:S(2)}, u32[]{:S(2)}) collective-permute-start(bf16[2,96,352]{2,1,0:T(8,128)(2,1)S(1)} %get-tuple-element.31), channel_id=1, source_target_pairs={{0,448},{32,480},{64,0},{96,32},{128,64},{160,96},{192,128},{224,1... | collective-permute-start | bytes 405512 | tf_op jit(solution)/shard_map/ppermute | solution.py:19
  49.2 3.6 %collective-permute-start.3 = (bf16[2,96,352]{2,1,0:T(8,128)(2,1)S(1)}, bf16[2,96,352]{2,1,0:T(8,128)(2,1)S(1)}, u32[]{:S(2)}, u32[]{:S(2)}) collective-permute-start(bf16[2,96,352]{2,1,0:T(8,128)(2,1)S(1)} %get-tuple-element.32), channel_id=1, source_target_pairs={{0,64},{32,96},{64,128},{96,160},{128,192},{160,224},{192,256},{22... | collective-permute-start | bytes 405512 | tf_op jit(solution)/shard_map/ppermute | solution.py:19
  52.8 2.5 %collective-permute-done.2 = bf16[2,96,352]{2,1,0:T(8,128)(2,1)S(1)} collective-permute-done((bf16[2,96,352]{2,1,0:T(8,128)(2,1)S(1)}, bf16[2,96,352]{2,1,0:T(8,128)(2,1)S(1)}, u32[]{:S(2)}, u32[]{:S(2)}) %collective-permute-start.2) | collective-permute-done | bytes 135200 | tf_op jit(solution)/shard_map/ppermute | solution.py:19
  55.3 4.6 %collective-permute-done.3 = bf16[2,96,352]{2,1,0:T(8,128)(2,1)S(1)} collective-permute-done((bf16[2,96,352]{2,1,0:T(8,128)(2,1)S(1)}, bf16[2,96,352]{2,1,0:T(8,128)(2,1)S(1)}, u32[]{:S(2)}, u32[]{:S(2)}) %collective-permute-start.3) | collective-permute-done | bytes 135200 | tf_op jit(solution)/shard_map/ppermute | solution.py:19
  59.9 0.1 pad_maximum_fusion.1
  60.0 0.0 all-to-all-done.1.refs_0_
  60.0 1.2 broadcast_in_dim.11
  61.1 4.8 %all-to-all-start.2 = ((bf16[4,4,96,352]{3,2,1,0:T(8,128)(2,1)}), bf16[4,4,96,352]{3,2,1,0:T(8,128)(2,1)S(1)}, u32[]{:S(2)}, u32[]{:S(2)}) async-start(bf16[4,4,96,352]{3,2,1,0:T(8,128)(2,1)} %broadcast_in_dim.11), calls=%async_computation.2 | async-start | bytes 2359296 | tf_op jit(solution)/shard_map/all_to_all | solution.py:24
  65.9 1.3 fusion
  67.3 1.9 %collective-permute-start.4 = (bf16[3,4,96,352]{3,2,1,0:T(8,128)(2,1)}, bf16[3,4,96,352]{3,2,1,0:T(8,128)(2,1)S(1)}, u32[]{:S(2)}, u32[]{:S(2)}) collective-permute-start(bf16[3,4,96,352]{3,2,1,0:T(8,128)(2,1)} %fusion), channel_id=1, source_target_pairs={{0,480},{32,0},{64,32},{96,64},{128,96},{160,128},{192,160},{224,1... | collective-permute-start | bytes 2433032 | tf_op jit(solution)/shard_map/ppermute | solution.py:19
  69.2 3.9 %collective-permute-start.5 = (bf16[3,4,96,352]{3,2,1,0:T(8,128)(2,1)}, bf16[3,4,96,352]{3,2,1,0:T(8,128)(2,1)}, u32[]{:S(2)}, u32[]{:S(2)}) collective-permute-start(bf16[3,4,96,352]{3,2,1,0:T(8,128)(2,1)} %fusion), channel_id=1, source_target_pairs={{0,32},{32,64},{64,96},{96,128},{128,160},{160,192},{192,224},{224... | collective-permute-start | bytes 2433032 | tf_op jit(solution)/shard_map/ppermute | solution.py:19
  73.1 3.6 %collective-permute-start.1 = (bf16[4,96,352]{2,1,0:T(8,128)(2,1)}, bf16[4,96,352]{2,1,0:T(8,128)(2,1)S(1)}, u32[]{:S(2)}, u32[]{:S(2)}) collective-permute-start(bf16[4,96,352]{2,1,0:T(8,128)(2,1)} %all_to_all.25), channel_id=1, source_target_pairs={{0,32},{32,64},{64,96},{96,128},{128,160},{160,192},{192,224},{224... | collective-permute-start | bytes 811016 | tf_op jit(solution)/shard_map/ppermute | solution.py:19
  76.7 3.5 %collective-permute-start = (bf16[4,96,352]{2,1,0:T(8,128)(2,1)}, bf16[4,96,352]{2,1,0:T(8,128)(2,1)}, u32[]{:S(2)}, u32[]{:S(2)}) collective-permute-start(bf16[4,96,352]{2,1,0:T(8,128)(2,1)} %all_to_all.25), channel_id=1, source_target_pairs={{0,480},{32,0},{64,32},{96,64},{128,96},{160,128},{192,160},{224,1... | collective-permute-start | bytes 811016 | tf_op jit(solution)/shard_map/ppermute | solution.py:19
  80.2 0.1 pad_add_fusion.at
  80.3 0.0 copy-done.13
  80.3 1.0 copy-done
  81.3 1.0 copy-done.7
  82.4 1.0 copy-done.8
  83.4 1.0 shard_map.103
  84.4 0.0 copy-start.3
  84.4 0.8 copy-done.3
  85.2 0.8 copy-done.5
  86.0 0.8 copy-done.11
  86.7 10.9 %collective-permute-done.1.refs_2_ = bf16[4,96,352]{2,1,0:T(8,128)(2,1)S(1)} collective-permute-done((bf16[4,96,352]{2,1,0:T(8,128)(2,1)}, bf16[4,96,352]{2,1,0:T(8,128)(2,1)S(1)}, u32[]{:S(2)}, u32[]{:S(2)}) %collective-permute-start.1) | collective-permute-done | bytes 270368 | tf_op jit(solution)/shard_map/ppermute | solution.py:19
  97.6 0.0 collective-permute-done.refs_1_
  97.6 0.0 all-to-all-done.2.refs_3_
  97.6 0.0 collective-permute-done.4.refs_4_
  97.6 0.0 collective-permute-done.5.refs_5_
  97.6 0.0 copy-start.4
  97.6 1.0 copy-done.4
  98.7 1.0 copy-done.6
  99.7 3.2 %shard_map.104 = (bf16[4,16,32,352]{3,2,1,0:T(8,128)(2,1)S(1)}, bf16[128,352]{1,0:T(8,128)(2,1)S(1)}, bf16[128,352]{1,0:T(8,128)(2,1)S(1)}) custom-call(s32[4]{0:T(128)S(1)} %pad_add_fusion.at, bf16[128,2048]{1,0:T(8,128)(2,1)S(1)} %copy-done.4, bf16[128,2048]{1,0:T(8,128)(2,1)S(1)} %copy-done.6, bf16[4,4,96,352]{3,2,1,0:T(8,128)(2,1)S(1)} %all-to-all-done.1.refs_0_, ...), custom_call_target="tpu_custom_call" | custom-call | tf_op jit(solution)/shard_map/pallas_call | solution.py:117
  102.9 1.1 copy-done.2
  104.1 4.7 %shard_map.105 = (bf16[64,4096]{1,0:T(8,128)(2,1)S(1)}, bf16[64,4096]{1,0:T(8,128)(2,1)}) custom-call(s32[4]{0:T(128)S(1)} %pad_add_fusion.at, bf16[128,2048]{1,0:T(8,128)(2,1)S(1)} %copy-done.12, bf16[128,352]{1,0:T(8,128)(2,1)S(1)} %get-tuple-element.18.gd, bf16[128,352]{1,0:T(8,128)(2,1)S(1)} %get-tuple-element.19.ud, ...), custom_call_target="tpu_custom_call" | custom-call | tf_op jit(solution)/shard_map/pallas_call | solution.py:117
  108.7 0.8 copy-done.9
  109.5 1.9 %collective-permute-start.6 = (bf16[64,4096]{1,0:T(8,128)(2,1)}, bf16[64,4096]{1,0:T(8,128)(2,1)S(1)}, u32[]{:S(2)}, u32[]{:S(2)}) collective-permute-start(bf16[64,4096]{1,0:T(8,128)(2,1)} %get-tuple-element.21), channel_id=1, source_target_pairs={{0,1},{1,0},{2,3},{3,2},{4,5},{5,4},{6,7},{7,6},{8,9},{9,8},{10,11... | collective-permute-start | bytes 1572872 | tf_op jit(solution)/shard_map/ppermute | solution.py:19
  111.4 0.0 copy-start.10
  111.4 4.9 %all-to-all-start.3 = ((bf16[4,16,32,352]{3,2,1,0:T(8,128)(2,1)}), bf16[4,16,32,352]{3,2,1,0:T(8,128)(2,1)S(1)}, u32[]{:S(2)}, u32[]{:S(2)}) async-start(bf16[4,16,32,352]{3,2,1,0:T(8,128)(2,1)} %copy-done.2), calls=%async_computation.3 | async-start | bytes 3145728 | tf_op jit(solution)/shard_map/all_to_all | solution.py:134
  116.4 0.0 collective-permute-done.6.other
  116.4 0.7 shard_map.106
  117.1 3.4 %collective-permute-start.7 = (bf16[16,4096]{1,0:T(8,128)(2,1)S(1)}, bf16[16,4096]{1,0:T(8,128)(2,1)S(1)}, u32[]{:S(2)}, u32[]{:S(2)}) collective-permute-start(bf16[16,4096]{1,0:T(8,128)(2,1)S(1)} %get-tuple-element.23), channel_id=1, source_target_pairs={{0,2},{2,4},{4,6},{6,0},{1,3},{3,5},{5,7},{7,1},{8,10},{10,12},{12... | collective-permute-start | bytes 393224 | tf_op jit(solution)/shard_map/ppermute | solution.py:19
  120.5 4.7 %collective-permute-start.8 = (bf16[16,4096]{1,0:T(8,128)(2,1)S(1)}, bf16[16,4096]{1,0:T(8,128)(2,1)S(1)}, u32[]{:S(2)}, u32[]{:S(2)}) collective-permute-start(bf16[16,4096]{1,0:T(8,128)(2,1)S(1)} %get-tuple-element.24), channel_id=1, source_target_pairs={{0,4},{2,6},{4,0},{6,2},{1,5},{3,7},{5,1},{7,3},{8,12},{10,14},{12... | collective-permute-start | bytes 393224 | tf_op jit(solution)/shard_map/ppermute | solution.py:19
  125.1 3.3 %collective-permute-start.9 = (bf16[16,4096]{1,0:T(8,128)(2,1)S(1)}, bf16[16,4096]{1,0:T(8,128)(2,1)S(1)}, u32[]{:S(2)}, u32[]{:S(2)}) collective-permute-start(bf16[16,4096]{1,0:T(8,128)(2,1)S(1)} %get-tuple-element.25), channel_id=1, source_target_pairs={{0,6},{2,0},{4,2},{6,4},{1,7},{3,1},{5,3},{7,5},{8,14},{10,8},{12,... | collective-permute-start | bytes 393224 | tf_op jit(solution)/shard_map/ppermute | solution.py:19
  128.5 0.0 collective-permute-done.7.p1
  128.5 0.8 collective-permute-done.8.p2
  129.3 2.7 %collective-permute-done.9.p3 = bf16[16,4096]{1,0:T(8,128)(2,1)S(1)} collective-permute-done((bf16[16,4096]{1,0:T(8,128)(2,1)S(1)}, bf16[16,4096]{1,0:T(8,128)(2,1)S(1)}, u32[]{:S(2)}, u32[]{:S(2)}) %collective-permute-start.9) | collective-permute-done | bytes 131104 | tf_op jit(solution)/shard_map/ppermute | solution.py:19
  132.0 0.7 shard_map.107
  132.7 13.5 %all_gather.3 = bf16[64,4096]{1,0:T(8,128)(2,1)S(1)} all-gather(bf16[16,4096]{1,0:T(8,128)(2,1)S(1)} %shard_map.107), channel_id=1, replica_groups=mesh['za'=4,'zb'=4,'y'=4,'x'=4,'c'=2] {'x'}, dimensions={0}, use_global_device_ids=true | all-gather | bytes 655360 | tf_op jit(solution)/shard_map/all_gather | solution.py:163
  146.2 1.9 %collective-permute-start.10 = (bf16[64,4096]{1,0:T(8,128)(2,1)S(1)}, bf16[64,4096]{1,0:T(8,128)(2,1)S(1)}, u32[]{:S(2)}, u32[]{:S(2)}) collective-permute-start(bf16[64,4096]{1,0:T(8,128)(2,1)S(1)} %all_gather.3), channel_id=1, source_target_pairs={{0,1},{1,0},{2,3},{3,2},{4,5},{5,4},{6,7},{7,6},{8,9},{9,8},{10,11... | collective-permute-start | bytes 1572872 | tf_op jit(solution)/shard_map/ppermute | solution.py:19
  148.1 0.0 all-to-all-done.3
  148.1 1.1 reduce_sum.21
  149.2 7.1 %all-to-all-start.4 = ((bf16[16,32,352]{2,1,0:T(8,128)(2,1)}), bf16[16,32,352]{2,1,0:T(8,128)(2,1)S(1)}, u32[]{:S(2)}, u32[]{:S(2)}) async-start(bf16[16,32,352]{2,1,0:T(8,128)(2,1)} %reduce_sum.21), calls=%async_computation.4 | async-start | bytes 786432 | tf_op jit(solution)/shard_map/all_to_all | solution.py:134
  156.3 0.0 collective-permute-done.10
  156.3 0.1 broadcast_select_fusion
  156.4 0.0 copy-start.14
  156.4 1.0 pad_maximum_fusion
  157.5 24.2 %all-to-all-done.4 = bf16[16,32,352]{2,1,0:T(8,128)(2,1)S(1)} async-done(((bf16[16,32,352]{2,1,0:T(8,128)(2,1)}), bf16[16,32,352]{2,1,0:T(8,128)(2,1)S(1)}, u32[]{:S(2)}, u32[]{:S(2)}) %all-to-all-start.4) | async-done | bytes 360480 | tf_op jit(solution)/shard_map/all_to_all | solution.py:134
  181.7 0.1 convert_reduce_fusion
  181.8 0.6 add.13
  (16 shorter events, 0.1 us)
Async XLA Ops:
  37.9 22.1 %all-to-all-start.1 = ((bf16[4,4,96,352]{3,2,1,0:T(8,128)(2,1)}), bf16[4,4,96,352]{3,2,1,0:T(8,128)(2,1)S(1)}, u32[]{:S(2)}, u32[]{:S(2)}) async-start(bf16[4,4,96,352]{3,2,1,0:T(8,128)(2,1)} %broadcast_in_dim.10), calls=%async_computation.1 | async-start | bytes 2359296 | tf_op jit(solution)/shard_map/all_to_all | solution.py:24
  43.7 11.6 %collective-permute-start.2 = (bf16[2,96,352]{2,1,0:T(8,128)(2,1)S(1)}, bf16[2,96,352]{2,1,0:T(8,128)(2,1)S(1)}, u32[]{:S(2)}, u32[]{:S(2)}) collective-permute-start(bf16[2,96,352]{2,1,0:T(8,128)(2,1)S(1)} %get-tuple-element.31), channel_id=1, source_target_pairs={{0,448},{32,480},{64,0},{96,32},{128,64},{160,96},{192,128},{224,1... | collective-permute-start | bytes 405512 | tf_op jit(solution)/shard_map/ppermute | solution.py:19
  49.2 10.7 %collective-permute-start.3 = (bf16[2,96,352]{2,1,0:T(8,128)(2,1)S(1)}, bf16[2,96,352]{2,1,0:T(8,128)(2,1)S(1)}, u32[]{:S(2)}, u32[]{:S(2)}) collective-permute-start(bf16[2,96,352]{2,1,0:T(8,128)(2,1)S(1)} %get-tuple-element.32), channel_id=1, source_target_pairs={{0,64},{32,96},{64,128},{96,160},{128,192},{160,224},{192,256},{22... | collective-permute-start | bytes 405512 | tf_op jit(solution)/shard_map/ppermute | solution.py:19
  61.1 36.5 %all-to-all-start.2 = ((bf16[4,4,96,352]{3,2,1,0:T(8,128)(2,1)}), bf16[4,4,96,352]{3,2,1,0:T(8,128)(2,1)S(1)}, u32[]{:S(2)}, u32[]{:S(2)}) async-start(bf16[4,4,96,352]{3,2,1,0:T(8,128)(2,1)} %broadcast_in_dim.11), calls=%async_computation.2 | async-start | bytes 2359296 | tf_op jit(solution)/shard_map/all_to_all | solution.py:24
  65.9 14.3 %copy-start.13 = (f32[2048]{0:T(1024)S(1)}, f32[2048]{0:T(1024)}, u32[]{:S(2)}) copy-start(f32[2048]{0:T(1024)} %param.11) | copy-start | bytes 24580
  67.3 30.3 %collective-permute-start.4 = (bf16[3,4,96,352]{3,2,1,0:T(8,128)(2,1)}, bf16[3,4,96,352]{3,2,1,0:T(8,128)(2,1)S(1)}, u32[]{:S(2)}, u32[]{:S(2)}) collective-permute-start(bf16[3,4,96,352]{3,2,1,0:T(8,128)(2,1)} %fusion), channel_id=1, source_target_pairs={{0,480},{32,0},{64,32},{96,64},{128,96},{160,128},{192,160},{224,1... | collective-permute-start | bytes 2433032 | tf_op jit(solution)/shard_map/ppermute | solution.py:19
  69.2 28.4 %collective-permute-start.5 = (bf16[3,4,96,352]{3,2,1,0:T(8,128)(2,1)}, bf16[3,4,96,352]{3,2,1,0:T(8,128)(2,1)}, u32[]{:S(2)}, u32[]{:S(2)}) collective-permute-start(bf16[3,4,96,352]{3,2,1,0:T(8,128)(2,1)} %fusion), channel_id=1, source_target_pairs={{0,32},{32,64},{64,96},{96,128},{128,160},{160,192},{192,224},{224... | collective-permute-start | bytes 2433032 | tf_op jit(solution)/shard_map/ppermute | solution.py:19
  73.1 24.5 %collective-permute-start.1 = (bf16[4,96,352]{2,1,0:T(8,128)(2,1)}, bf16[4,96,352]{2,1,0:T(8,128)(2,1)S(1)}, u32[]{:S(2)}, u32[]{:S(2)}) collective-permute-start(bf16[4,96,352]{2,1,0:T(8,128)(2,1)} %all_to_all.25), channel_id=1, source_target_pairs={{0,32},{32,64},{64,96},{96,128},{128,160},{160,192},{192,224},{224... | collective-permute-start | bytes 811016 | tf_op jit(solution)/shard_map/ppermute | solution.py:19
  76.7 20.9 %collective-permute-start = (bf16[4,96,352]{2,1,0:T(8,128)(2,1)}, bf16[4,96,352]{2,1,0:T(8,128)(2,1)}, u32[]{:S(2)}, u32[]{:S(2)}) collective-permute-start(bf16[4,96,352]{2,1,0:T(8,128)(2,1)} %all_to_all.25), channel_id=1, source_target_pairs={{0,480},{32,0},{64,32},{96,64},{128,96},{160,128},{192,160},{224,1... | collective-permute-start | bytes 811016 | tf_op jit(solution)/shard_map/ppermute | solution.py:19
  80.3 1.0 copy-start
  81.3 1.0 copy-start.7
  82.4 1.0 copy-start.8
  84.4 0.8 copy-start.3
  85.2 0.8 copy-start.5
  85.9 0.8 copy-start.11
  97.6 1.0 copy-start.4
  98.7 1.0 copy-start.6
  99.7 4.4 %copy-start.12 = (bf16[128,2048]{1,0:T(8,128)(2,1)S(1)}, bf16[128,2048]{1,0:T(8,128)(2,1)}, u32[]{:S(2)}) copy-start(bf16[128,2048]{1,0:T(8,128)(2,1)} %copy-done.11) | copy-start | bytes 1572868
  102.9 1.1 copy-start.2
  108.7 0.8 copy-start.9
  109.5 6.9 %collective-permute-start.6 = (bf16[64,4096]{1,0:T(8,128)(2,1)}, bf16[64,4096]{1,0:T(8,128)(2,1)S(1)}, u32[]{:S(2)}, u32[]{:S(2)}) collective-permute-start(bf16[64,4096]{1,0:T(8,128)(2,1)} %get-tuple-element.21), channel_id=1, source_target_pairs={{0,1},{1,0},{2,3},{3,2},{4,5},{5,4},{6,7},{7,6},{8,9},{9,8},{10,11... | collective-permute-start | bytes 1572872 | tf_op jit(solution)/shard_map/ppermute | solution.py:19
  111.4 5.0 %copy-start.10 = (bf16[64,4096]{1,0:T(8,128)(2,1)S(1)}, bf16[64,4096]{1,0:T(8,128)(2,1)}, u32[]{:S(2)}) copy-start(bf16[64,4096]{1,0:T(8,128)(2,1)} %copy-done.9) | copy-start | bytes 1572868
  111.4 36.6 %all-to-all-start.3 = ((bf16[4,16,32,352]{3,2,1,0:T(8,128)(2,1)}), bf16[4,16,32,352]{3,2,1,0:T(8,128)(2,1)S(1)}, u32[]{:S(2)}, u32[]{:S(2)}) async-start(bf16[4,16,32,352]{3,2,1,0:T(8,128)(2,1)} %copy-done.2), calls=%async_computation.3 | async-start | bytes 3145728 | tf_op jit(solution)/shard_map/all_to_all | solution.py:134
  116.4 15.6 %copy-start.1 = (bf16[128,2048]{1,0:T(8,128)(2,1)S(1)}, bf16[128,2048]{1,0:T(8,128)(2,1)}, u32[]{:S(2)}) copy-start(bf16[128,2048]{1,0:T(8,128)(2,1)} %bt.3) | copy-start | bytes 1572868
  117.1 11.4 %collective-permute-start.7 = (bf16[16,4096]{1,0:T(8,128)(2,1)S(1)}, bf16[16,4096]{1,0:T(8,128)(2,1)S(1)}, u32[]{:S(2)}, u32[]{:S(2)}) collective-permute-start(bf16[16,4096]{1,0:T(8,128)(2,1)S(1)} %get-tuple-element.23), channel_id=1, source_target_pairs={{0,2},{2,4},{4,6},{6,0},{1,3},{3,5},{5,7},{7,1},{8,10},{10,12},{12... | collective-permute-start | bytes 393224 | tf_op jit(solution)/shard_map/ppermute | solution.py:19
  120.5 8.9 %collective-permute-start.8 = (bf16[16,4096]{1,0:T(8,128)(2,1)S(1)}, bf16[16,4096]{1,0:T(8,128)(2,1)S(1)}, u32[]{:S(2)}, u32[]{:S(2)}) collective-permute-start(bf16[16,4096]{1,0:T(8,128)(2,1)S(1)} %get-tuple-element.24), channel_id=1, source_target_pairs={{0,4},{2,6},{4,0},{6,2},{1,5},{3,7},{5,1},{7,3},{8,12},{10,14},{12... | collective-permute-start | bytes 393224 | tf_op jit(solution)/shard_map/ppermute | solution.py:19
  125.1 6.9 %collective-permute-start.9 = (bf16[16,4096]{1,0:T(8,128)(2,1)S(1)}, bf16[16,4096]{1,0:T(8,128)(2,1)S(1)}, u32[]{:S(2)}, u32[]{:S(2)}) collective-permute-start(bf16[16,4096]{1,0:T(8,128)(2,1)S(1)} %get-tuple-element.25), channel_id=1, source_target_pairs={{0,6},{2,0},{4,2},{6,4},{1,7},{3,1},{5,3},{7,5},{8,14},{10,8},{12,... | collective-permute-start | bytes 393224 | tf_op jit(solution)/shard_map/ppermute | solution.py:19
  146.2 10.2 %collective-permute-start.10 = (bf16[64,4096]{1,0:T(8,128)(2,1)S(1)}, bf16[64,4096]{1,0:T(8,128)(2,1)S(1)}, u32[]{:S(2)}, u32[]{:S(2)}) collective-permute-start(bf16[64,4096]{1,0:T(8,128)(2,1)S(1)} %all_gather.3), channel_id=1, source_target_pairs={{0,1},{1,0},{2,3},{3,2},{4,5},{5,4},{6,7},{7,6},{8,9},{9,8},{10,11... | collective-permute-start | bytes 1572872 | tf_op jit(solution)/shard_map/ppermute | solution.py:19
  149.2 32.5 %all-to-all-start.4 = ((bf16[16,32,352]{2,1,0:T(8,128)(2,1)}), bf16[16,32,352]{2,1,0:T(8,128)(2,1)S(1)}, u32[]{:S(2)}, u32[]{:S(2)}) async-start(bf16[16,32,352]{2,1,0:T(8,128)(2,1)} %reduce_sum.21), calls=%async_computation.4 | async-start | bytes 786432 | tf_op jit(solution)/shard_map/all_to_all | solution.py:134
  156.4 25.4 %copy-start.14 = (f32[32,352]{1,0:T(8,128)S(1)}, f32[32,352]{1,0:T(8,128)}, u32[]{:S(2)}) copy-start(f32[32,352]{1,0:T(8,128)} %param.15) | copy-start | bytes 135172
where the time goes:
time: 184 us; the launch traced here: 182 us
  starting transfers between devices  58.8 us (32%)
  blocking collectives  47.8 us (26%)
  waiting for transfers between devices  45.7 us (25%)
  local copies, waits for them, and re-layouts  13.8 us (8%)
  Pallas kernels  10.2 us (6%)
  other arithmetic  5.2 us (3%)
    ppermute x11, starting transfers between devices, shift(): return lax.ppermute(array, axis, [(k, (k + by) % n) for k in range(n)])  37.2 us
    all_to_all x1, blocking collectives, copies_to_all(): return lax.all_to_all(copies, axis, split_axis=0, concat_axis=0, tiled=True)  34.3 us
    all_to_all x2, waiting for transfers between devices, exchange(): return lax.all_to_all(array, axis, split_axis=0, concat_axis=0, tiled=True)  24.2 us
    ppermute x11, waiting for transfers between devices, shift(): return lax.ppermute(array, axis, [(k, (k + by) % n) for k in range(n)])  21.5 us
    all_gather x1, blocking collectives, shards(): half = lax.all_gather(done, 'x', axis=0, tiled=True)  13.5 us
    all_to_all x2, starting transfers between devices, exchange(): return lax.all_to_all(array, axis, split_axis=0, concat_axis=0, tiled=True)  12 us
    pallas_call x5, Pallas kernels, call(): pl.pallas_call(body, out_shape=tuple((jax.ShapeDtypeStruct(o, BF) for o i...  10.2 us
    all_to_all x2, starting transfers between devices, copies_to_all(): return lax.all_to_all(copies, axis, split_axis=0, concat_axis=0, tiled=True)  9.59 us
  transfers between devices with their start and end apart: 15, of which 6 were waited for; matrix products, arithmetic and copies ran while one was open for 3% of the time, Pallas kernels for 1%

commit v1 on v0

--- a/solution.py
+++ b/solution.py
@@ -54,33 +54,56 @@
             whole[rows, :] = piece[(*spot, slice(m * 32, (m + 1) * 32))]
 
 
-def prepare(at, bt, ft, og, gain, bn, fn, oc):
-    bn[...] = normalize(bt[...], gain[...])
+def prepare(at, bt, ft, og, gain, bo, fn, b0, b1, b2, b3, split):
+    y = at[1]
     fn[...] = normalize(ft[...], gain[...])
-    oc[...] = og[...]
-
-
-def backward(at, bn, og, *refs):
-    pieces, (grads, gd_out, ud_out, wg, wu, wd) = refs[:6], refs[6:]
+    normed = normalize(bt[...], gain[...])
+    bo[0] = normed
+    bo[1] = og[...]
+    tiles = [normed[:, z * 128 : (z + 1) * 128].astype(F32) for z in range(16)]
+    spot = lax.broadcasted_iota(jnp.int32, (128, 128), 1) // 32
+    for yy in range(4):
+        for q in range(4):
+            tile = tiles[4 * q]
+            for j in range(4):
+                moved = tiles[4 * q + j]
+                if j != yy:
+                    moved = pltpu.roll(moved, (j - yy) % 4 * 32, 1)
+                tile = jnp.where(spot == j, moved, tile)
+            split[yy, :, q * 128 : (q + 1) * 128] = tile.astype(BF)
+    for k, out in enumerate((b0, b1, b2, b3)):
+        out[...] = split[(y + k) % 4]
+
+
+def backward(at, bo, *refs):
+    pieces, (gds, both, wg, wu, wd) = refs[:6], refs[6:]
     assemble(at, pieces, (wg, wu, wd))
-    gate = dot(bn[...], wg[...], 1, 0)
-    up = dot(bn[...], wu[...], 1, 0)
-    hid = 0.5 * dot(og[...], wd[...], 1, 0)
+    gate = dot(bo[0], wg[...], 1, 0)
+    up = dot(bo[0], wu[...], 1, 0)
+    hid = 0.5 * dot(bo[1], wd[...], 1, 0)
     s = jax.nn.sigmoid(gate)
     gd = (hid * up * s * (1.0 + gate * (1.0 - s))).astype(BF)
-    gd_out[...] = gd
-    ud_out[...] = (hid * gate * s).astype(BF)
-    part = dot(bn[...], gd, 0, 0).astype(BF)
-    for yy in range(4):
-        for z in range(16):
-            row = (z * 4 + yy) * 32
-            grads[yy, z, :, :] = part[row : row + 32, :]
-
-
-def rest(at, fn, gd, ud, *refs):
+    for k in range(4):
+        for j in range(4):
+            gds[k, j] = gd[j * 32 : (j + 1) * 32, :]
+    both[0] = gd
+    both[1] = (hid * gate * s).astype(BF)
+
+
+def outer(at, b0, b1, b2, b3, gds, grads):
+    y = at[1]
+    total = dot(b0[...], gds[y].reshape(128, 352), 0, 0)
+    for k, piece in ((1, b1), (2, b2), (3, b3)):
+        total = total + dot(piece[...], gds[(y + 4 - k) % 4].reshape(128, 352), 0, 0)
+    total = total.astype(BF)
+    for z in range(16):
+        grads[z] = total[z * 32 : (z + 1) * 32, :]
+
+
+def rest(at, fn, both, *refs):
     pieces, (keep, give, wg, wu, wd, parts) = refs[:6], refs[6:]
     assemble(at, pieces, (wg, wu, wd))
-    diff = dot(gd[...], wg[...], 1, 1) + dot(ud[...], wu[...], 1, 1)
+    diff = dot(both[0], wg[...], 1, 1) + dot(both[1], wu[...], 1, 1)
     parts[:, 2048:4096] = diff.astype(BF)
     gate = dot(fn[...], wg[...], 1, 0)
     up = dot(fn[...], wu[...], 1, 0)
@@ -128,6 +151,7 @@
 W = (2048, 352)
 TOK = (128, 2048)
 HID = (128, 352)
+COL = (128, 512)
 
 
 def exchange(array, axis):
@@ -150,15 +174,20 @@
     z3 = shift(others, Z, 1)
     far = copies_to_all(a2, "y")
     pieces = (near, a1, a3, far, z1, z3)
-    bn, fn, oc = call(prepare, (TOK,) * 3, (), at, bt, ft, og, gain)
-    grads, gd, ud = call(backward, ((4, 16, 32, 352), HID, HID), (W,) * 3, at, bn, oc, *pieces)
-    gy = exchange(grads, "y")
-    keep, give = call(rest, ((64, 4096),) * 2, (W, W, W, (128, 4096)), at, fn, gd, ud, *pieces)
+    bo, fn, b0, b1, b2, b3 = call(
+        prepare, ((2, *TOK), TOK) + (COL,) * 4, ((4, *COL),), at, bt, ft, og, gain
+    )
+    b1 = shift(b1, "y", 1)
+    b2 = shift(b2, "y", 2)
+    b3 = shift(b3, "y", 3)
+    gds, both = call(backward, ((4, 4, 32, 352), (2, *HID)), (W,) * 3, at, bo, *pieces)
+    gds = exchange(gds, "y")
+    keep, give = call(rest, ((64, 4096),) * 2, (W, W, W, (128, 4096)), at, fn, both, *pieces)
+    (grads,) = call(outer, ((16, 32, 352),), (), at, b0, b1, b2, b3, gds)
+    gz = exchange(grads, Z)
     other = shift(give, "c", 1)
     p0, p1, p2, p3 = call(pair, ((16, 4096),) * 4, (), at, keep, other)
     p1, p2, p3 = shift(p1, "x", 1), shift(p2, "x", 2), shift(p3, "x", -1)
-    gy = gy.astype(F32).sum(axis=0).astype(BF)
-    gz = exchange(gy, Z)
     (done,) = call(finish, ((16, 4096),), (), at, p0, p1, p2, p3, bt, gain)
     half = lax.all_gather(done, "x", axis=0, tiled=True)
     other = shift(half, "c", 1)

time: 184 us -> 196 us (1.065)
  the two profiles are of different devices: /device:TPU:16 before, /device:TPU:8 now
where the time goes in v1:
time: 196 us; the launch traced here: 195 us
  starting transfers between devices  69.3 us (35%)
  waiting for transfers between devices  47.8 us (24%)
  blocking collectives  47.5 us (24%)
  local copies, waits for them, and re-layouts  13.1 us (7%)
  Pallas kernels  12 us (6%)
  other arithmetic  4.05 us (2%)
    ppermute x14, starting transfers between devices, shift(): return lax.ppermute(array, axis, [(k, (k + by) % n) for k in range(n)])  47.7 us
    all_to_all x1, blocking collectives, copies_to_all(): return lax.all_to_all(copies, axis, split_axis=0, concat_axis=0, tiled=True)  34.3 us
    ppermute x14, waiting for transfers between devices, shift(): return lax.ppermute(array, axis, [(k, (k + by) % n) for k in range(n)])  25.1 us
    all_to_all x2, waiting for transfers between devices, exchange(): return lax.all_to_all(array, axis, split_axis=0, concat_axis=0, tiled=True)  22.8 us
    all_gather x1, blocking collectives, shards(): half = lax.all_gather(done, 'x', axis=0, tiled=True)  13.1 us
    pallas_call x6, Pallas kernels, call(): pl.pallas_call(body, out_shape=tuple((jax.ShapeDtypeStruct(o, BF) for o i...  12 us
    all_to_all x2, starting transfers between devices, exchange(): return lax.all_to_all(array, axis, split_axis=0, concat_axis=0, tiled=True)  11.9 us
    all_to_all x2, starting transfers between devices, copies_to_all(): return lax.all_to_all(copies, axis, split_axis=0, concat_axis=0, tiled=True)  9.71 us
  transfers between devices with their start and end apart: 18, of which 9 were waited for; matrix products, arithmetic and copies ran while one was open for 2% of the time, Pallas kernels for 2%

profile of v1, /device:TPU:8, one launch (start us, length us, event | category | flops | bytes accessed | tf_op | source)
XLA Modules:
  0.0 194.7 jit_solution(13073673204419354701)
XLA Ops:
  0.6 0.8 pad_maximum_fusion.2
  1.5 34.3 %all_to_all.25 = bf16[4,96,352]{2,1,0:T(8,128)(2,1)} all-to-all(bf16[4,96,352]{2,1,0:T(8,128)(2,1)S(1)} %broadcast_in_dim.9), channel_id=1, replica_groups=mesh['za'=4,'zb'=4,'y'=4,'x'=4,'c'=2] {'za'}, dimensions={0} | all-to-all | bytes 540672 | tf_op jit(solution)/shard_map/all_to_all | solution.py:24
  35.8 2.1 %broadcast_in_dim.10 = bf16[4,4,96,352]{3,2,1,0:T(8,128)(2,1)} broadcast(bf16[4,96,352]{2,1,0:T(8,128)(2,1)} %all_to_all.25), dimensions={1,2,3} | broadcast | bytes 1351680 | tf_op jit(solution)/shard_map/broadcast_in_dim | solution.py:23
  37.9 4.9 %all-to-all-start.1 = ((bf16[4,4,96,352]{3,2,1,0:T(8,128)(2,1)}), bf16[4,4,96,352]{3,2,1,0:T(8,128)(2,1)S(1)}, u32[]{:S(2)}, u32[]{:S(2)}) async-start(bf16[4,4,96,352]{3,2,1,0:T(8,128)(2,1)} %broadcast_in_dim.10), calls=%async_computation.1 | async-start | bytes 2359296 | tf_op jit(solution)/shard_map/all_to_all | solution.py:24
  42.8 1.0 fusion.2
  43.8 5.5 %collective-permute-start.2 = (bf16[2,96,352]{2,1,0:T(8,128)(2,1)S(1)}, bf16[2,96,352]{2,1,0:T(8,128)(2,1)S(1)}, u32[]{:S(2)}, u32[]{:S(2)}) collective-permute-start(bf16[2,96,352]{2,1,0:T(8,128)(2,1)S(1)} %get-tuple-element.35), channel_id=1, source_target_pairs={{0,448},{32,480},{64,0},{96,32},{128,64},{160,96},{192,128},{224,1... | collective-permute-start | bytes 405512 | tf_op jit(solution)/shard_map/ppermute | solution.py:19
  49.3 3.6 %collective-permute-start.3 = (bf16[2,96,352]{2,1,0:T(8,128)(2,1)S(1)}, bf16[2,96,352]{2,1,0:T(8,128)(2,1)S(1)}, u32[]{:S(2)}, u32[]{:S(2)}) collective-permute-start(bf16[2,96,352]{2,1,0:T(8,128)(2,1)S(1)} %get-tuple-element.36), channel_id=1, source_target_pairs={{0,64},{32,96},{64,128},{96,160},{128,192},{160,224},{192,256},{22... | collective-permute-start | bytes 405512 | tf_op jit(solution)/shard_map/ppermute | solution.py:19
  52.9 2.5 %collective-permute-done.2 = bf16[2,96,352]{2,1,0:T(8,128)(2,1)S(1)} collective-permute-done((bf16[2,96,352]{2,1,0:T(8,128)(2,1)S(1)}, bf16[2,96,352]{2,1,0:T(8,128)(2,1)S(1)}, u32[]{:S(2)}, u32[]{:S(2)}) %collective-permute-start.2) | collective-permute-done | bytes 135200 | tf_op jit(solution)/shard_map/ppermute | solution.py:19
  55.5 4.6 %collective-permute-done.3 = bf16[2,96,352]{2,1,0:T(8,128)(2,1)S(1)} collective-permute-done((bf16[2,96,352]{2,1,0:T(8,128)(2,1)S(1)}, bf16[2,96,352]{2,1,0:T(8,128)(2,1)S(1)}, u32[]{:S(2)}, u32[]{:S(2)}) %collective-permute-start.3) | collective-permute-done | bytes 135200 | tf_op jit(solution)/shard_map/ppermute | solution.py:19
  60.0 0.1 pad_maximum_fusion.1
  60.1 0.0 all-to-all-done.1.refs_0_
  60.1 1.2 broadcast_in_dim.11
  61.3 4.8 %all-to-all-start.2 = ((bf16[4,4,96,352]{3,2,1,0:T(8,128)(2,1)}), bf16[4,4,96,352]{3,2,1,0:T(8,128)(2,1)S(1)}, u32[]{:S(2)}, u32[]{:S(2)}) async-start(bf16[4,4,96,352]{3,2,1,0:T(8,128)(2,1)} %broadcast_in_dim.11), calls=%async_computation.2 | async-start | bytes 2359296 | tf_op jit(solution)/shard_map/all_to_all | solution.py:24
  66.1 1.3 fusion
  67.4 1.9 collective-permute-start.4
  69.3 3.9 %collective-permute-start.5 = (bf16[3,4,96,352]{3,2,1,0:T(8,128)(2,1)}, bf16[3,4,96,352]{3,2,1,0:T(8,128)(2,1)}, u32[]{:S(2)}, u32[]{:S(2)}) collective-permute-start(bf16[3,4,96,352]{3,2,1,0:T(8,128)(2,1)} %fusion), channel_id=1, source_target_pairs={{0,32},{32,64},{64,96},{96,128},{128,160},{160,192},{192,224},{224... | collective-permute-start | bytes 2433032 | tf_op jit(solution)/shard_map/ppermute | solution.py:19
  73.2 3.6 %collective-permute-start.1 = (bf16[4,96,352]{2,1,0:T(8,128)(2,1)}, bf16[4,96,352]{2,1,0:T(8,128)(2,1)S(1)}, u32[]{:S(2)}, u32[]{:S(2)}) collective-permute-start(bf16[4,96,352]{2,1,0:T(8,128)(2,1)} %all_to_all.25), channel_id=1, source_target_pairs={{0,32},{32,64},{64,96},{96,128},{128,160},{160,192},{192,224},{224... | collective-permute-start | bytes 811016 | tf_op jit(solution)/shard_map/ppermute | solution.py:19
  76.8 3.5 %collective-permute-start = (bf16[4,96,352]{2,1,0:T(8,128)(2,1)}, bf16[4,96,352]{2,1,0:T(8,128)(2,1)}, u32[]{:S(2)}, u32[]{:S(2)}) collective-permute-start(bf16[4,96,352]{2,1,0:T(8,128)(2,1)} %all_to_all.25), channel_id=1, source_target_pairs={{0,480},{32,0},{64,32},{96,64},{128,96},{160,128},{192,160},{224,1... | collective-permute-start | bytes 811016 | tf_op jit(solution)/shard_map/ppermute | solution.py:19
  80.3 0.1 pad_add_fusion.at
  80.4 1.0 copy-done
  81.4 1.0 copy-done.4
  82.5 1.0 copy-done.5
  83.5 1.4 shard_map.103
  85.0 1.0 copy-done.2
  85.9 0.8 copy-done.6
  86.7 0.6 copy-done.8
  87.4 0.6 copy-done.11
  88.0 0.7 copy-done.13
  88.7 0.7 copy-done.15
  89.3 8.4 %collective-permute-done.1.refs_2_ = bf16[4,96,352]{2,1,0:T(8,128)(2,1)S(1)} collective-permute-done((bf16[4,96,352]{2,1,0:T(8,128)(2,1)}, bf16[4,96,352]{2,1,0:T(8,128)(2,1)S(1)}, u32[]{:S(2)}, u32[]{:S(2)}) %collective-permute-start.1) | collective-permute-done | bytes 270368 | tf_op jit(solution)/shard_map/ppermute | solution.py:19
  97.7 0.0 collective-permute-done.refs_1_
  97.7 0.0 all-to-all-done.2.refs_3_
  97.7 0.0 collective-permute-done.4.refs_4_
  97.8 1.2 copy-done.3
  99.0 3.5 %shard_map.104 = (bf16[4,4,32,352]{3,2,1,0:T(8,128)(2,1)}, bf16[2,128,352]{2,1,0:T(8,128)(2,1)S(1)}) custom-call(s32[4]{0:T(128)S(1)} %pad_add_fusion.at, bf16[2,128,2048]{2,1,0:T(8,128)(2,1)S(1)} %copy-done.3, bf16[4,4,96,352]{3,2,1,0:T(8,128)(2,1)S(1)} %all-to-all-done.1.refs_0_, bf16[4,96,352]{2,1,0:T(8,128)(2,1)} %collective-permute-done.refs_1_, ...), custom_call_target="tpu_custom_call" | custom-call | tf_op jit(solution)/shard_map/pallas_call | solution.py:140
  102.4 3.8 %shard_map.105 = (bf16[64,4096]{1,0:T(8,128)(2,1)S(1)}, bf16[64,4096]{1,0:T(8,128)(2,1)S(1)}) custom-call(s32[4]{0:T(128)S(1)} %pad_add_fusion.at, bf16[128,2048]{1,0:T(8,128)(2,1)S(1)} %copy-done.7, bf16[2,128,352]{2,1,0:T(8,128)(2,1)S(1)} %get-tuple-element.19.both, bf16[4,4,96,352]{3,2,1,0:T(8,128)(2,1)S(1)} %all-to-all-done.1.refs_0_, ...), custom_call_target="tpu_custom_call" | custom-call | tf_op jit(solution)/shard_map/pallas_call | solution.py:140
  106.3 0.0 copy-start.1
  106.3 2.1 %collective-permute-start.6 = (bf16[64,4096]{1,0:T(8,128)(2,1)S(1)}, bf16[64,4096]{1,0:T(8,128)(2,1)S(1)}, u32[]{:S(2)}, u32[]{:S(2)}) collective-permute-start(bf16[64,4096]{1,0:T(8,128)(2,1)S(1)} %get-tuple-element.21), channel_id=1, source_target_pairs={{0,1},{1,0},{2,3},{3,2},{4,5},{5,4},{6,7},{7,6},{8,9},{9,8},{10,11... | collective-permute-start | bytes 1572872 | tf_op jit(solution)/shard_map/ppermute | solution.py:19
  108.3 1.9 collective-permute-done.6.other
  110.2 0.7 shard_map.106
  110.9 3.4 %collective-permute-start.7 = (bf16[16,4096]{1,0:T(8,128)(2,1)S(1)}, bf16[16,4096]{1,0:T(8,128)(2,1)S(1)}, u32[]{:S(2)}, u32[]{:S(2)}) collective-permute-start(bf16[16,4096]{1,0:T(8,128)(2,1)S(1)} %get-tuple-element.23), channel_id=1, source_target_pairs={{0,2},{2,4},{4,6},{6,0},{1,3},{3,5},{5,7},{7,1},{8,10},{10,12},{12... | collective-permute-start | bytes 393224 | tf_op jit(solution)/shard_map/ppermute | solution.py:19
  114.3 4.6 %collective-permute-start.8 = (bf16[16,4096]{1,0:T(8,128)(2,1)S(1)}, bf16[16,4096]{1,0:T(8,128)(2,1)S(1)}, u32[]{:S(2)}, u32[]{:S(2)}) collective-permute-start(bf16[16,4096]{1,0:T(8,128)(2,1)S(1)} %get-tuple-element.24), channel_id=1, source_target_pairs={{0,4},{2,6},{4,0},{6,2},{1,5},{3,7},{5,1},{7,3},{8,12},{10,14},{12... | collective-permute-start | bytes 393224 | tf_op jit(solution)/shard_map/ppermute | solution.py:19
  119.0 3.3 %collective-permute-start.9 = (bf16[16,4096]{1,0:T(8,128)(2,1)S(1)}, bf16[16,4096]{1,0:T(8,128)(2,1)S(1)}, u32[]{:S(2)}, u32[]{:S(2)}) collective-permute-start(bf16[16,4096]{1,0:T(8,128)(2,1)S(1)} %get-tuple-element.25), channel_id=1, source_target_pairs={{0,6},{2,0},{4,2},{6,4},{1,7},{3,1},{5,3},{7,5},{8,14},{10,8},{12,... | collective-permute-start | bytes 393224 | tf_op jit(solution)/shard_map/ppermute | solution.py:19
  122.3 0.0 collective-permute-done.7.p1
  122.3 1.0 collective-permute-done.8.p2
  123.4 2.5 %collective-permute-done.9.p3 = bf16[16,4096]{1,0:T(8,128)(2,1)S(1)} collective-permute-done((bf16[16,4096]{1,0:T(8,128)(2,1)S(1)}, bf16[16,4096]{1,0:T(8,128)(2,1)S(1)}, u32[]{:S(2)}, u32[]{:S(2)}) %collective-permute-start.9) | collective-permute-done | bytes 131104 | tf_op jit(solution)/shard_map/ppermute | solution.py:19
  125.9 0.7 shard_map.107
  126.6 13.1 %all_gather.3 = bf16[64,4096]{1,0:T(8,128)(2,1)S(1)} all-gather(bf16[16,4096]{1,0:T(8,128)(2,1)S(1)} %shard_map.107), channel_id=1, replica_groups=mesh['za'=4,'zb'=4,'y'=4,'x'=4,'c'=2] {'x'}, dimensions={0}, use_global_device_ids=true | all-gather | bytes 655360 | tf_op jit(solution)/shard_map/all_gather | solution.py:192
  139.7 1.9 collective-permute-start.10
  141.6 4.8 %all-to-all-start.3 = ((bf16[4,4,32,352]{3,2,1,0:T(8,128)(2,1)}), bf16[4,4,32,352]{3,2,1,0:T(8,128)(2,1)S(1)}, u32[]{:S(2)}, u32[]{:S(2)}) async-start(bf16[4,4,32,352]{3,2,1,0:T(8,128)(2,1)} %get-tuple-element.30), calls=%async_computation.3 | async-start | bytes 786432 | tf_op jit(solution)/shard_map/all_to_all | solution.py:158
  146.4 3.4 %collective-permute-start.11 = (bf16[128,512]{1,0:T(8,128)(2,1)S(1)}, bf16[128,512]{1,0:T(8,128)(2,1)S(1)}, u32[]{:S(2)}, u32[]{:S(2)}) collective-permute-start(bf16[128,512]{1,0:T(8,128)(2,1)S(1)} %copy-done.16), channel_id=1, source_target_pairs={{0,8},{8,16},{16,24},{24,0},{1,9},{9,17},{17,25},{25,1},{2,10},{10... | collective-permute-start | bytes 393224 | tf_op jit(solution)/shard_map/ppermute | solution.py:19
  149.8 2.5 %collective-permute-start.12 = (bf16[128,512]{1,0:T(8,128)(2,1)S(1)}, bf16[128,512]{1,0:T(8,128)(2,1)S(1)}, u32[]{:S(2)}, u32[]{:S(2)}) collective-permute-start(bf16[128,512]{1,0:T(8,128)(2,1)S(1)} %copy-done.14), channel_id=1, source_target_pairs={{0,16},{8,24},{16,0},{24,8},{1,17},{9,25},{17,1},{25,9},{2,18},{10... | collective-permute-start | bytes 393224 | tf_op jit(solution)/shard_map/ppermute | solution.py:19
  152.3 4.5 %collective-permute-start.13 = (bf16[128,512]{1,0:T(8,128)(2,1)S(1)}, bf16[128,512]{1,0:T(8,128)(2,1)S(1)}, u32[]{:S(2)}, u32[]{:S(2)}) collective-permute-start(bf16[128,512]{1,0:T(8,128)(2,1)S(1)} %copy-done.12), channel_id=1, source_target_pairs={{0,24},{8,0},{16,8},{24,16},{1,25},{9,1},{17,9},{25,17},{2,26},{10... | collective-permute-start | bytes 393224 | tf_op jit(solution)/shard_map/ppermute | solution.py:19
  156.8 2.2 %collective-permute-done.12.b2 = bf16[128,512]{1,0:T(8,128)(2,1)S(1)} collective-permute-done((bf16[128,512]{1,0:T(8,128)(2,1)S(1)}, bf16[128,512]{1,0:T(8,128)(2,1)S(1)}, u32[]{:S(2)}, u32[]{:S(2)}) %collective-permute-start.12) | collective-permute-done | bytes 131104 | tf_op jit(solution)/shard_map/ppermute | solution.py:19
  159.1 1.9 collective-permute-done.13.b3
  161.0 1.9 shard_map.108
  162.9 7.1 %all-to-all-start.4 = ((bf16[16,32,352]{2,1,0:T(8,128)(2,1)}), bf16[16,32,352]{2,1,0:T(8,128)(2,1)S(1)}, u32[]{:S(2)}, u32[]{:S(2)}) async-start(bf16[16,32,352]{2,1,0:T(8,128)(2,1)} %shard_map.108), calls=%async_computation.4 | async-start | bytes 786432 | tf_op jit(solution)/shard_map/all_to_all | solution.py:158
  170.1 0.0 collective-permute-done.10
  170.1 0.1 broadcast_select_fusion
  170.2 0.0 copy-start.17
  170.2 1.0 pad_maximum_fusion
  171.2 22.8 %all-to-all-done.4 = bf16[16,32,352]{2,1,0:T(8,128)(2,1)S(1)} async-done(((bf16[16,32,352]{2,1,0:T(8,128)(2,1)}), bf16[16,32,352]{2,1,0:T(8,128)(2,1)S(1)}, u32[]{:S(2)}, u32[]{:S(2)}) %all-to-all-start.4) | async-done | bytes 360480 | tf_op jit(solution)/shard_map/all_to_all | solution.py:158
  194.0 0.1 convert_reduce_fusion
  194.1 0.6 add.13
  (28 shorter events, 0.1 us)
Async XLA Ops:
  37.9 22.2 %all-to-all-start.1 = ((bf16[4,4,96,352]{3,2,1,0:T(8,128)(2,1)}), bf16[4,4,96,352]{3,2,1,0:T(8,128)(2,1)S(1)}, u32[]{:S(2)}, u32[]{:S(2)}) async-start(bf16[4,4,96,352]{3,2,1,0:T(8,128)(2,1)} %broadcast_in_dim.10), calls=%async_computation.1 | async-start | bytes 2359296 | tf_op jit(solution)/shard_map/all_to_all | solution.py:24
  43.8 11.6 %collective-permute-start.2 = (bf16[2,96,352]{2,1,0:T(8,128)(2,1)S(1)}, bf16[2,96,352]{2,1,0:T(8,128)(2,1)S(1)}, u32[]{:S(2)}, u32[]{:S(2)}) collective-permute-start(bf16[2,96,352]{2,1,0:T(8,128)(2,1)S(1)} %get-tuple-element.35), channel_id=1, source_target_pairs={{0,448},{32,480},{64,0},{96,32},{128,64},{160,96},{192,128},{224,1... | collective-permute-start | bytes 405512 | tf_op jit(solution)/shard_map/ppermute | solution.py:19
  49.3 10.7 %collective-permute-start.3 = (bf16[2,96,352]{2,1,0:T(8,128)(2,1)S(1)}, bf16[2,96,352]{2,1,0:T(8,128)(2,1)S(1)}, u32[]{:S(2)}, u32[]{:S(2)}) collective-permute-start(bf16[2,96,352]{2,1,0:T(8,128)(2,1)S(1)} %get-tuple-element.36), channel_id=1, source_target_pairs={{0,64},{32,96},{64,128},{96,160},{128,192},{160,224},{192,256},{22... | collective-permute-start | bytes 405512 | tf_op jit(solution)/shard_map/ppermute | solution.py:19
  61.3 36.5 %all-to-all-start.2 = ((bf16[4,4,96,352]{3,2,1,0:T(8,128)(2,1)}), bf16[4,4,96,352]{3,2,1,0:T(8,128)(2,1)S(1)}, u32[]{:S(2)}, u32[]{:S(2)}) async-start(bf16[4,4,96,352]{3,2,1,0:T(8,128)(2,1)} %broadcast_in_dim.11), calls=%async_computation.2 | async-start | bytes 2359296 | tf_op jit(solution)/shard_map/all_to_all | solution.py:24
  66.1 14.3 %copy-start.10 = (f32[2048]{0:T(1024)S(1)}, f32[2048]{0:T(1024)}, u32[]{:S(2)}) copy-start(f32[2048]{0:T(1024)} %param.11) | copy-start | bytes 24580
  67.4 30.3 %collective-permute-start.4 = (bf16[3,4,96,352]{3,2,1,0:T(8,128)(2,1)}, bf16[3,4,96,352]{3,2,1,0:T(8,128)(2,1)S(1)}, u32[]{:S(2)}, u32[]{:S(2)}) collective-permute-start(bf16[3,4,96,352]{3,2,1,0:T(8,128)(2,1)} %fusion), channel_id=1, source_target_pairs={{0,480},{32,0},{64,32},{96,64},{128,96},{160,128},{192,160},{224,1... | collective-permute-start | bytes 2433032 | tf_op jit(solution)/shard_map/ppermute | solution.py:19
  69.3 28.4 %collective-permute-start.5 = (bf16[3,4,96,352]{3,2,1,0:T(8,128)(2,1)}, bf16[3,4,96,352]{3,2,1,0:T(8,128)(2,1)}, u32[]{:S(2)}, u32[]{:S(2)}) collective-permute-start(bf16[3,4,96,352]{3,2,1,0:T(8,128)(2,1)} %fusion), channel_id=1, source_target_pairs={{0,32},{32,64},{64,96},{96,128},{128,160},{160,192},{192,224},{224... | collective-permute-start | bytes 2433032 | tf_op jit(solution)/shard_map/ppermute | solution.py:19
  73.2 24.5 %collective-permute-start.1 = (bf16[4,96,352]{2,1,0:T(8,128)(2,1)}, bf16[4,96,352]{2,1,0:T(8,128)(2,1)S(1)}, u32[]{:S(2)}, u32[]{:S(2)}) collective-permute-start(bf16[4,96,352]{2,1,0:T(8,128)(2,1)} %all_to_all.25), channel_id=1, source_target_pairs={{0,32},{32,64},{64,96},{96,128},{128,160},{160,192},{192,224},{224... | collective-permute-start | bytes 811016 | tf_op jit(solution)/shard_map/ppermute | solution.py:19
  76.8 20.9 %collective-permute-start = (bf16[4,96,352]{2,1,0:T(8,128)(2,1)}, bf16[4,96,352]{2,1,0:T(8,128)(2,1)}, u32[]{:S(2)}, u32[]{:S(2)}) collective-permute-start(bf16[4,96,352]{2,1,0:T(8,128)(2,1)} %all_to_all.25), channel_id=1, source_target_pairs={{0,480},{32,0},{64,32},{96,64},{128,96},{160,128},{192,160},{224,1... | collective-permute-start | bytes 811016 | tf_op jit(solution)/shard_map/ppermute | solution.py:19
  80.4 1.0 copy-start
  81.4 1.0 copy-start.4
  82.5 1.0 copy-start.5
  85.0 1.0 copy-start.2
  85.9 0.8 copy-start.6
  86.7 0.6 copy-start.8
  87.4 0.6 copy-start.11
  88.0 0.7 copy-start.13
  88.7 0.7 copy-start.15
  97.7 1.2 copy-start.3
  99.0 3.5 %copy-start.7 = (bf16[128,2048]{1,0:T(8,128)(2,1)S(1)}, bf16[128,2048]{1,0:T(8,128)(2,1)}, u32[]{:S(2)}) copy-start(bf16[128,2048]{1,0:T(8,128)(2,1)} %copy-done.6) | copy-start | bytes 1572868
  106.3 19.6 %copy-start.1 = (bf16[128,2048]{1,0:T(8,128)(2,1)S(1)}, bf16[128,2048]{1,0:T(8,128)(2,1)}, u32[]{:S(2)}) copy-start(bf16[128,2048]{1,0:T(8,128)(2,1)} %bt.3) | copy-start | bytes 1572868
  106.3 3.9 %collective-permute-start.6 = (bf16[64,4096]{1,0:T(8,128)(2,1)S(1)}, bf16[64,4096]{1,0:T(8,128)(2,1)S(1)}, u32[]{:S(2)}, u32[]{:S(2)}) collective-permute-start(bf16[64,4096]{1,0:T(8,128)(2,1)S(1)} %get-tuple-element.21), channel_id=1, source_target_pairs={{0,1},{1,0},{2,3},{3,2},{4,5},{5,4},{6,7},{7,6},{8,9},{9,8},{10,11... | collective-permute-start | bytes 1572872 | tf_op jit(solution)/shard_map/ppermute | solution.py:19
  110.9 11.4 %collective-permute-start.7 = (bf16[16,4096]{1,0:T(8,128)(2,1)S(1)}, bf16[16,4096]{1,0:T(8,128)(2,1)S(1)}, u32[]{:S(2)}, u32[]{:S(2)}) collective-permute-start(bf16[16,4096]{1,0:T(8,128)(2,1)S(1)} %get-tuple-element.23), channel_id=1, source_target_pairs={{0,2},{2,4},{4,6},{6,0},{1,3},{3,5},{5,7},{7,1},{8,10},{10,12},{12... | collective-permute-start | bytes 393224 | tf_op jit(solution)/shard_map/ppermute | solution.py:19
  114.3 9.0 %collective-permute-start.8 = (bf16[16,4096]{1,0:T(8,128)(2,1)S(1)}, bf16[16,4096]{1,0:T(8,128)(2,1)S(1)}, u32[]{:S(2)}, u32[]{:S(2)}) collective-permute-start(bf16[16,4096]{1,0:T(8,128)(2,1)S(1)} %get-tuple-element.24), channel_id=1, source_target_pairs={{0,4},{2,6},{4,0},{6,2},{1,5},{3,7},{5,1},{7,3},{8,12},{10,14},{12... | collective-permute-start | bytes 393224 | tf_op jit(solution)/shard_map/ppermute | solution.py:19
  119.0 6.9 %collective-permute-start.9 = (bf16[16,4096]{1,0:T(8,128)(2,1)S(1)}, bf16[16,4096]{1,0:T(8,128)(2,1)S(1)}, u32[]{:S(2)}, u32[]{:S(2)}) collective-permute-start(bf16[16,4096]{1,0:T(8,128)(2,1)S(1)} %get-tuple-element.25), channel_id=1, source_target_pairs={{0,6},{2,0},{4,2},{6,4},{1,7},{3,1},{5,3},{7,5},{8,14},{10,8},{12,... | collective-permute-start | bytes 393224 | tf_op jit(solution)/shard_map/ppermute | solution.py:19
  125.8 20.5 %copy-start.16 = (bf16[128,512]{1,0:T(8,128)(2,1)S(1)}, bf16[128,512]{1,0:T(8,128)(2,1)}, u32[]{:S(2)}) copy-start(bf16[128,512]{1,0:T(8,128)(2,1)} %copy-done.15) | copy-start | bytes 393220
  125.8 23.9 %copy-start.14 = (bf16[128,512]{1,0:T(8,128)(2,1)S(1)}, bf16[128,512]{1,0:T(8,128)(2,1)}, u32[]{:S(2)}) copy-start(bf16[128,512]{1,0:T(8,128)(2,1)} %copy-done.13) | copy-start | bytes 393220
  125.8 26.4 %copy-start.12 = (bf16[128,512]{1,0:T(8,128)(2,1)S(1)}, bf16[128,512]{1,0:T(8,128)(2,1)}, u32[]{:S(2)}) copy-start(bf16[128,512]{1,0:T(8,128)(2,1)} %copy-done.11) | copy-start | bytes 393220
  125.9 35.2 %copy-start.9 = (bf16[128,512]{1,0:T(8,128)(2,1)S(1)}, bf16[128,512]{1,0:T(8,128)(2,1)}, u32[]{:S(2)}) copy-start(bf16[128,512]{1,0:T(8,128)(2,1)} %copy-done.8) | copy-start | bytes 393220
  139.7 30.4 %collective-permute-start.10 = (bf16[64,4096]{1,0:T(8,128)(2,1)S(1)}, bf16[64,4096]{1,0:T(8,128)(2,1)S(1)}, u32[]{:S(2)}, u32[]{:S(2)}) collective-permute-start(bf16[64,4096]{1,0:T(8,128)(2,1)S(1)} %all_gather.3), channel_id=1, source_target_pairs={{0,1},{1,0},{2,3},{3,2},{4,5},{5,4},{6,7},{7,6},{8,9},{9,8},{10,11... | collective-permute-start | bytes 1572872 | tf_op jit(solution)/shard_map/ppermute | solution.py:19
  141.6 19.4 %all-to-all-start.3 = ((bf16[4,4,32,352]{3,2,1,0:T(8,128)(2,1)}), bf16[4,4,32,352]{3,2,1,0:T(8,128)(2,1)S(1)}, u32[]{:S(2)}, u32[]{:S(2)}) async-start(bf16[4,4,32,352]{3,2,1,0:T(8,128)(2,1)} %get-tuple-element.30), calls=%async_computation.3 | async-start | bytes 786432 | tf_op jit(solution)/shard_map/all_to_all | solution.py:158
  146.4 10.5 %collective-permute-start.11 = (bf16[128,512]{1,0:T(8,128)(2,1)S(1)}, bf16[128,512]{1,0:T(8,128)(2,1)S(1)}, u32[]{:S(2)}, u32[]{:S(2)}) collective-permute-start(bf16[128,512]{1,0:T(8,128)(2,1)S(1)} %copy-done.16), channel_id=1, source_target_pairs={{0,8},{8,16},{16,24},{24,0},{1,9},{9,17},{17,25},{25,1},{2,10},{10... | collective-permute-start | bytes 393224 | tf_op jit(solution)/shard_map/ppermute | solution.py:19
  149.8 9.3 %collective-permute-start.12 = (bf16[128,512]{1,0:T(8,128)(2,1)S(1)}, bf16[128,512]{1,0:T(8,128)(2,1)S(1)}, u32[]{:S(2)}, u32[]{:S(2)}) collective-permute-start(bf16[128,512]{1,0:T(8,128)(2,1)S(1)} %copy-done.14), channel_id=1, source_target_pairs={{0,16},{8,24},{16,0},{24,8},{1,17},{9,25},{17,1},{25,9},{2,18},{10... | collective-permute-start | bytes 393224 | tf_op jit(solution)/shard_map/ppermute | solution.py:19
  152.3 8.7 %collective-permute-start.13 = (bf16[128,512]{1,0:T(8,128)(2,1)S(1)}, bf16[128,512]{1,0:T(8,128)(2,1)S(1)}, u32[]{:S(2)}, u32[]{:S(2)}) collective-permute-start(bf16[128,512]{1,0:T(8,128)(2,1)S(1)} %copy-done.12), channel_id=1, source_target_pairs={{0,24},{8,0},{16,8},{24,16},{1,25},{9,1},{17,9},{25,17},{2,26},{10... | collective-permute-start | bytes 393224 | tf_op jit(solution)/shard_map/ppermute | solution.py:19
  162.9 31.1 %all-to-all-start.4 = ((bf16[16,32,352]{2,1,0:T(8,128)(2,1)}), bf16[16,32,352]{2,1,0:T(8,128)(2,1)S(1)}, u32[]{:S(2)}, u32[]{:S(2)}) async-start(bf16[16,32,352]{2,1,0:T(8,128)(2,1)} %shard_map.108), calls=%async_computation.4 | async-start | bytes 786432 | tf_op jit(solution)/shard_map/all_to_all | solution.py:158
  170.2 23.9 %copy-start.17 = (f32[32,352]{1,0:T(8,128)S(1)}, f32[32,352]{1,0:T(8,128)}, u32[]{:S(2)}) copy-start(f32[32,352]{1,0:T(8,128)} %param.15) | copy-start | bytes 135172

commit v2 on v1

--- a/solution.py
+++ b/solution.py
@@ -90,11 +90,15 @@
     both[1] = (hid * gate * s).astype(BF)
 
 
-def outer(at, b0, b1, b2, b3, gds, grads):
-    y = at[1]
-    total = dot(b0[...], gds[y].reshape(128, 352), 0, 0)
-    for k, piece in ((1, b1), (2, b2), (3, b3)):
-        total = total + dot(piece[...], gds[(y + 4 - k) % 4].reshape(128, 352), 0, 0)
+def merge(at, b0, b1, b2, b3, out):
+    for k, piece in enumerate((b0, b1, b2, b3)):
+        out[(at[1] + 4 - k) % 4] = piece[...]
+
+
+def outer(at, columns, gds, grads):
+    total = dot(columns[0], gds[0].reshape(128, 352), 0, 0)
+    for k in range(1, 4):
+        total = total + dot(columns[k], gds[k].reshape(128, 352), 0, 0)
     total = total.astype(BF)
     for z in range(16):
         grads[z] = total[z * 32 : (z + 1) * 32, :]
@@ -180,10 +184,11 @@
     b1 = shift(b1, "y", 1)
     b2 = shift(b2, "y", 2)
     b3 = shift(b3, "y", 3)
+    (columns,) = call(merge, ((4, *COL),), (), at, b0, b1, b2, b3)
     gds, both = call(backward, ((4, 4, 32, 352), (2, *HID)), (W,) * 3, at, bo, *pieces)
     gds = exchange(gds, "y")
     keep, give = call(rest, ((64, 4096),) * 2, (W, W, W, (128, 4096)), at, fn, both, *pieces)
-    (grads,) = call(outer, ((16, 32, 352),), (), at, b0, b1, b2, b3, gds)
+    (grads,) = call(outer, ((16, 32, 352),), (), at, columns, gds)
     gz = exchange(grads, Z)
     other = shift(give, "c", 1)
     p0, p1, p2, p3 = call(pair, ((16, 4096),) * 4, (), at, keep, other)

time: 196 us -> 196 us (level)
    pallas_call x6 -> x7, Pallas kernels: 12 us -> 12.6 us  [call(): pl.pallas_call(body, out_shape=tuple((jax.ShapeDtypeStruct(o, BF) for o i...]
where the time goes in v2:
time: 196 us; the launch traced here: 195 us
  starting transfers between devices  69.3 us (35%)
  waiting for transfers between devices  47.8 us (24%)
  blocking collectives  47.5 us (24%)
  local copies, waits for them, and re-layouts  13.1 us (7%)
  Pallas kernels  12.6 us (6%)
  other arithmetic  4.05 us (2%)
    ppermute x14, starting transfers between devices, shift(): return lax.ppermute(array, axis, [(k, (k + by) % n) for k in range(n)])  47.7 us
    all_to_all x1, blocking collectives, copies_to_all(): return lax.all_to_all(copies, axis, split_axis=0, concat_axis=0, tiled=True)  34.3 us
    ppermute x14, waiting for transfers between devices, shift(): return lax.ppermute(array, axis, [(k, (k + by) % n) for k in range(n)])  25.1 us
    all_to_all x2, waiting for transfers between devices, exchange(): return lax.all_to_all(array, axis, split_axis=0, concat_axis=0, tiled=True)  22.8 us
    all_gather x1, blocking collectives, shards(): half = lax.all_gather(done, 'x', axis=0, tiled=True)  13.1 us
    pallas_call x7, Pallas kernels, call(): pl.pallas_call(body, out_shape=tuple((jax.ShapeDtypeStruct(o, BF) for o i...  12.6 us
    all_to_all x2, starting transfers between devices, exchange(): return lax.all_to_all(array, axis, split_axis=0, concat_axis=0, tiled=True)  11.9 us
    all_to_all x2, starting transfers between devices, copies_to_all(): return lax.all_to_all(copies, axis, split_axis=0, concat_axis=0, tiled=True)  9.71 us
  transfers between devices with their start and end apart: 18, of which 9 were waited for; matrix products, arithmetic and copies ran while one was open for 2% of the time, Pallas kernels for 2%

profile of v2, /device:TPU:8, one launch (start us, length us, event | category | flops | bytes accessed | tf_op | source)
XLA Modules:
  0.0 195.3 jit_solution(4312245963300574553)
XLA Ops:
  0.6 0.8 pad_maximum_fusion.2
  1.5 34.3 %all_to_all.25 = bf16[4,96,352]{2,1,0:T(8,128)(2,1)} all-to-all(bf16[4,96,352]{2,1,0:T(8,128)(2,1)S(1)} %broadcast_in_dim.9), channel_id=1, replica_groups=mesh['za'=4,'zb'=4,'y'=4,'x'=4,'c'=2] {'za'}, dimensions={0} | all-to-all | bytes 540672 | tf_op jit(solution)/shard_map/all_to_all | solution.py:24
  35.8 2.1 %broadcast_in_dim.10 = bf16[4,4,96,352]{3,2,1,0:T(8,128)(2,1)} broadcast(bf16[4,96,352]{2,1,0:T(8,128)(2,1)} %all_to_all.25), dimensions={1,2,3} | broadcast | bytes 1351680 | tf_op jit(solution)/shard_map/broadcast_in_dim | solution.py:23
  37.9 4.9 %all-to-all-start.1 = ((bf16[4,4,96,352]{3,2,1,0:T(8,128)(2,1)}), bf16[4,4,96,352]{3,2,1,0:T(8,128)(2,1)S(1)}, u32[]{:S(2)}, u32[]{:S(2)}) async-start(bf16[4,4,96,352]{3,2,1,0:T(8,128)(2,1)} %broadcast_in_dim.10), calls=%async_computation.1 | async-start | bytes 2359296 | tf_op jit(solution)/shard_map/all_to_all | solution.py:24
  42.8 1.0 fusion.2
  43.8 5.5 %collective-permute-start.2 = (bf16[2,96,352]{2,1,0:T(8,128)(2,1)S(1)}, bf16[2,96,352]{2,1,0:T(8,128)(2,1)S(1)}, u32[]{:S(2)}, u32[]{:S(2)}) collective-permute-start(bf16[2,96,352]{2,1,0:T(8,128)(2,1)S(1)} %get-tuple-element.35), channel_id=1, source_target_pairs={{0,448},{32,480},{64,0},{96,32},{128,64},{160,96},{192,128},{224,1... | collective-permute-start | bytes 405512 | tf_op jit(solution)/shard_map/ppermute | solution.py:19
  49.3 3.6 %collective-permute-start.3 = (bf16[2,96,352]{2,1,0:T(8,128)(2,1)S(1)}, bf16[2,96,352]{2,1,0:T(8,128)(2,1)S(1)}, u32[]{:S(2)}, u32[]{:S(2)}) collective-permute-start(bf16[2,96,352]{2,1,0:T(8,128)(2,1)S(1)} %get-tuple-element.36), channel_id=1, source_target_pairs={{0,64},{32,96},{64,128},{96,160},{128,192},{160,224},{192,256},{22... | collective-permute-start | bytes 405512 | tf_op jit(solution)/shard_map/ppermute | solution.py:19
  52.9 2.5 %collective-permute-done.2 = bf16[2,96,352]{2,1,0:T(8,128)(2,1)S(1)} collective-permute-done((bf16[2,96,352]{2,1,0:T(8,128)(2,1)S(1)}, bf16[2,96,352]{2,1,0:T(8,128)(2,1)S(1)}, u32[]{:S(2)}, u32[]{:S(2)}) %collective-permute-start.2) | collective-permute-done | bytes 135200 | tf_op jit(solution)/shard_map/ppermute | solution.py:19
  55.5 4.6 %collective-permute-done.3 = bf16[2,96,352]{2,1,0:T(8,128)(2,1)S(1)} collective-permute-done((bf16[2,96,352]{2,1,0:T(8,128)(2,1)S(1)}, bf16[2,96,352]{2,1,0:T(8,128)(2,1)S(1)}, u32[]{:S(2)}, u32[]{:S(2)}) %collective-permute-start.3) | collective-permute-done | bytes 135200 | tf_op jit(solution)/shard_map/ppermute | solution.py:19
  60.0 0.1 pad_maximum_fusion.1
  60.1 0.0 all-to-all-done.1.refs_0_
  60.1 1.2 broadcast_in_dim.11
  61.3 4.8 %all-to-all-start.2 = ((bf16[4,4,96,352]{3,2,1,0:T(8,128)(2,1)}), bf16[4,4,96,352]{3,2,1,0:T(8,128)(2,1)S(1)}, u32[]{:S(2)}, u32[]{:S(2)}) async-start(bf16[4,4,96,352]{3,2,1,0:T(8,128)(2,1)} %broadcast_in_dim.11), calls=%async_computation.2 | async-start | bytes 2359296 | tf_op jit(solution)/shard_map/all_to_all | solution.py:24
  66.1 1.3 fusion
  67.4 1.9 collective-permute-start.4
  69.3 3.9 %collective-permute-start.5 = (bf16[3,4,96,352]{3,2,1,0:T(8,128)(2,1)}, bf16[3,4,96,352]{3,2,1,0:T(8,128)(2,1)}, u32[]{:S(2)}, u32[]{:S(2)}) collective-permute-start(bf16[3,4,96,352]{3,2,1,0:T(8,128)(2,1)} %fusion), channel_id=1, source_target_pairs={{0,32},{32,64},{64,96},{96,128},{128,160},{160,192},{192,224},{224... | collective-permute-start | bytes 2433032 | tf_op jit(solution)/shard_map/ppermute | solution.py:19
  73.2 3.6 %collective-permute-start.1 = (bf16[4,96,352]{2,1,0:T(8,128)(2,1)}, bf16[4,96,352]{2,1,0:T(8,128)(2,1)S(1)}, u32[]{:S(2)}, u32[]{:S(2)}) collective-permute-start(bf16[4,96,352]{2,1,0:T(8,128)(2,1)} %all_to_all.25), channel_id=1, source_target_pairs={{0,32},{32,64},{64,96},{96,128},{128,160},{160,192},{192,224},{224... | collective-permute-start | bytes 811016 | tf_op jit(solution)/shard_map/ppermute | solution.py:19
  76.8 3.5 %collective-permute-start = (bf16[4,96,352]{2,1,0:T(8,128)(2,1)}, bf16[4,96,352]{2,1,0:T(8,128)(2,1)}, u32[]{:S(2)}, u32[]{:S(2)}) collective-permute-start(bf16[4,96,352]{2,1,0:T(8,128)(2,1)} %all_to_all.25), channel_id=1, source_target_pairs={{0,480},{32,0},{64,32},{96,64},{128,96},{160,128},{192,160},{224,1... | collective-permute-start | bytes 811016 | tf_op jit(solution)/shard_map/ppermute | solution.py:19
  80.3 0.1 pad_add_fusion.at
  80.4 1.0 copy-done
  81.4 1.0 copy-done.4
  82.5 1.0 copy-done.5
  83.5 1.4 shard_map.103
  85.0 1.0 copy-done.2
  85.9 0.8 copy-done.6
  86.7 0.6 copy-done.8
  87.4 0.6 copy-done.11
  88.0 0.7 copy-done.13
  88.7 0.7 copy-done.15
  89.3 8.4 %collective-permute-done.1.refs_2_ = bf16[4,96,352]{2,1,0:T(8,128)(2,1)S(1)} collective-permute-done((bf16[4,96,352]{2,1,0:T(8,128)(2,1)}, bf16[4,96,352]{2,1,0:T(8,128)(2,1)S(1)}, u32[]{:S(2)}, u32[]{:S(2)}) %collective-permute-start.1) | collective-permute-done | bytes 270368 | tf_op jit(solution)/shard_map/ppermute | solution.py:19
  97.7 0.0 collective-permute-done.refs_1_
  97.8 1.2 copy-done.3
  99.0 3.5 %shard_map.104 = (bf16[4,4,32,352]{3,2,1,0:T(8,128)(2,1)}, bf16[2,128,352]{2,1,0:T(8,128)(2,1)S(1)}) custom-call(s32[4]{0:T(128)S(1)} %pad_add_fusion.at, bf16[2,128,2048]{2,1,0:T(8,128)(2,1)S(1)} %copy-done.3, bf16[4,4,96,352]{3,2,1,0:T(8,128)(2,1)S(1)} %all-to-all-done.1.refs_0_, bf16[4,96,352]{2,1,0:T(8,128)(2,1)} %collective-permute-done.refs_1_, ...), custom_call_target="tpu_custom_call" | custom-call | tf_op jit(solution)/shard_map/pallas_call | solution.py:144
  102.4 3.8 %shard_map.105 = (bf16[64,4096]{1,0:T(8,128)(2,1)S(1)}, bf16[64,4096]{1,0:T(8,128)(2,1)S(1)}) custom-call(s32[4]{0:T(128)S(1)} %pad_add_fusion.at, bf16[128,2048]{1,0:T(8,128)(2,1)S(1)} %copy-done.7, bf16[2,128,352]{2,1,0:T(8,128)(2,1)S(1)} %get-tuple-element.19.both, bf16[4,4,96,352]{3,2,1,0:T(8,128)(2,1)S(1)} %all-to-all-done.1.refs_0_, ...), custom_call_target="tpu_custom_call" | custom-call | tf_op jit(solution)/shard_map/pallas_call | solution.py:144
  106.3 0.0 copy-start.1
  106.3 2.1 %collective-permute-start.6 = (bf16[64,4096]{1,0:T(8,128)(2,1)S(1)}, bf16[64,4096]{1,0:T(8,128)(2,1)S(1)}, u32[]{:S(2)}, u32[]{:S(2)}) collective-permute-start(bf16[64,4096]{1,0:T(8,128)(2,1)S(1)} %get-tuple-element.21), channel_id=1, source_target_pairs={{0,1},{1,0},{2,3},{3,2},{4,5},{5,4},{6,7},{7,6},{8,9},{9,8},{10,11... | collective-permute-start | bytes 1572872 | tf_op jit(solution)/shard_map/ppermute | solution.py:19
  108.3 1.9 collective-permute-done.6.other
  110.2 0.7 shard_map.106
  110.9 3.4 %collective-permute-start.7 = (bf16[16,4096]{1,0:T(8,128)(2,1)S(1)}, bf16[16,4096]{1,0:T(8,128)(2,1)S(1)}, u32[]{:S(2)}, u32[]{:S(2)}) collective-permute-start(bf16[16,4096]{1,0:T(8,128)(2,1)S(1)} %get-tuple-element.23), channel_id=1, source_target_pairs={{0,2},{2,4},{4,6},{6,0},{1,3},{3,5},{5,7},{7,1},{8,10},{10,12},{12... | collective-permute-start | bytes 393224 | tf_op jit(solution)/shard_map/ppermute | solution.py:19
  114.3 4.6 %collective-permute-start.8 = (bf16[16,4096]{1,0:T(8,128)(2,1)S(1)}, bf16[16,4096]{1,0:T(8,128)(2,1)S(1)}, u32[]{:S(2)}, u32[]{:S(2)}) collective-permute-start(bf16[16,4096]{1,0:T(8,128)(2,1)S(1)} %get-tuple-element.24), channel_id=1, source_target_pairs={{0,4},{2,6},{4,0},{6,2},{1,5},{3,7},{5,1},{7,3},{8,12},{10,14},{12... | collective-permute-start | bytes 393224 | tf_op jit(solution)/shard_map/ppermute | solution.py:19
  119.0 3.3 %collective-permute-start.9 = (bf16[16,4096]{1,0:T(8,128)(2,1)S(1)}, bf16[16,4096]{1,0:T(8,128)(2,1)S(1)}, u32[]{:S(2)}, u32[]{:S(2)}) collective-permute-start(bf16[16,4096]{1,0:T(8,128)(2,1)S(1)} %get-tuple-element.25), channel_id=1, source_target_pairs={{0,6},{2,0},{4,2},{6,4},{1,7},{3,1},{5,3},{7,5},{8,14},{10,8},{12,... | collective-permute-start | bytes 393224 | tf_op jit(solution)/shard_map/ppermute | solution.py:19
  122.3 0.0 collective-permute-done.7.p1
  122.3 1.0 collective-permute-done.8.p2
  123.4 2.5 %collective-permute-done.9.p3 = bf16[16,4096]{1,0:T(8,128)(2,1)S(1)} collective-permute-done((bf16[16,4096]{1,0:T(8,128)(2,1)S(1)}, bf16[16,4096]{1,0:T(8,128)(2,1)S(1)}, u32[]{:S(2)}, u32[]{:S(2)}) %collective-permute-start.9) | collective-permute-done | bytes 131104 | tf_op jit(solution)/shard_map/ppermute | solution.py:19
  125.9 0.7 shard_map.107
  126.6 13.1 %all_gather.3 = bf16[64,4096]{1,0:T(8,128)(2,1)S(1)} all-gather(bf16[16,4096]{1,0:T(8,128)(2,1)S(1)} %shard_map.107), channel_id=1, replica_groups=mesh['za'=4,'zb'=4,'y'=4,'x'=4,'c'=2] {'x'}, dimensions={0}, use_global_device_ids=true | all-gather | bytes 655360 | tf_op jit(solution)/shard_map/all_gather | solution.py:197
  139.7 1.9 collective-permute-start.10
  141.6 4.8 %all-to-all-start.3 = ((bf16[4,4,32,352]{3,2,1,0:T(8,128)(2,1)}), bf16[4,4,32,352]{3,2,1,0:T(8,128)(2,1)S(1)}, u32[]{:S(2)}, u32[]{:S(2)}) async-start(bf16[4,4,32,352]{3,2,1,0:T(8,128)(2,1)} %get-tuple-element.30), calls=%async_computation.3 | async-start | bytes 786432 | tf_op jit(solution)/shard_map/all_to_all | solution.py:162
  146.4 3.4 %collective-permute-start.11 = (bf16[128,512]{1,0:T(8,128)(2,1)S(1)}, bf16[128,512]{1,0:T(8,128)(2,1)S(1)}, u32[]{:S(2)}, u32[]{:S(2)}) collective-permute-start(bf16[128,512]{1,0:T(8,128)(2,1)S(1)} %copy-done.16), channel_id=1, source_target_pairs={{0,8},{8,16},{16,24},{24,0},{1,9},{9,17},{17,25},{25,1},{2,10},{10... | collective-permute-start | bytes 393224 | tf_op jit(solution)/shard_map/ppermute | solution.py:19
  149.8 2.5 %collective-permute-start.12 = (bf16[128,512]{1,0:T(8,128)(2,1)S(1)}, bf16[128,512]{1,0:T(8,128)(2,1)S(1)}, u32[]{:S(2)}, u32[]{:S(2)}) collective-permute-start(bf16[128,512]{1,0:T(8,128)(2,1)S(1)} %copy-done.14), channel_id=1, source_target_pairs={{0,16},{8,24},{16,0},{24,8},{1,17},{9,25},{17,1},{25,9},{2,18},{10... | collective-permute-start | bytes 393224 | tf_op jit(solution)/shard_map/ppermute | solution.py:19
  152.3 4.5 %collective-permute-start.13 = (bf16[128,512]{1,0:T(8,128)(2,1)S(1)}, bf16[128,512]{1,0:T(8,128)(2,1)S(1)}, u32[]{:S(2)}, u32[]{:S(2)}) collective-permute-start(bf16[128,512]{1,0:T(8,128)(2,1)S(1)} %copy-done.12), channel_id=1, source_target_pairs={{0,24},{8,0},{16,8},{24,16},{1,25},{9,1},{17,9},{25,17},{2,26},{10... | collective-permute-start | bytes 393224 | tf_op jit(solution)/shard_map/ppermute | solution.py:19
  156.8 2.2 %collective-permute-done.12.b2 = bf16[128,512]{1,0:T(8,128)(2,1)S(1)} collective-permute-done((bf16[128,512]{1,0:T(8,128)(2,1)S(1)}, bf16[128,512]{1,0:T(8,128)(2,1)S(1)}, u32[]{:S(2)}, u32[]{:S(2)}) %collective-permute-start.12) | collective-permute-done | bytes 131104 | tf_op jit(solution)/shard_map/ppermute | solution.py:19
  159.1 1.9 collective-permute-done.13.b3
  161.0 0.6 shard_map.108.columns
  161.6 0.0 all-to-all-done.3.gds
  161.6 1.9 shard_map.109
  163.5 7.1 %all-to-all-start.4 = ((bf16[16,32,352]{2,1,0:T(8,128)(2,1)}), bf16[16,32,352]{2,1,0:T(8,128)(2,1)S(1)}, u32[]{:S(2)}, u32[]{:S(2)}) async-start(bf16[16,32,352]{2,1,0:T(8,128)(2,1)} %shard_map.109), calls=%async_computation.4 | async-start | bytes 786432 | tf_op jit(solution)/shard_map/all_to_all | solution.py:162
  170.7 0.0 collective-permute-done.10
  170.7 0.1 broadcast_select_fusion
  170.8 0.0 copy-start.17
  170.8 1.0 pad_maximum_fusion
  171.8 22.8 %all-to-all-done.4 = bf16[16,32,352]{2,1,0:T(8,128)(2,1)S(1)} async-done(((bf16[16,32,352]{2,1,0:T(8,128)(2,1)}), bf16[16,32,352]{2,1,0:T(8,128)(2,1)S(1)}, u32[]{:S(2)}, u32[]{:S(2)}) %all-to-all-start.4) | async-done | bytes 360480 | tf_op jit(solution)/shard_map/all_to_all | solution.py:162
  194.6 0.1 convert_reduce_fusion
  194.7 0.6 add.13
  (29 shorter events, 0.1 us)
Async XLA Ops:
  37.9 22.2 %all-to-all-start.1 = ((bf16[4,4,96,352]{3,2,1,0:T(8,128)(2,1)}), bf16[4,4,96,352]{3,2,1,0:T(8,128)(2,1)S(1)}, u32[]{:S(2)}, u32[]{:S(2)}) async-start(bf16[4,4,96,352]{3,2,1,0:T(8,128)(2,1)} %broadcast_in_dim.10), calls=%async_computation.1 | async-start | bytes 2359296 | tf_op jit(solution)/shard_map/all_to_all | solution.py:24
  43.8 11.6 %collective-permute-start.2 = (bf16[2,96,352]{2,1,0:T(8,128)(2,1)S(1)}, bf16[2,96,352]{2,1,0:T(8,128)(2,1)S(1)}, u32[]{:S(2)}, u32[]{:S(2)}) collective-permute-start(bf16[2,96,352]{2,1,0:T(8,128)(2,1)S(1)} %get-tuple-element.35), channel_id=1, source_target_pairs={{0,448},{32,480},{64,0},{96,32},{128,64},{160,96},{192,128},{224,1... | collective-permute-start | bytes 405512 | tf_op jit(solution)/shard_map/ppermute | solution.py:19
  49.3 10.7 %collective-permute-start.3 = (bf16[2,96,352]{2,1,0:T(8,128)(2,1)S(1)}, bf16[2,96,352]{2,1,0:T(8,128)(2,1)S(1)}, u32[]{:S(2)}, u32[]{:S(2)}) collective-permute-start(bf16[2,96,352]{2,1,0:T(8,128)(2,1)S(1)} %get-tuple-element.36), channel_id=1, source_target_pairs={{0,64},{32,96},{64,128},{96,160},{128,192},{160,224},{192,256},{22... | collective-permute-start | bytes 405512 | tf_op jit(solution)/shard_map/ppermute | solution.py:19
  61.3 36.5 %all-to-all-start.2 = ((bf16[4,4,96,352]{3,2,1,0:T(8,128)(2,1)}), bf16[4,4,96,352]{3,2,1,0:T(8,128)(2,1)S(1)}, u32[]{:S(2)}, u32[]{:S(2)}) async-start(bf16[4,4,96,352]{3,2,1,0:T(8,128)(2,1)} %broadcast_in_dim.11), calls=%async_computation.2 | async-start | bytes 2359296 | tf_op jit(solution)/shard_map/all_to_all | solution.py:24
  66.1 14.3 %copy-start.10 = (f32[2048]{0:T(1024)S(1)}, f32[2048]{0:T(1024)}, u32[]{:S(2)}) copy-start(f32[2048]{0:T(1024)} %param.11) | copy-start | bytes 24580
  67.4 30.3 %collective-permute-start.4 = (bf16[3,4,96,352]{3,2,1,0:T(8,128)(2,1)}, bf16[3,4,96,352]{3,2,1,0:T(8,128)(2,1)S(1)}, u32[]{:S(2)}, u32[]{:S(2)}) collective-permute-start(bf16[3,4,96,352]{3,2,1,0:T(8,128)(2,1)} %fusion), channel_id=1, source_target_pairs={{0,480},{32,0},{64,32},{96,64},{128,96},{160,128},{192,160},{224,1... | collective-permute-start | bytes 2433032 | tf_op jit(solution)/shard_map/ppermute | solution.py:19
  69.3 28.4 %collective-permute-start.5 = (bf16[3,4,96,352]{3,2,1,0:T(8,128)(2,1)}, bf16[3,4,96,352]{3,2,1,0:T(8,128)(2,1)}, u32[]{:S(2)}, u32[]{:S(2)}) collective-permute-start(bf16[3,4,96,352]{3,2,1,0:T(8,128)(2,1)} %fusion), channel_id=1, source_target_pairs={{0,32},{32,64},{64,96},{96,128},{128,160},{160,192},{192,224},{224... | collective-permute-start | bytes 2433032 | tf_op jit(solution)/shard_map/ppermute | solution.py:19
  73.2 24.5 %collective-permute-start.1 = (bf16[4,96,352]{2,1,0:T(8,128)(2,1)}, bf16[4,96,352]{2,1,0:T(8,128)(2,1)S(1)}, u32[]{:S(2)}, u32[]{:S(2)}) collective-permute-start(bf16[4,96,352]{2,1,0:T(8,128)(2,1)} %all_to_all.25), channel_id=1, source_target_pairs={{0,32},{32,64},{64,96},{96,128},{128,160},{160,192},{192,224},{224... | collective-permute-start | bytes 811016 | tf_op jit(solution)/shard_map/ppermute | solution.py:19
  76.8 20.9 %collective-permute-start = (bf16[4,96,352]{2,1,0:T(8,128)(2,1)}, bf16[4,96,352]{2,1,0:T(8,128)(2,1)}, u32[]{:S(2)}, u32[]{:S(2)}) collective-permute-start(bf16[4,96,352]{2,1,0:T(8,128)(2,1)} %all_to_all.25), channel_id=1, source_target_pairs={{0,480},{32,0},{64,32},{96,64},{128,96},{160,128},{192,160},{224,1... | collective-permute-start | bytes 811016 | tf_op jit(solution)/shard_map/ppermute | solution.py:19
  80.4 1.0 copy-start
  81.4 1.0 copy-start.4
  82.5 1.0 copy-start.5
  85.0 1.0 copy-start.2
  85.9 0.8 copy-start.6
  86.7 0.6 copy-start.8
  87.4 0.6 copy-start.11
  88.0 0.7 copy-start.13
  88.7 0.7 copy-start.15
  97.7 1.2 copy-start.3
  99.0 3.5 %copy-start.7 = (bf16[128,2048]{1,0:T(8,128)(2,1)S(1)}, bf16[128,2048]{1,0:T(8,128)(2,1)}, u32[]{:S(2)}) copy-start(bf16[128,2048]{1,0:T(8,128)(2,1)} %copy-done.6) | copy-start | bytes 1572868
  106.3 19.6 %copy-start.1 = (bf16[128,2048]{1,0:T(8,128)(2,1)S(1)}, bf16[128,2048]{1,0:T(8,128)(2,1)}, u32[]{:S(2)}) copy-start(bf16[128,2048]{1,0:T(8,128)(2,1)} %bt.3) | copy-start | bytes 1572868
  106.3 3.9 %collective-permute-start.6 = (bf16[64,4096]{1,0:T(8,128)(2,1)S(1)}, bf16[64,4096]{1,0:T(8,128)(2,1)S(1)}, u32[]{:S(2)}, u32[]{:S(2)}) collective-permute-start(bf16[64,4096]{1,0:T(8,128)(2,1)S(1)} %get-tuple-element.21), channel_id=1, source_target_pairs={{0,1},{1,0},{2,3},{3,2},{4,5},{5,4},{6,7},{7,6},{8,9},{9,8},{10,11... | collective-permute-start | bytes 1572872 | tf_op jit(solution)/shard_map/ppermute | solution.py:19
  110.9 11.4 %collective-permute-start.7 = (bf16[16,4096]{1,0:T(8,128)(2,1)S(1)}, bf16[16,4096]{1,0:T(8,128)(2,1)S(1)}, u32[]{:S(2)}, u32[]{:S(2)}) collective-permute-start(bf16[16,4096]{1,0:T(8,128)(2,1)S(1)} %get-tuple-element.23), channel_id=1, source_target_pairs={{0,2},{2,4},{4,6},{6,0},{1,3},{3,5},{5,7},{7,1},{8,10},{10,12},{12... | collective-permute-start | bytes 393224 | tf_op jit(solution)/shard_map/ppermute | solution.py:19
  114.3 9.0 %collective-permute-start.8 = (bf16[16,4096]{1,0:T(8,128)(2,1)S(1)}, bf16[16,4096]{1,0:T(8,128)(2,1)S(1)}, u32[]{:S(2)}, u32[]{:S(2)}) collective-permute-start(bf16[16,4096]{1,0:T(8,128)(2,1)S(1)} %get-tuple-element.24), channel_id=1, source_target_pairs={{0,4},{2,6},{4,0},{6,2},{1,5},{3,7},{5,1},{7,3},{8,12},{10,14},{12... | collective-permute-start | bytes 393224 | tf_op jit(solution)/shard_map/ppermute | solution.py:19
  119.0 6.9 %collective-permute-start.9 = (bf16[16,4096]{1,0:T(8,128)(2,1)S(1)}, bf16[16,4096]{1,0:T(8,128)(2,1)S(1)}, u32[]{:S(2)}, u32[]{:S(2)}) collective-permute-start(bf16[16,4096]{1,0:T(8,128)(2,1)S(1)} %get-tuple-element.25), channel_id=1, source_target_pairs={{0,6},{2,0},{4,2},{6,4},{1,7},{3,1},{5,3},{7,5},{8,14},{10,8},{12,... | collective-permute-start | bytes 393224 | tf_op jit(solution)/shard_map/ppermute | solution.py:19
  125.8 20.5 %copy-start.16 = (bf16[128,512]{1,0:T(8,128)(2,1)S(1)}, bf16[128,512]{1,0:T(8,128)(2,1)}, u32[]{:S(2)}) copy-start(bf16[128,512]{1,0:T(8,128)(2,1)} %copy-done.15) | copy-start | bytes 393220
  125.8 23.9 %copy-start.14 = (bf16[128,512]{1,0:T(8,128)(2,1)S(1)}, bf16[128,512]{1,0:T(8,128)(2,1)}, u32[]{:S(2)}) copy-start(bf16[128,512]{1,0:T(8,128)(2,1)} %copy-done.13) | copy-start | bytes 393220
  125.8 26.4 %copy-start.12 = (bf16[128,512]{1,0:T(8,128)(2,1)S(1)}, bf16[128,512]{1,0:T(8,128)(2,1)}, u32[]{:S(2)}) copy-start(bf16[128,512]{1,0:T(8,128)(2,1)} %copy-done.11) | copy-start | bytes 393220
  125.9 35.2 %copy-start.9 = (bf16[128,512]{1,0:T(8,128)(2,1)S(1)}, bf16[128,512]{1,0:T(8,128)(2,1)}, u32[]{:S(2)}) copy-start(bf16[128,512]{1,0:T(8,128)(2,1)} %copy-done.8) | copy-start | bytes 393220
  139.7 31.0 %collective-permute-start.10 = (bf16[64,4096]{1,0:T(8,128)(2,1)S(1)}, bf16[64,4096]{1,0:T(8,128)(2,1)S(1)}, u32[]{:S(2)}, u32[]{:S(2)}) collective-permute-start(bf16[64,4096]{1,0:T(8,128)(2,1)S(1)} %all_gather.3), channel_id=1, source_target_pairs={{0,1},{1,0},{2,3},{3,2},{4,5},{5,4},{6,7},{7,6},{8,9},{9,8},{10,11... | collective-permute-start | bytes 1572872 | tf_op jit(solution)/shard_map/ppermute | solution.py:19
  141.6 20.0 %all-to-all-start.3 = ((bf16[4,4,32,352]{3,2,1,0:T(8,128)(2,1)}), bf16[4,4,32,352]{3,2,1,0:T(8,128)(2,1)S(1)}, u32[]{:S(2)}, u32[]{:S(2)}) async-start(bf16[4,4,32,352]{3,2,1,0:T(8,128)(2,1)} %get-tuple-element.30), calls=%async_computation.3 | async-start | bytes 786432 | tf_op jit(solution)/shard_map/all_to_all | solution.py:162
  146.4 10.5 %collective-permute-start.11 = (bf16[128,512]{1,0:T(8,128)(2,1)S(1)}, bf16[128,512]{1,0:T(8,128)(2,1)S(1)}, u32[]{:S(2)}, u32[]{:S(2)}) collective-permute-start(bf16[128,512]{1,0:T(8,128)(2,1)S(1)} %copy-done.16), channel_id=1, source_target_pairs={{0,8},{8,16},{16,24},{24,0},{1,9},{9,17},{17,25},{25,1},{2,10},{10... | collective-permute-start | bytes 393224 | tf_op jit(solution)/shard_map/ppermute | solution.py:19
  149.8 9.3 %collective-permute-start.12 = (bf16[128,512]{1,0:T(8,128)(2,1)S(1)}, bf16[128,512]{1,0:T(8,128)(2,1)S(1)}, u32[]{:S(2)}, u32[]{:S(2)}) collective-permute-start(bf16[128,512]{1,0:T(8,128)(2,1)S(1)} %copy-done.14), channel_id=1, source_target_pairs={{0,16},{8,24},{16,0},{24,8},{1,17},{9,25},{17,1},{25,9},{2,18},{10... | collective-permute-start | bytes 393224 | tf_op jit(solution)/shard_map/ppermute | solution.py:19
  152.3 8.7 %collective-permute-start.13 = (bf16[128,512]{1,0:T(8,128)(2,1)S(1)}, bf16[128,512]{1,0:T(8,128)(2,1)S(1)}, u32[]{:S(2)}, u32[]{:S(2)}) collective-permute-start(bf16[128,512]{1,0:T(8,128)(2,1)S(1)} %copy-done.12), channel_id=1, source_target_pairs={{0,24},{8,0},{16,8},{24,16},{1,25},{9,1},{17,9},{25,17},{2,26},{10... | collective-permute-start | bytes 393224 | tf_op jit(solution)/shard_map/ppermute | solution.py:19
  163.5 31.1 %all-to-all-start.4 = ((bf16[16,32,352]{2,1,0:T(8,128)(2,1)}), bf16[16,32,352]{2,1,0:T(8,128)(2,1)S(1)}, u32[]{:S(2)}, u32[]{:S(2)}) async-start(bf16[16,32,352]{2,1,0:T(8,128)(2,1)} %shard_map.109), calls=%async_computation.4 | async-start | bytes 786432 | tf_op jit(solution)/shard_map/all_to_all | solution.py:162
  170.8 23.9 %copy-start.17 = (f32[32,352]{1,0:T(8,128)S(1)}, f32[32,352]{1,0:T(8,128)}, u32[]{:S(2)}) copy-start(f32[32,352]{1,0:T(8,128)} %param.15) | copy-start | bytes 135172

commit v3 on v2

--- a/solution.py
+++ b/solution.py
@@ -54,12 +54,9 @@
             whole[rows, :] = piece[(*spot, slice(m * 32, (m + 1) * 32))]
 
 
-def prepare(at, bt, ft, og, gain, bo, fn, b0, b1, b2, b3, split):
+def columns(at, bt, gain, b0, b1, b2, b3, split):
     y = at[1]
-    fn[...] = normalize(ft[...], gain[...])
     normed = normalize(bt[...], gain[...])
-    bo[0] = normed
-    bo[1] = og[...]
     tiles = [normed[:, z * 128 : (z + 1) * 128].astype(F32) for z in range(16)]
     spot = lax.broadcasted_iota(jnp.int32, (128, 128), 1) // 32
     for yy in range(4):
@@ -75,47 +72,46 @@
         out[...] = split[(y + k) % 4]
 
 
-def backward(at, bo, *refs):
-    pieces, (gds, both, wg, wu, wd) = refs[:6], refs[6:]
+def tokens(at, bt, ft, og, gain, out):
+    out[0] = normalize(bt[...], gain[...])
+    out[1] = og[...]
+    out[2] = normalize(ft[...], gain[...])
+
+
+def products(at, tok, *refs):
+    pieces, (gds, keep, give, wg, wu, wd, parts) = refs[:6], refs[6:]
     assemble(at, pieces, (wg, wu, wd))
-    gate = dot(bo[0], wg[...], 1, 0)
-    up = dot(bo[0], wu[...], 1, 0)
-    hid = 0.5 * dot(bo[1], wd[...], 1, 0)
+    gate = dot(tok[0], wg[...], 1, 0)
+    up = dot(tok[0], wu[...], 1, 0)
+    hid = 0.5 * dot(tok[1], wd[...], 1, 0)
     s = jax.nn.sigmoid(gate)
     gd = (hid * up * s * (1.0 + gate * (1.0 - s))).astype(BF)
+    ud = (hid * gate * s).astype(BF)
     for k in range(4):
         for j in range(4):
             gds[k, j] = gd[j * 32 : (j + 1) * 32, :]
-    both[0] = gd
-    both[1] = (hid * gate * s).astype(BF)
-
-
-def merge(at, b0, b1, b2, b3, out):
-    for k, piece in enumerate((b0, b1, b2, b3)):
-        out[(at[1] + 4 - k) % 4] = piece[...]
-
-
-def outer(at, columns, gds, grads):
-    total = dot(columns[0], gds[0].reshape(128, 352), 0, 0)
-    for k in range(1, 4):
-        total = total + dot(columns[k], gds[k].reshape(128, 352), 0, 0)
-    total = total.astype(BF)
-    for z in range(16):
-        grads[z] = total[z * 32 : (z + 1) * 32, :]
-
-
-def rest(at, fn, both, *refs):
-    pieces, (keep, give, wg, wu, wd, parts) = refs[:6], refs[6:]
-    assemble(at, pieces, (wg, wu, wd))
-    diff = dot(both[0], wg[...], 1, 1) + dot(both[1], wu[...], 1, 1)
-    parts[:, 2048:4096] = diff.astype(BF)
-    gate = dot(fn[...], wg[...], 1, 0)
-    up = dot(fn[...], wu[...], 1, 0)
+    parts[:, 2048:4096] = (dot(gd, wg[...], 1, 1) + dot(ud, wu[...], 1, 1)).astype(BF)
+    gate = dot(tok[2], wg[...], 1, 0)
+    up = dot(tok[2], wu[...], 1, 0)
     hidden = (gate * jax.nn.sigmoid(gate) * up).astype(BF)
     parts[:, 0:2048] = dot(hidden, wd[...], 1, 1).astype(BF)
     c = at[2]
     keep[...] = parts[pl.ds(pl.multiple_of(c * 64, 64), 64), :]
     give[...] = parts[pl.ds(pl.multiple_of((1 - c) * 64, 64), 64), :]
+
+
+def merge(at, b0, b1, b2, b3, out):
+    for k, piece in enumerate((b0, b1, b2, b3)):
+        out[(at[1] + 4 - k) % 4] = piece[...]
+
+
+def outer(at, cols, gds, grads):
+    total = dot(cols[0], gds[0].reshape(128, 352), 0, 0)
+    for k in range(1, 4):
+        total = total + dot(cols[k], gds[k].reshape(128, 352), 0, 0)
+    total = total.astype(BF)
+    for z in range(16):
+        grads[z] = total[z * 32 : (z + 1) * 32, :]
 
 
 def pair(at, keep, other, *outs):
@@ -154,7 +150,6 @@
 LIMIT = 24 * 1024 * 1024
 W = (2048, 352)
 TOK = (128, 2048)
-HID = (128, 352)
 COL = (128, 512)
 
 
@@ -178,17 +173,20 @@
     z3 = shift(others, Z, 1)
     far = copies_to_all(a2, "y")
     pieces = (near, a1, a3, far, z1, z3)
-    bo, fn, b0, b1, b2, b3 = call(
-        prepare, ((2, *TOK), TOK) + (COL,) * 4, ((4, *COL),), at, bt, ft, og, gain
-    )
+    b0, b1, b2, b3 = call(columns, (COL,) * 4, ((4, *COL),), at, bt, gain)
+    (tok,) = call(tokens, ((3, *TOK),), (), at, bt, ft, og, gain)
     b1 = shift(b1, "y", 1)
     b2 = shift(b2, "y", 2)
     b3 = shift(b3, "y", 3)
-    (columns,) = call(merge, ((4, *COL),), (), at, b0, b1, b2, b3)
-    gds, both = call(backward, ((4, 4, 32, 352), (2, *HID)), (W,) * 3, at, bo, *pieces)
+    (cols,) = call(merge, ((4, *COL),), (), at, b0, b1, b2, b3)
+    gds, keep, give = call(
+        products,
+        ((4, 4, 32, 352), (64, 4096), (64, 4096)),
+        (W, W, W, (128, 4096)),
+        at, tok, *pieces,
+    )
     gds = exchange(gds, "y")
-    keep, give = call(rest, ((64, 4096),) * 2, (W, W, W, (128, 4096)), at, fn, both, *pieces)
-    (grads,) = call(outer, ((16, 32, 352),), (), at, columns, gds)
+    (grads,) = call(outer, ((16, 32, 352),), (), at, cols, gds)
     gz = exchange(grads, Z)
     other = shift(give, "c", 1)
     p0, p1, p2, p3 = call(pair, ((16, 4096),) * 4, (), at, keep, other)

time: 196 us -> 195 us (level)
  waiting for transfers between devices: 47.8 us -> 55.4 us
  local copies, waits for them, and re-layouts: 13.1 us -> 6.39 us
    ppermute x14, waiting for transfers between devices: 25.1 us -> 32.6 us  [shift(): return lax.ppermute(array, axis, [(k, (k + by) % n) for k in range(n)])]
    unnamed x36 -> x12, local copies, waits for them, and re-layouts: 8.75 us -> 2.1 us
  transfers between devices with their start and end apart: 18 -> 18, of which waited for: 9 -> 10; matrix products, arithmetic and copies ran while one was open for 2% -> 2% of each run, Pallas kernels for 2% -> 2%
where the time goes in v3:
time: 195 us; the launch traced here: 194 us
  starting transfers between devices  68 us (35%)
  waiting for transfers between devices  55.4 us (28%)
  blocking collectives  47.4 us (24%)
  Pallas kernels  11.5 us (6%)
  local copies, waits for them, and re-layouts  6.39 us (3%)
  other arithmetic  4.06 us (2%)
    ppermute x14, starting transfers between devices, shift(): return lax.ppermute(array, axis, [(k, (k + by) % n) for k in range(n)])  46.8 us
    all_to_all x1, blocking collectives, copies_to_all(): return lax.all_to_all(copies, axis, split_axis=0, concat_axis=0, tiled=True)  34.3 us
    ppermute x14, waiting for transfers between devices, shift(): return lax.ppermute(array, axis, [(k, (k + by) % n) for k in range(n)])  32.6 us
    all_to_all x2, waiting for transfers between devices, exchange(): return lax.all_to_all(array, axis, split_axis=0, concat_axis=0, tiled=True)  22.8 us
    all_gather x1, blocking collectives, shards(): half = lax.all_gather(done, 'x', axis=0, tiled=True)  13.1 us
    pallas_call x7, Pallas kernels, call(): pl.pallas_call(body, out_shape=tuple((jax.ShapeDtypeStruct(o, BF) for o i...  11.5 us
    all_to_all x2, starting transfers between devices, exchange(): return lax.all_to_all(array, axis, split_axis=0, concat_axis=0, tiled=True)  11.5 us
    all_to_all x2, starting transfers between devices, copies_to_all(): return lax.all_to_all(copies, axis, split_axis=0, concat_axis=0, tiled=True)  9.71 us
  transfers between devices with their start and end apart: 18, of which 10 were waited for; matrix products, arithmetic and copies ran while one was open for 2% of the time, Pallas kernels for 2%

profile of v3, /device:TPU:8, one launch (start us, length us, event | category | flops | bytes accessed | tf_op | source)
XLA Modules:
  0.0 193.7 jit_solution(9503898439951494146)
XLA Ops:
  0.6 0.8 pad_maximum_fusion.2
  1.5 34.3 %all_to_all.25 = bf16[4,96,352]{2,1,0:T(8,128)(2,1)} all-to-all(bf16[4,96,352]{2,1,0:T(8,128)(2,1)S(1)} %broadcast_in_dim.9), channel_id=1, replica_groups=mesh['za'=4,'zb'=4,'y'=4,'x'=4,'c'=2] {'za'}, dimensions={0} | all-to-all | bytes 540672 | tf_op jit(solution)/shard_map/all_to_all | solution.py:24
  35.8 2.1 %broadcast_in_dim.10 = bf16[4,4,96,352]{3,2,1,0:T(8,128)(2,1)} broadcast(bf16[4,96,352]{2,1,0:T(8,128)(2,1)} %all_to_all.25), dimensions={1,2,3} | broadcast | bytes 1351680 | tf_op jit(solution)/shard_map/broadcast_in_dim | solution.py:23
  37.9 4.9 %all-to-all-start.1 = ((bf16[4,4,96,352]{3,2,1,0:T(8,128)(2,1)}), bf16[4,4,96,352]{3,2,1,0:T(8,128)(2,1)S(1)}, u32[]{:S(2)}, u32[]{:S(2)}) async-start(bf16[4,4,96,352]{3,2,1,0:T(8,128)(2,1)} %broadcast_in_dim.10), calls=%async_computation.1 | async-start | bytes 2359296 | tf_op jit(solution)/shard_map/all_to_all | solution.py:24
  42.8 1.0 fusion.2
  43.8 5.5 %collective-permute-start.2 = (bf16[2,96,352]{2,1,0:T(8,128)(2,1)S(1)}, bf16[2,96,352]{2,1,0:T(8,128)(2,1)S(1)}, u32[]{:S(2)}, u32[]{:S(2)}) collective-permute-start(bf16[2,96,352]{2,1,0:T(8,128)(2,1)S(1)} %get-tuple-element.29), channel_id=1, source_target_pairs={{0,448},{32,480},{64,0},{96,32},{128,64},{160,96},{192,128},{224,1... | collective-permute-start | bytes 405512 | tf_op jit(solution)/shard_map/ppermute | solution.py:19
  49.3 3.6 %collective-permute-start.3 = (bf16[2,96,352]{2,1,0:T(8,128)(2,1)S(1)}, bf16[2,96,352]{2,1,0:T(8,128)(2,1)S(1)}, u32[]{:S(2)}, u32[]{:S(2)}) collective-permute-start(bf16[2,96,352]{2,1,0:T(8,128)(2,1)S(1)} %get-tuple-element.30), channel_id=1, source_target_pairs={{0,64},{32,96},{64,128},{96,160},{128,192},{160,224},{192,256},{22... | collective-permute-start | bytes 405512 | tf_op jit(solution)/shard_map/ppermute | solution.py:19
  52.9 2.5 %collective-permute-done.2 = bf16[2,96,352]{2,1,0:T(8,128)(2,1)S(1)} collective-permute-done((bf16[2,96,352]{2,1,0:T(8,128)(2,1)S(1)}, bf16[2,96,352]{2,1,0:T(8,128)(2,1)S(1)}, u32[]{:S(2)}, u32[]{:S(2)}) %collective-permute-start.2) | collective-permute-done | bytes 135200 | tf_op jit(solution)/shard_map/ppermute | solution.py:19
  55.4 4.6 %collective-permute-done.3 = bf16[2,96,352]{2,1,0:T(8,128)(2,1)S(1)} collective-permute-done((bf16[2,96,352]{2,1,0:T(8,128)(2,1)S(1)}, bf16[2,96,352]{2,1,0:T(8,128)(2,1)S(1)}, u32[]{:S(2)}, u32[]{:S(2)}) %collective-permute-start.3) | collective-permute-done | bytes 135200 | tf_op jit(solution)/shard_map/ppermute | solution.py:19
  60.0 0.1 pad_maximum_fusion.1
  60.1 0.0 all-to-all-done.1.refs_0_
  60.1 1.1 broadcast_in_dim.11
  61.2 4.8 %all-to-all-start.2 = ((bf16[4,4,96,352]{3,2,1,0:T(8,128)(2,1)}), bf16[4,4,96,352]{3,2,1,0:T(8,128)(2,1)}, u32[]{:S(2)}, u32[]{:S(2)}) async-start(bf16[4,4,96,352]{3,2,1,0:T(8,128)(2,1)} %broadcast_in_dim.11), calls=%async_computation.2 | async-start | bytes 2359296 | tf_op jit(solution)/shard_map/all_to_all | solution.py:24
  66.0 1.3 fusion
  67.4 1.9 collective-permute-start.4
  69.3 4.3 %collective-permute-start.5 = (bf16[3,4,96,352]{3,2,1,0:T(8,128)(2,1)}, bf16[3,4,96,352]{3,2,1,0:T(8,128)(2,1)}, u32[]{:S(2)}, u32[]{:S(2)}) collective-permute-start(bf16[3,4,96,352]{3,2,1,0:T(8,128)(2,1)} %fusion), channel_id=1, source_target_pairs={{0,32},{32,64},{64,96},{96,128},{128,160},{160,192},{192,224},{224... | collective-permute-start | bytes 2433032 | tf_op jit(solution)/shard_map/ppermute | solution.py:19
  73.6 2.8 %collective-permute-start = (bf16[4,96,352]{2,1,0:T(8,128)(2,1)}, bf16[4,96,352]{2,1,0:T(8,128)(2,1)}, u32[]{:S(2)}, u32[]{:S(2)}) collective-permute-start(bf16[4,96,352]{2,1,0:T(8,128)(2,1)} %all_to_all.25), channel_id=1, source_target_pairs={{0,480},{32,0},{64,32},{96,64},{128,96},{160,128},{192,160},{224,1... | collective-permute-start | bytes 811016 | tf_op jit(solution)/shard_map/ppermute | solution.py:19
  76.4 3.1 %collective-permute-start.1 = (bf16[4,96,352]{2,1,0:T(8,128)(2,1)}, bf16[4,96,352]{2,1,0:T(8,128)(2,1)}, u32[]{:S(2)}, u32[]{:S(2)}) collective-permute-start(bf16[4,96,352]{2,1,0:T(8,128)(2,1)} %all_to_all.25), channel_id=1, source_target_pairs={{0,32},{32,64},{64,96},{96,128},{128,160},{160,192},{192,224},{224... | collective-permute-start | bytes 811016 | tf_op jit(solution)/shard_map/ppermute | solution.py:19
  79.5 0.1 pad_add_fusion.at
  79.5 0.0 copy-done
  79.5 0.0 copy-done.4
  79.5 1.0 copy-done.1
  80.6 1.0 copy-done.2
  81.6 1.0 shard_map.103.tok
  82.6 12.9 %collective-permute-done.refs_1_ = bf16[4,96,352]{2,1,0:T(8,128)(2,1)} collective-permute-done((bf16[4,96,352]{2,1,0:T(8,128)(2,1)}, bf16[4,96,352]{2,1,0:T(8,128)(2,1)}, u32[]{:S(2)}, u32[]{:S(2)}) %collective-permute-start) | collective-permute-done | bytes 270368 | tf_op jit(solution)/shard_map/ppermute | solution.py:19
  95.5 3.1 %collective-permute-done.1.refs_2_ = bf16[4,96,352]{2,1,0:T(8,128)(2,1)} collective-permute-done((bf16[4,96,352]{2,1,0:T(8,128)(2,1)}, bf16[4,96,352]{2,1,0:T(8,128)(2,1)}, u32[]{:S(2)}, u32[]{:S(2)}) %collective-permute-start.1) | collective-permute-done | bytes 270368 | tf_op jit(solution)/shard_map/ppermute | solution.py:19
  98.5 0.0 all-to-all-done.2.refs_3_
  98.5 0.0 collective-permute-done.4.refs_4_
  98.5 0.0 collective-permute-done.5.refs_5_
  98.5 5.5 %shard_map.104 = (bf16[4,4,32,352]{3,2,1,0:T(8,128)(2,1)S(1)}, bf16[64,4096]{1,0:T(8,128)(2,1)S(1)}, bf16[64,4096]{1,0:T(8,128)(2,1)S(1)}) custom-call(s32[4]{0:T(128)S(1)} %pad_add_fusion.at, bf16[3,128,2048]{2,1,0:T(8,128)(2,1)S(1)} %shard_map.103.tok, bf16[4,4,96,352]{3,2,1,0:T(8,128)(2,1)S(1)} %all-to-all-done.1.refs_0_, ...), custom_call_target="tpu_custom_call" | custom-call | tf_op jit(solution)/shard_map/pallas_call | solution.py:140
  104.0 0.0 copy-start.3
  104.0 1.9 collective-permute-start.6
  106.0 1.9 collective-permute-done.6.other
  107.9 0.7 shard_map.105
  108.5 3.4 %collective-permute-start.7 = (bf16[16,4096]{1,0:T(8,128)(2,1)S(1)}, bf16[16,4096]{1,0:T(8,128)(2,1)S(1)}, u32[]{:S(2)}, u32[]{:S(2)}) collective-permute-start(bf16[16,4096]{1,0:T(8,128)(2,1)S(1)} %get-tuple-element.17), channel_id=1, source_target_pairs={{0,2},{2,4},{4,6},{6,0},{1,3},{3,5},{5,7},{7,1},{8,10},{10,12},{12... | collective-permute-start | bytes 393224 | tf_op jit(solution)/shard_map/ppermute | solution.py:19
  111.9 4.6 %collective-permute-start.8 = (bf16[16,4096]{1,0:T(8,128)(2,1)S(1)}, bf16[16,4096]{1,0:T(8,128)(2,1)S(1)}, u32[]{:S(2)}, u32[]{:S(2)}) collective-permute-start(bf16[16,4096]{1,0:T(8,128)(2,1)S(1)} %get-tuple-element.18), channel_id=1, source_target_pairs={{0,4},{2,6},{4,0},{6,2},{1,5},{3,7},{5,1},{7,3},{8,12},{10,14},{12... | collective-permute-start | bytes 393224 | tf_op jit(solution)/shard_map/ppermute | solution.py:19
  116.6 3.3 %collective-permute-start.9 = (bf16[16,4096]{1,0:T(8,128)(2,1)S(1)}, bf16[16,4096]{1,0:T(8,128)(2,1)S(1)}, u32[]{:S(2)}, u32[]{:S(2)}) collective-permute-start(bf16[16,4096]{1,0:T(8,128)(2,1)S(1)} %get-tuple-element.19), channel_id=1, source_target_pairs={{0,6},{2,0},{4,2},{6,4},{1,7},{3,1},{5,3},{7,5},{8,14},{10,8},{12,... | collective-permute-start | bytes 393224 | tf_op jit(solution)/shard_map/ppermute | solution.py:19
  119.9 0.0 collective-permute-done.7.p1
  119.9 1.0 collective-permute-done.8.p2
  121.0 2.5 %collective-permute-done.9.p3 = bf16[16,4096]{1,0:T(8,128)(2,1)S(1)} collective-permute-done((bf16[16,4096]{1,0:T(8,128)(2,1)S(1)}, bf16[16,4096]{1,0:T(8,128)(2,1)S(1)}, u32[]{:S(2)}, u32[]{:S(2)}) %collective-permute-start.9) | collective-permute-done | bytes 131104 | tf_op jit(solution)/shard_map/ppermute | solution.py:19
  123.5 0.7 shard_map.106
  124.1 13.1 %all_gather.3 = bf16[64,4096]{1,0:T(8,128)(2,1)S(1)} all-gather(bf16[16,4096]{1,0:T(8,128)(2,1)S(1)} %shard_map.106), channel_id=1, replica_groups=mesh['za'=4,'zb'=4,'y'=4,'x'=4,'c'=2] {'x'}, dimensions={0}, use_global_device_ids=true | all-gather | bytes 655360 | tf_op jit(solution)/shard_map/all_gather | solution.py:195
  137.3 0.0 copy-done.3
  137.3 1.9 collective-permute-start.10
  139.2 4.8 %all-to-all-start.3 = ((bf16[4,4,32,352]{3,2,1,0:T(8,128)(2,1)}), bf16[4,4,32,352]{3,2,1,0:T(8,128)(2,1)S(1)}, u32[]{:S(2)}, u32[]{:S(2)}) async-start(bf16[4,4,32,352]{3,2,1,0:T(8,128)(2,1)} %copy-done.3), calls=%async_computation.3 | async-start | bytes 786432 | tf_op jit(solution)/shard_map/all_to_all | solution.py:157
  144.0 1.2 shard_map.107
  145.2 3.4 %collective-permute-start.11 = (bf16[128,512]{1,0:T(8,128)(2,1)S(1)}, bf16[128,512]{1,0:T(8,128)(2,1)S(1)}, u32[]{:S(2)}, u32[]{:S(2)}) collective-permute-start(bf16[128,512]{1,0:T(8,128)(2,1)S(1)} %get-tuple-element.21), channel_id=1, source_target_pairs={{0,8},{8,16},{16,24},{24,0},{1,9},{9,17},{17,25},{25,1},{2,10},{10... | collective-permute-start | bytes 393224 | tf_op jit(solution)/shard_map/ppermute | solution.py:19
  148.6 2.5 %collective-permute-start.12 = (bf16[128,512]{1,0:T(8,128)(2,1)S(1)}, bf16[128,512]{1,0:T(8,128)(2,1)S(1)}, u32[]{:S(2)}, u32[]{:S(2)}) collective-permute-start(bf16[128,512]{1,0:T(8,128)(2,1)S(1)} %get-tuple-element.22), channel_id=1, source_target_pairs={{0,16},{8,24},{16,0},{24,8},{1,17},{9,25},{17,1},{25,9},{2,18},{10... | collective-permute-start | bytes 393224 | tf_op jit(solution)/shard_map/ppermute | solution.py:19
  151.2 4.5 %collective-permute-start.13 = (bf16[128,512]{1,0:T(8,128)(2,1)S(1)}, bf16[128,512]{1,0:T(8,128)(2,1)S(1)}, u32[]{:S(2)}, u32[]{:S(2)}) collective-permute-start(bf16[128,512]{1,0:T(8,128)(2,1)S(1)} %get-tuple-element.23), channel_id=1, source_target_pairs={{0,24},{8,0},{16,8},{24,16},{1,25},{9,1},{17,9},{25,17},{2,26},{10... | collective-permute-start | bytes 393224 | tf_op jit(solution)/shard_map/ppermute | solution.py:19
  155.7 0.0 collective-permute-done.11.b1
  155.7 2.3 %collective-permute-done.12.b2 = bf16[128,512]{1,0:T(8,128)(2,1)S(1)} collective-permute-done((bf16[128,512]{1,0:T(8,128)(2,1)S(1)}, bf16[128,512]{1,0:T(8,128)(2,1)S(1)}, u32[]{:S(2)}, u32[]{:S(2)}) %collective-permute-start.12) | collective-permute-done | bytes 131104 | tf_op jit(solution)/shard_map/ppermute | solution.py:19
  158.0 1.9 collective-permute-done.13.b3
  159.9 0.6 shard_map.108.cols
  160.5 0.0 all-to-all-done.3.gds
  160.5 1.9 shard_map.109
  162.4 6.7 %all-to-all-start.4 = ((bf16[16,32,352]{2,1,0:T(8,128)(2,1)}), bf16[16,32,352]{2,1,0:T(8,128)(2,1)S(1)}, u32[]{:S(2)}, u32[]{:S(2)}) async-start(bf16[16,32,352]{2,1,0:T(8,128)(2,1)} %shard_map.109), calls=%async_computation.4 | async-start | bytes 786432 | tf_op jit(solution)/shard_map/all_to_all | solution.py:157
  169.1 0.0 collective-permute-done.10
  169.1 0.1 broadcast_select_fusion
  169.2 0.0 copy-start.5
  169.2 1.0 pad_maximum_fusion
  170.2 22.8 %all-to-all-done.4 = bf16[16,32,352]{2,1,0:T(8,128)(2,1)S(1)} async-done(((bf16[16,32,352]{2,1,0:T(8,128)(2,1)}), bf16[16,32,352]{2,1,0:T(8,128)(2,1)S(1)}, u32[]{:S(2)}, u32[]{:S(2)}) %all-to-all-start.4) | async-done | bytes 360480 | tf_op jit(solution)/shard_map/all_to_all | solution.py:157
  193.0 0.1 convert_reduce_fusion
  193.1 0.0 copy-done.5
  193.1 0.6 add.13
  (5 shorter events, 0.0 us)
Async XLA Ops:
  37.9 22.2 %all-to-all-start.1 = ((bf16[4,4,96,352]{3,2,1,0:T(8,128)(2,1)}), bf16[4,4,96,352]{3,2,1,0:T(8,128)(2,1)S(1)}, u32[]{:S(2)}, u32[]{:S(2)}) async-start(bf16[4,4,96,352]{3,2,1,0:T(8,128)(2,1)} %broadcast_in_dim.10), calls=%async_computation.1 | async-start | bytes 2359296 | tf_op jit(solution)/shard_map/all_to_all | solution.py:24
  43.8 11.6 %collective-permute-start.2 = (bf16[2,96,352]{2,1,0:T(8,128)(2,1)S(1)}, bf16[2,96,352]{2,1,0:T(8,128)(2,1)S(1)}, u32[]{:S(2)}, u32[]{:S(2)}) collective-permute-start(bf16[2,96,352]{2,1,0:T(8,128)(2,1)S(1)} %get-tuple-element.29), channel_id=1, source_target_pairs={{0,448},{32,480},{64,0},{96,32},{128,64},{160,96},{192,128},{224,1... | collective-permute-start | bytes 405512 | tf_op jit(solution)/shard_map/ppermute | solution.py:19
  49.3 10.7 %collective-permute-start.3 = (bf16[2,96,352]{2,1,0:T(8,128)(2,1)S(1)}, bf16[2,96,352]{2,1,0:T(8,128)(2,1)S(1)}, u32[]{:S(2)}, u32[]{:S(2)}) collective-permute-start(bf16[2,96,352]{2,1,0:T(8,128)(2,1)S(1)} %get-tuple-element.30), channel_id=1, source_target_pairs={{0,64},{32,96},{64,128},{96,160},{128,192},{160,224},{192,256},{22... | collective-permute-start | bytes 405512 | tf_op jit(solution)/shard_map/ppermute | solution.py:19
  61.2 37.3 %all-to-all-start.2 = ((bf16[4,4,96,352]{3,2,1,0:T(8,128)(2,1)}), bf16[4,4,96,352]{3,2,1,0:T(8,128)(2,1)}, u32[]{:S(2)}, u32[]{:S(2)}) async-start(bf16[4,4,96,352]{3,2,1,0:T(8,128)(2,1)} %broadcast_in_dim.11), calls=%async_computation.2 | async-start | bytes 2359296 | tf_op jit(solution)/shard_map/all_to_all | solution.py:24
  66.0 13.5 %copy-start = (bf16[128,2048]{1,0:T(8,128)(2,1)S(1)}, bf16[128,2048]{1,0:T(8,128)(2,1)}, u32[]{:S(2)}) copy-start(bf16[128,2048]{1,0:T(8,128)(2,1)} %bt.5) | copy-start | bytes 1572868
  66.0 13.5 %copy-start.4 = (f32[2048]{0:T(1024)S(1)}, f32[2048]{0:T(1024)}, u32[]{:S(2)}) copy-start(f32[2048]{0:T(1024)} %param.11) | copy-start | bytes 24580
  67.4 31.2 %collective-permute-start.4 = (bf16[3,4,96,352]{3,2,1,0:T(8,128)(2,1)}, bf16[3,4,96,352]{3,2,1,0:T(8,128)(2,1)}, u32[]{:S(2)}, u32[]{:S(2)}) collective-permute-start(bf16[3,4,96,352]{3,2,1,0:T(8,128)(2,1)} %fusion), channel_id=1, source_target_pairs={{0,480},{32,0},{64,32},{96,64},{128,96},{160,128},{192,160},{224,1... | collective-permute-start | bytes 2433032 | tf_op jit(solution)/shard_map/ppermute | solution.py:19
  69.3 29.3 %collective-permute-start.5 = (bf16[3,4,96,352]{3,2,1,0:T(8,128)(2,1)}, bf16[3,4,96,352]{3,2,1,0:T(8,128)(2,1)}, u32[]{:S(2)}, u32[]{:S(2)}) collective-permute-start(bf16[3,4,96,352]{3,2,1,0:T(8,128)(2,1)} %fusion), channel_id=1, source_target_pairs={{0,32},{32,64},{64,96},{96,128},{128,160},{160,192},{192,224},{224... | collective-permute-start | bytes 2433032 | tf_op jit(solution)/shard_map/ppermute | solution.py:19
  73.6 21.9 %collective-permute-start = (bf16[4,96,352]{2,1,0:T(8,128)(2,1)}, bf16[4,96,352]{2,1,0:T(8,128)(2,1)}, u32[]{:S(2)}, u32[]{:S(2)}) collective-permute-start(bf16[4,96,352]{2,1,0:T(8,128)(2,1)} %all_to_all.25), channel_id=1, source_target_pairs={{0,480},{32,0},{64,32},{96,64},{128,96},{160,128},{192,160},{224,1... | collective-permute-start | bytes 811016 | tf_op jit(solution)/shard_map/ppermute | solution.py:19
  76.4 22.2 %collective-permute-start.1 = (bf16[4,96,352]{2,1,0:T(8,128)(2,1)}, bf16[4,96,352]{2,1,0:T(8,128)(2,1)}, u32[]{:S(2)}, u32[]{:S(2)}) collective-permute-start(bf16[4,96,352]{2,1,0:T(8,128)(2,1)} %all_to_all.25), channel_id=1, source_target_pairs={{0,32},{32,64},{64,96},{96,128},{128,160},{160,192},{192,224},{224... | collective-permute-start | bytes 811016 | tf_op jit(solution)/shard_map/ppermute | solution.py:19
  79.5 1.0 copy-start.1
  80.6 1.0 copy-start.2
  104.0 33.2 %copy-start.3 = (bf16[4,4,32,352]{3,2,1,0:T(8,128)(2,1)}, bf16[4,4,32,352]{3,2,1,0:T(8,128)(2,1)S(1)}, u32[]{:S(2)}) copy-start(bf16[4,4,32,352]{3,2,1,0:T(8,128)(2,1)S(1)} %get-tuple-element.24) | copy-start | bytes 1081348
  104.0 3.8 %collective-permute-start.6 = (bf16[64,4096]{1,0:T(8,128)(2,1)S(1)}, bf16[64,4096]{1,0:T(8,128)(2,1)S(1)}, u32[]{:S(2)}, u32[]{:S(2)}) collective-permute-start(bf16[64,4096]{1,0:T(8,128)(2,1)S(1)} %get-tuple-element.15), channel_id=1, source_target_pairs={{0,1},{1,0},{2,3},{3,2},{4,5},{5,4},{6,7},{7,6},{8,9},{9,8},{10,11... | collective-permute-start | bytes 1572872 | tf_op jit(solution)/shard_map/ppermute | solution.py:19
  108.5 11.4 %collective-permute-start.7 = (bf16[16,4096]{1,0:T(8,128)(2,1)S(1)}, bf16[16,4096]{1,0:T(8,128)(2,1)S(1)}, u32[]{:S(2)}, u32[]{:S(2)}) collective-permute-start(bf16[16,4096]{1,0:T(8,128)(2,1)S(1)} %get-tuple-element.17), channel_id=1, source_target_pairs={{0,2},{2,4},{4,6},{6,0},{1,3},{3,5},{5,7},{7,1},{8,10},{10,12},{12... | collective-permute-start | bytes 393224 | tf_op jit(solution)/shard_map/ppermute | solution.py:19
  111.9 9.0 %collective-permute-start.8 = (bf16[16,4096]{1,0:T(8,128)(2,1)S(1)}, bf16[16,4096]{1,0:T(8,128)(2,1)S(1)}, u32[]{:S(2)}, u32[]{:S(2)}) collective-permute-start(bf16[16,4096]{1,0:T(8,128)(2,1)S(1)} %get-tuple-element.18), channel_id=1, source_target_pairs={{0,4},{2,6},{4,0},{6,2},{1,5},{3,7},{5,1},{7,3},{8,12},{10,14},{12... | collective-permute-start | bytes 393224 | tf_op jit(solution)/shard_map/ppermute | solution.py:19
  116.6 6.9 %collective-permute-start.9 = (bf16[16,4096]{1,0:T(8,128)(2,1)S(1)}, bf16[16,4096]{1,0:T(8,128)(2,1)S(1)}, u32[]{:S(2)}, u32[]{:S(2)}) collective-permute-start(bf16[16,4096]{1,0:T(8,128)(2,1)S(1)} %get-tuple-element.19), channel_id=1, source_target_pairs={{0,6},{2,0},{4,2},{6,4},{1,7},{3,1},{5,3},{7,5},{8,14},{10,8},{12,... | collective-permute-start | bytes 393224 | tf_op jit(solution)/shard_map/ppermute | solution.py:19
  137.3 31.8 %collective-permute-start.10 = (bf16[64,4096]{1,0:T(8,128)(2,1)S(1)}, bf16[64,4096]{1,0:T(8,128)(2,1)S(1)}, u32[]{:S(2)}, u32[]{:S(2)}) collective-permute-start(bf16[64,4096]{1,0:T(8,128)(2,1)S(1)} %all_gather.3), channel_id=1, source_target_pairs={{0,1},{1,0},{2,3},{3,2},{4,5},{5,4},{6,7},{7,6},{8,9},{9,8},{10,11... | collective-permute-start | bytes 1572872 | tf_op jit(solution)/shard_map/ppermute | solution.py:19
  139.2 21.3 %all-to-all-start.3 = ((bf16[4,4,32,352]{3,2,1,0:T(8,128)(2,1)}), bf16[4,4,32,352]{3,2,1,0:T(8,128)(2,1)S(1)}, u32[]{:S(2)}, u32[]{:S(2)}) async-start(bf16[4,4,32,352]{3,2,1,0:T(8,128)(2,1)} %copy-done.3), calls=%async_computation.3 | async-start | bytes 786432 | tf_op jit(solution)/shard_map/all_to_all | solution.py:157
  145.2 10.5 %collective-permute-start.11 = (bf16[128,512]{1,0:T(8,128)(2,1)S(1)}, bf16[128,512]{1,0:T(8,128)(2,1)S(1)}, u32[]{:S(2)}, u32[]{:S(2)}) collective-permute-start(bf16[128,512]{1,0:T(8,128)(2,1)S(1)} %get-tuple-element.21), channel_id=1, source_target_pairs={{0,8},{8,16},{16,24},{24,0},{1,9},{9,17},{17,25},{25,1},{2,10},{10... | collective-permute-start | bytes 393224 | tf_op jit(solution)/shard_map/ppermute | solution.py:19
  148.6 9.3 %collective-permute-start.12 = (bf16[128,512]{1,0:T(8,128)(2,1)S(1)}, bf16[128,512]{1,0:T(8,128)(2,1)S(1)}, u32[]{:S(2)}, u32[]{:S(2)}) collective-permute-start(bf16[128,512]{1,0:T(8,128)(2,1)S(1)} %get-tuple-element.22), channel_id=1, source_target_pairs={{0,16},{8,24},{16,0},{24,8},{1,17},{9,25},{17,1},{25,9},{2,18},{10... | collective-permute-start | bytes 393224 | tf_op jit(solution)/shard_map/ppermute | solution.py:19
  151.2 8.7 %collective-permute-start.13 = (bf16[128,512]{1,0:T(8,128)(2,1)S(1)}, bf16[128,512]{1,0:T(8,128)(2,1)S(1)}, u32[]{:S(2)}, u32[]{:S(2)}) collective-permute-start(bf16[128,512]{1,0:T(8,128)(2,1)S(1)} %get-tuple-element.23), channel_id=1, source_target_pairs={{0,24},{8,0},{16,8},{24,16},{1,25},{9,1},{17,9},{25,17},{2,26},{10... | collective-permute-start | bytes 393224 | tf_op jit(solution)/shard_map/ppermute | solution.py:19
  162.4 30.6 %all-to-all-start.4 = ((bf16[16,32,352]{2,1,0:T(8,128)(2,1)}), bf16[16,32,352]{2,1,0:T(8,128)(2,1)S(1)}, u32[]{:S(2)}, u32[]{:S(2)}) async-start(bf16[16,32,352]{2,1,0:T(8,128)(2,1)} %shard_map.109), calls=%async_computation.4 | async-start | bytes 786432 | tf_op jit(solution)/shard_map/all_to_all | solution.py:157
  169.2 23.9 %copy-start.5 = (f32[32,352]{1,0:T(8,128)S(1)}, f32[32,352]{1,0:T(8,128)}, u32[]{:S(2)}) copy-start(f32[32,352]{1,0:T(8,128)} %param.15) | copy-start | bytes 135172

commit v4 on v3

--- a/solution.py
+++ b/solution.py
@@ -34,24 +34,22 @@
     return lax.dot_general(a, b, (((ca,), (cb,)), ((), ())), preferred_element_type=F32)
 
 
-def assemble(at, pieces, wholes):
+def assemble(at, pieces, wholes, sems):
     zb, y = at[0], at[1]
     near, a1, a3, far, z1, z3 = pieces
     todo = []
     for yy in range(4):
-        for za in range(4):
-            todo.append((near, (yy, za), za * 512 + zb * 128 + yy * 32))
-            todo.append((far, (yy, za), za * 512 + (zb + 2) % 4 * 128 + yy * 32))
+        todo.append((near.at[yy], 0, yy))
+        todo.append((far.at[yy], 2, yy))
     for r, mine, other in ((1, a1, z1), (3, a3, z3)):
-        base = (zb + r) % 4 * 128
-        for za in range(4):
-            todo.append((mine, (za,), za * 512 + base + y * 32))
-            for dy in range(1, 4):
-                todo.append((other, (dy - 1, za), za * 512 + base + (y + dy) % 4 * 32))
-    for piece, spot, row in todo:
-        rows = pl.ds(pl.multiple_of(row, 32), 32)
-        for m, whole in enumerate(wholes):
-            whole[rows, :] = piece[(*spot, slice(m * 32, (m + 1) * 32))]
+        todo.append((mine, r, y))
+        for dy in range(1, 4):
+            todo.append((other.at[dy - 1], r, (y + dy) % 4))
+    for m, whole in enumerate(wholes):
+        for piece, r, yy in todo:
+            pltpu.make_async_copy(
+                piece.at[:, pl.ds(m * 32, 32), :], whole.at[:, (zb + r) % 4, yy], sems.at[m]
+            ).start()
 
 
 def columns(at, bt, gain, b0, b1, b2, b3, split):
@@ -79,25 +77,34 @@
 
 
 def products(at, tok, *refs):
-    pieces, (gds, keep, give, wg, wu, wd, parts) = refs[:6], refs[6:]
-    assemble(at, pieces, (wg, wu, wd))
-    gate = dot(tok[0], wg[...], 1, 0)
-    up = dot(tok[0], wu[...], 1, 0)
-    hid = 0.5 * dot(tok[1], wd[...], 1, 0)
+    pieces, (gds, both, wg, wu, wd, parts, sems) = refs[:6], refs[6:]
+    assemble(at, pieces, (wg, wu, wd), sems)
+    ready = [False] * 3
+
+    def weight(m):
+        whole = (wg, wu, wd)[m]
+        if not ready[m]:
+            pltpu.make_async_copy(whole, whole, sems.at[m]).wait()
+            ready[m] = True
+        return whole[...].reshape(2048, 352)
+
+    gate = dot(tok[0], weight(0), 1, 0)
+    up = dot(tok[0], weight(1), 1, 0)
+    hid = 0.5 * dot(tok[1], weight(2), 1, 0)
     s = jax.nn.sigmoid(gate)
     gd = (hid * up * s * (1.0 + gate * (1.0 - s))).astype(BF)
     ud = (hid * gate * s).astype(BF)
     for k in range(4):
         for j in range(4):
             gds[k, j] = gd[j * 32 : (j + 1) * 32, :]
-    parts[:, 2048:4096] = (dot(gd, wg[...], 1, 1) + dot(ud, wu[...], 1, 1)).astype(BF)
-    gate = dot(tok[2], wg[...], 1, 0)
-    up = dot(tok[2], wu[...], 1, 0)
+    parts[:, 2048:4096] = (dot(gd, weight(0), 1, 1) + dot(ud, weight(1), 1, 1)).astype(BF)
+    gate = dot(tok[2], weight(0), 1, 0)
+    up = dot(tok[2], weight(1), 1, 0)
     hidden = (gate * jax.nn.sigmoid(gate) * up).astype(BF)
-    parts[:, 0:2048] = dot(hidden, wd[...], 1, 1).astype(BF)
+    parts[:, 0:2048] = dot(hidden, weight(2), 1, 1).astype(BF)
     c = at[2]
-    keep[...] = parts[pl.ds(pl.multiple_of(c * 64, 64), 64), :]
-    give[...] = parts[pl.ds(pl.multiple_of((1 - c) * 64, 64), 64), :]
+    both[0] = parts[pl.ds(pl.multiple_of(c * 64, 64), 64), :]
+    both[1] = parts[pl.ds(pl.multiple_of((1 - c) * 64, 64), 64), :]
 
 
 def merge(at, b0, b1, b2, b3, out):
@@ -117,7 +124,7 @@
 def pair(at, keep, other, *outs):
     for k, out in enumerate(outs):
         rows = pl.ds(pl.multiple_of((at[3] + k) % 4 * 16, 16), 16)
-        out[...] = (keep[rows, :].astype(F32) + other[rows, :].astype(F32)).astype(BF)
+        out[...] = (keep[0, rows, :].astype(F32) + other[1, rows, :].astype(F32)).astype(BF)
 
 
 def finish(at, p0, p1, p2, p3, bt, gain, out):
@@ -136,19 +143,19 @@
 SM = pl.BlockSpec(memory_space=pltpu.SMEM)
 
 
-def call(body, outs, scratch, *args):
+def call(body, outs, scratch, *args, ins=None):
     return pl.pallas_call(
         body,
         out_shape=tuple(jax.ShapeDtypeStruct(o, BF) for o in outs),
-        in_specs=[SM] + [VM] * (len(args) - 1),
+        in_specs=[SM] + (ins or [VM] * (len(args) - 1)),
         out_specs=(VM,) * len(outs),
-        scratch_shapes=[pltpu.VMEM(o, BF) for o in scratch],
+        scratch_shapes=[pltpu.VMEM(o, BF) if isinstance(o, tuple) else o for o in scratch],
         compiler_params=pltpu.CompilerParams(vmem_limit_bytes=LIMIT),
     )(*args)
 
 
 LIMIT = 24 * 1024 * 1024
-W = (2048, 352)
+W = (4, 4, 4, 32, 352)
 TOK = (128, 2048)
 COL = (128, 512)
 
@@ -167,7 +174,7 @@
     near = copies_to_all(a, "y")
     a1 = shift(a, Z, -1)
     a3 = shift(a, Z, 1)
-    a2 = jnp.concatenate([shift(a[:2], Z, -2), shift(a[2:], Z, 2)])
+    a2 = lax.ppermute(a, Z, [(k, (k + (2 if k % 2 else -2)) % 16) for k in range(16)])
     others = lax.dynamic_slice_in_dim(jnp.concatenate([near, near]), y + 1, 3)
     z1 = shift(others, Z, -1)
     z3 = shift(others, Z, 1)
@@ -179,17 +186,18 @@
     b2 = shift(b2, "y", 2)
     b3 = shift(b3, "y", 3)
     (cols,) = call(merge, ((4, *COL),), (), at, b0, b1, b2, b3)
-    gds, keep, give = call(
+    gds, both = call(
         products,
-        ((4, 4, 32, 352), (64, 4096), (64, 4096)),
-        (W, W, W, (128, 4096)),
+        ((4, 4, 32, 352), (2, 64, 4096)),
+        (W, W, W, (128, 4096), pltpu.SemaphoreType.DMA((3,))),
         at, tok, *pieces,
+        ins=[VM] + [pl.BlockSpec(memory_space=pl.ANY)] * 6,
     )
     gds = exchange(gds, "y")
     (grads,) = call(outer, ((16, 32, 352),), (), at, cols, gds)
     gz = exchange(grads, Z)
-    other = shift(give, "c", 1)
-    p0, p1, p2, p3 = call(pair, ((16, 4096),) * 4, (), at, keep, other)
+    other = shift(both, "c", 1)
+    p0, p1, p2, p3 = call(pair, ((16, 4096),) * 4, (), at, both, other)
     p1, p2, p3 = shift(p1, "x", 1), shift(p2, "x", 2), shift(p3, "x", -1)
     (done,) = call(finish, ((16, 4096),), (), at, p0, p1, p2, p3, bt, gain)
     half = lax.all_gather(done, "x", axis=0, tiled=True)

time: 195 us -> 174 us (0.89)
  the two profiles are of different devices: /device:TPU:8 before, /device:TPU:1 now
where the time goes in v4:
time: 174 us; the launch traced here: 173 us
  starting transfers between devices  77.6 us (45%)
  blocking collectives  40.7 us (23%)
  waiting for transfers between devices  30.5 us (18%)
  Pallas kernels  13.2 us (8%)
  local copies, waits for them, and re-layouts  6.12 us (4%)
  other arithmetic  4.01 us (2%)
    ppermute x12, starting transfers between devices, shift(): return lax.ppermute(array, axis, [(k, (k + by) % n) for k in range(n)])  49.7 us
    all_to_all x1, blocking collectives, copies_to_all(): return lax.all_to_all(copies, axis, split_axis=0, concat_axis=0, tiled=True)  30 us
    ppermute x12, waiting for transfers between devices, shift(): return lax.ppermute(array, axis, [(k, (k + by) % n) for k in range(n)])  24.3 us
    pallas_call x7, Pallas kernels, call(): pl.pallas_call(body, out_shape=tuple((jax.ShapeDtypeStruct(o, BF) for o i...  13.2 us
    all_gather x1, blocking collectives, shards(): half = lax.all_gather(done, 'x', axis=0, tiled=True)  10.6 us
    ppermute x1, starting transfers between devices, shards(): lax.ppermute(a, Z, [(k, (k + (2 if k % 2 else -2)) % 16) for k in range(1...  10.3 us
    all_to_all x2, starting transfers between devices, exchange(): return lax.all_to_all(array, axis, split_axis=0, concat_axis=0, tiled=True)  9.24 us
    all_to_all x2, starting transfers between devices, copies_to_all(): return lax.all_to_all(copies, axis, split_axis=0, concat_axis=0, tiled=True)  8.46 us
  transfers between devices with their start and end apart: 17, of which 8 were waited for; matrix products, arithmetic and copies ran while one was open for 1% of the time, Pallas kernels for 4%

profile of v4, /device:TPU:1, one launch (start us, length us, event | category | flops | bytes accessed | tf_op | source)
XLA Modules:
  0.0 173.1 jit_solution(11668290820438332624)
XLA Ops:
  0.6 0.8 pad_maximum_fusion.1
  1.5 30.0 %all_to_all.25 = bf16[4,96,352]{2,1,0:T(8,128)(2,1)} all-to-all(bf16[4,96,352]{2,1,0:T(8,128)(2,1)S(1)} %broadcast_in_dim.9), channel_id=1, replica_groups=mesh['za'=4,'zb'=4,'y'=4,'x'=4,'c'=2] {'za'}, dimensions={0} | all-to-all | bytes 540672 | tf_op jit(solution)/shard_map/all_to_all | solution.py:24
  31.5 2.1 %broadcast_in_dim.10 = bf16[4,4,96,352]{3,2,1,0:T(8,128)(2,1)} broadcast(bf16[4,96,352]{2,1,0:T(8,128)(2,1)} %all_to_all.25), dimensions={1,2,3} | broadcast | bytes 1351680 | tf_op jit(solution)/shard_map/broadcast_in_dim | solution.py:23
  33.6 4.2 %all-to-all-start.1 = ((bf16[4,4,96,352]{3,2,1,0:T(8,128)(2,1)}), bf16[4,4,96,352]{3,2,1,0:T(8,128)(2,1)S(1)}, u32[]{:S(2)}, u32[]{:S(2)}) async-start(bf16[4,4,96,352]{3,2,1,0:T(8,128)(2,1)} %broadcast_in_dim.10), calls=%async_computation.1 | async-start | bytes 2359296 | tf_op jit(solution)/shard_map/all_to_all | solution.py:24
  37.8 10.3 %collective-permute-start.2 = (bf16[4,96,352]{2,1,0:T(8,128)(2,1)}, bf16[4,96,352]{2,1,0:T(8,128)(2,1)S(1)}, u32[]{:S(2)}, u32[]{:S(2)}) collective-permute-start(bf16[4,96,352]{2,1,0:T(8,128)(2,1)} %all_to_all.25), channel_id=1, source_target_pairs={{0,448},{32,96},{64,0},{96,160},{128,64},{160,224},{192,128},{224,... | collective-permute-start | bytes 811016 | tf_op jit(solution)/shard_map/ppermute | solution.py:177
  48.1 6.2 %collective-permute-done.2 = bf16[4,96,352]{2,1,0:T(8,128)(2,1)S(1)} collective-permute-done((bf16[4,96,352]{2,1,0:T(8,128)(2,1)}, bf16[4,96,352]{2,1,0:T(8,128)(2,1)S(1)}, u32[]{:S(2)}, u32[]{:S(2)}) %collective-permute-start.2) | collective-permute-done | bytes 270368 | tf_op jit(solution)/shard_map/ppermute | solution.py:177
  54.2 0.0 all-to-all-done.1.refs_0_
  54.3 1.1 broadcast_in_dim.11
  55.4 4.3 %all-to-all-start.2 = ((bf16[4,4,96,352]{3,2,1,0:T(8,128)(2,1)}), bf16[4,4,96,352]{3,2,1,0:T(8,128)(2,1)}, u32[]{:S(2)}, u32[]{:S(2)}) async-start(bf16[4,4,96,352]{3,2,1,0:T(8,128)(2,1)} %broadcast_in_dim.11), calls=%async_computation.2 | async-start | bytes 2359296 | tf_op jit(solution)/shard_map/all_to_all | solution.py:24
  59.7 0.0 copy-start
  59.7 0.0 copy-start.4
  59.7 1.3 fusion
  61.0 4.1 %collective-permute-start.3 = (bf16[3,4,96,352]{3,2,1,0:T(8,128)(2,1)}, bf16[3,4,96,352]{3,2,1,0:T(8,128)(2,1)}, u32[]{:S(2)}, u32[]{:S(2)}) collective-permute-start(bf16[3,4,96,352]{3,2,1,0:T(8,128)(2,1)} %fusion), channel_id=1, source_target_pairs={{0,480},{32,0},{64,32},{96,64},{128,96},{160,128},{192,160},{224,1... | collective-permute-start | bytes 2433032 | tf_op jit(solution)/shard_map/ppermute | solution.py:19
  65.2 6.4 %collective-permute-start.4 = (bf16[3,4,96,352]{3,2,1,0:T(8,128)(2,1)}, bf16[3,4,96,352]{3,2,1,0:T(8,128)(2,1)}, u32[]{:S(2)}, u32[]{:S(2)}) collective-permute-start(bf16[3,4,96,352]{3,2,1,0:T(8,128)(2,1)} %fusion), channel_id=1, source_target_pairs={{0,32},{32,64},{64,96},{96,128},{128,160},{160,192},{192,224},{224... | collective-permute-start | bytes 2433032 | tf_op jit(solution)/shard_map/ppermute | solution.py:19
  71.6 3.1 %collective-permute-start = (bf16[4,96,352]{2,1,0:T(8,128)(2,1)}, bf16[4,96,352]{2,1,0:T(8,128)(2,1)}, u32[]{:S(2)}, u32[]{:S(2)}) collective-permute-start(bf16[4,96,352]{2,1,0:T(8,128)(2,1)} %all_to_all.25), channel_id=1, source_target_pairs={{0,480},{32,0},{64,32},{96,64},{128,96},{160,128},{192,160},{224,1... | collective-permute-start | bytes 811016 | tf_op jit(solution)/shard_map/ppermute | solution.py:19
  74.6 2.2 %collective-permute-start.1 = (bf16[4,96,352]{2,1,0:T(8,128)(2,1)}, bf16[4,96,352]{2,1,0:T(8,128)(2,1)}, u32[]{:S(2)}, u32[]{:S(2)}) collective-permute-start(bf16[4,96,352]{2,1,0:T(8,128)(2,1)} %all_to_all.25), channel_id=1, source_target_pairs={{0,32},{32,64},{64,96},{96,128},{128,160},{160,192},{192,224},{224... | collective-permute-start | bytes 811016 | tf_op jit(solution)/shard_map/ppermute | solution.py:19
  76.9 0.1 pad_add_fusion.at
  77.0 0.0 copy-done
  77.0 0.0 copy-done.4
  77.0 0.0 copy-start.1
  77.0 1.0 copy-done.1
  78.0 0.0 copy-start.2
  78.0 1.0 copy-done.2
  79.0 1.0 shard_map.103.tok
  80.0 13.4 %collective-permute-done.refs_1_ = bf16[4,96,352]{2,1,0:T(8,128)(2,1)} collective-permute-done((bf16[4,96,352]{2,1,0:T(8,128)(2,1)}, bf16[4,96,352]{2,1,0:T(8,128)(2,1)}, u32[]{:S(2)}, u32[]{:S(2)}) %collective-permute-start) | collective-permute-done | bytes 270368 | tf_op jit(solution)/shard_map/ppermute | solution.py:19
  93.4 3.7 %collective-permute-done.1.refs_2_ = bf16[4,96,352]{2,1,0:T(8,128)(2,1)} collective-permute-done((bf16[4,96,352]{2,1,0:T(8,128)(2,1)}, bf16[4,96,352]{2,1,0:T(8,128)(2,1)}, u32[]{:S(2)}, u32[]{:S(2)}) %collective-permute-start.1) | collective-permute-done | bytes 270368 | tf_op jit(solution)/shard_map/ppermute | solution.py:19
  97.1 0.0 all-to-all-done.2.refs_3_
  97.1 0.0 collective-permute-done.3.refs_4_
  97.1 0.0 collective-permute-done.4.refs_5_
  97.1 6.5 %shard_map.104 = (bf16[4,4,32,352]{3,2,1,0:T(8,128)(2,1)S(1)}, bf16[2,64,4096]{2,1,0:T(8,128)(2,1)}) custom-call(s32[4]{0:T(128)S(1)} %pad_add_fusion.at, bf16[3,128,2048]{2,1,0:T(8,128)(2,1)S(1)} %shard_map.103.tok, bf16[4,4,96,352]{3,2,1,0:T(8,128)(2,1)S(1)} %all-to-all-done.1.refs_0_, bf16[4,96,352]{2,1,0:T(8,128)(2,1)} %collective-permute-done.refs_1_, ...), custom_call_target="tpu_custom_call" | custom-call | tf_op jit(solution)/shard_map/pallas_call | solution.py:147
  103.6 0.0 copy-start.3
  103.7 0.7 copy-done.3
  104.4 4.7 %collective-permute-start.5 = (bf16[2,64,4096]{2,1,0:T(8,128)(2,1)}, bf16[2,64,4096]{2,1,0:T(8,128)(2,1)S(1)}, u32[]{:S(2)}, u32[]{:S(2)}) collective-permute-start(bf16[2,64,4096]{2,1,0:T(8,128)(2,1)} %get-tuple-element.13.keep), channel_id=1, source_target_pairs={{0,1},{1,0},{2,3},{3,2},{4,5},{5,4},{6,7},{7,6},{8,9},{9,8},{10,11... | collective-permute-start | bytes 3145736 | tf_op jit(solution)/shard_map/ppermute | solution.py:19
  109.1 4.2 %all-to-all-start.3 = ((bf16[4,4,32,352]{3,2,1,0:T(8,128)(2,1)}), bf16[4,4,32,352]{3,2,1,0:T(8,128)(2,1)S(1)}, u32[]{:S(2)}, u32[]{:S(2)}) async-start(bf16[4,4,32,352]{3,2,1,0:T(8,128)(2,1)} %copy-done.3), calls=%async_computation.3 | async-start | bytes 786432 | tf_op jit(solution)/shard_map/all_to_all | solution.py:164
  113.3 1.2 shard_map.107
  114.5 3.4 %collective-permute-start.10 = (bf16[128,512]{1,0:T(8,128)(2,1)S(1)}, bf16[128,512]{1,0:T(8,128)(2,1)S(1)}, u32[]{:S(2)}, u32[]{:S(2)}) collective-permute-start(bf16[128,512]{1,0:T(8,128)(2,1)S(1)} %get-tuple-element.19), channel_id=1, source_target_pairs={{0,8},{8,16},{16,24},{24,0},{1,9},{9,17},{17,25},{25,1},{2,10},{10... | collective-permute-start | bytes 393224 | tf_op jit(solution)/shard_map/ppermute | solution.py:19
  117.9 4.3 %collective-permute-start.11 = (bf16[128,512]{1,0:T(8,128)(2,1)S(1)}, bf16[128,512]{1,0:T(8,128)(2,1)S(1)}, u32[]{:S(2)}, u32[]{:S(2)}) collective-permute-start(bf16[128,512]{1,0:T(8,128)(2,1)S(1)} %get-tuple-element.20), channel_id=1, source_target_pairs={{0,16},{8,24},{16,0},{24,8},{1,17},{9,25},{17,1},{25,9},{2,18},{10... | collective-permute-start | bytes 393224 | tf_op jit(solution)/shard_map/ppermute | solution.py:19
  122.2 3.1 %collective-permute-start.12 = (bf16[128,512]{1,0:T(8,128)(2,1)S(1)}, bf16[128,512]{1,0:T(8,128)(2,1)S(1)}, u32[]{:S(2)}, u32[]{:S(2)}) collective-permute-start(bf16[128,512]{1,0:T(8,128)(2,1)S(1)} %get-tuple-element.21), channel_id=1, source_target_pairs={{0,24},{8,0},{16,8},{24,16},{1,25},{9,1},{17,9},{25,17},{2,26},{10... | collective-permute-start | bytes 393224 | tf_op jit(solution)/shard_map/ppermute | solution.py:19
  125.3 0.0 collective-permute-done.10.b1
  125.3 1.6 collective-permute-done.11.b2
  127.0 1.0 collective-permute-done.12.b3
  127.9 0.6 shard_map.108.cols
  128.5 0.0 all-to-all-done.3.gds
  128.5 1.9 %shard_map.109 = bf16[16,32,352]{2,1,0:T(8,128)(2,1)} custom-call(s32[4]{0:T(128)S(1)} %pad_add_fusion.at, bf16[4,128,512]{2,1,0:T(8,128)(2,1)S(1)} %shard_map.108.cols, bf16[4,4,32,352]{3,2,1,0:T(8,128)(2,1)S(1)} %all-to-all-done.3.gds), custom_call_target="tpu_custom_call" | custom-call | tf_op jit(solution)/shard_map/pallas_call | solution.py:147
  130.4 5.1 %all-to-all-start.4 = ((bf16[16,32,352]{2,1,0:T(8,128)(2,1)}), bf16[16,32,352]{2,1,0:T(8,128)(2,1)S(1)}, u32[]{:S(2)}, u32[]{:S(2)}) async-start(bf16[16,32,352]{2,1,0:T(8,128)(2,1)} %shard_map.109), calls=%async_computation.4 | async-start | bytes 786432 | tf_op jit(solution)/shard_map/all_to_all | solution.py:164
  135.5 0.0 collective-permute-done.5.other
  135.5 1.4 shard_map.105
  136.9 0.0 copy-start.5
  136.9 3.3 %collective-permute-start.6 = (bf16[16,4096]{1,0:T(8,128)(2,1)S(1)}, bf16[16,4096]{1,0:T(8,128)(2,1)S(1)}, u32[]{:S(2)}, u32[]{:S(2)}) collective-permute-start(bf16[16,4096]{1,0:T(8,128)(2,1)S(1)} %get-tuple-element.15), channel_id=1, source_target_pairs={{0,2},{2,4},{4,6},{6,0},{1,3},{3,5},{5,7},{7,1},{8,10},{10,12},{12... | collective-permute-start | bytes 393224 | tf_op jit(solution)/shard_map/ppermute | solution.py:19
  140.2 4.3 %collective-permute-start.7 = (bf16[16,4096]{1,0:T(8,128)(2,1)S(1)}, bf16[16,4096]{1,0:T(8,128)(2,1)S(1)}, u32[]{:S(2)}, u32[]{:S(2)}) collective-permute-start(bf16[16,4096]{1,0:T(8,128)(2,1)S(1)} %get-tuple-element.16), channel_id=1, source_target_pairs={{0,4},{2,6},{4,0},{6,2},{1,5},{3,7},{5,1},{7,3},{8,12},{10,14},{12... | collective-permute-start | bytes 393224 | tf_op jit(solution)/shard_map/ppermute | solution.py:19
  144.5 3.1 %collective-permute-start.8 = (bf16[16,4096]{1,0:T(8,128)(2,1)S(1)}, bf16[16,4096]{1,0:T(8,128)(2,1)S(1)}, u32[]{:S(2)}, u32[]{:S(2)}) collective-permute-start(bf16[16,4096]{1,0:T(8,128)(2,1)S(1)} %get-tuple-element.17), channel_id=1, source_target_pairs={{0,6},{2,0},{4,2},{6,4},{1,7},{3,1},{5,3},{7,5},{8,14},{10,8},{12,... | collective-permute-start | bytes 393224 | tf_op jit(solution)/shard_map/ppermute | solution.py:19
  147.6 0.0 collective-permute-done.6.p1
  147.6 0.9 collective-permute-done.7.p2
  148.5 2.9 %collective-permute-done.8.p3 = bf16[16,4096]{1,0:T(8,128)(2,1)S(1)} collective-permute-done((bf16[16,4096]{1,0:T(8,128)(2,1)S(1)}, bf16[16,4096]{1,0:T(8,128)(2,1)S(1)}, u32[]{:S(2)}, u32[]{:S(2)}) %collective-permute-start.8) | collective-permute-done | bytes 131104 | tf_op jit(solution)/shard_map/ppermute | solution.py:19
  151.4 0.7 shard_map.106
  152.1 10.6 %all_gather.3 = bf16[64,4096]{1,0:T(8,128)(2,1)S(1)} all-gather(bf16[16,4096]{1,0:T(8,128)(2,1)S(1)} %shard_map.106), channel_id=1, replica_groups=mesh['za'=4,'zb'=4,'y'=4,'x'=4,'c'=2] {'x'}, dimensions={0}, use_global_device_ids=true | all-gather | bytes 655360 | tf_op jit(solution)/shard_map/all_gather | solution.py:203
  162.8 7.7 %collective-permute-start.9 = (bf16[64,4096]{1,0:T(8,128)(2,1)S(1)}, bf16[64,4096]{1,0:T(8,128)(2,1)S(1)}, u32[]{:S(2)}, u32[]{:S(2)}) collective-permute-start(bf16[64,4096]{1,0:T(8,128)(2,1)S(1)} %all_gather.3), channel_id=1, source_target_pairs={{0,1},{1,0},{2,3},{3,2},{4,5},{5,4},{6,7},{7,6},{8,9},{9,8},{10,11... | collective-permute-start | bytes 1572872 | tf_op jit(solution)/shard_map/ppermute | solution.py:19
  170.5 0.0 all-to-all-done.4
  170.5 0.1 convert_reduce_fusion
  170.6 0.0 copy-done.5
  170.6 0.6 add.13
  171.2 0.8 collective-permute-done.9
  172.0 0.1 broadcast_select_fusion
  172.1 1.0 pad_maximum_fusion
  (1 shorter events, 0.0 us)
Async XLA Ops:
  33.6 20.7 %all-to-all-start.1 = ((bf16[4,4,96,352]{3,2,1,0:T(8,128)(2,1)}), bf16[4,4,96,352]{3,2,1,0:T(8,128)(2,1)S(1)}, u32[]{:S(2)}, u32[]{:S(2)}) async-start(bf16[4,4,96,352]{3,2,1,0:T(8,128)(2,1)} %broadcast_in_dim.10), calls=%async_computation.1 | async-start | bytes 2359296 | tf_op jit(solution)/shard_map/all_to_all | solution.py:24
  37.8 16.5 %collective-permute-start.2 = (bf16[4,96,352]{2,1,0:T(8,128)(2,1)}, bf16[4,96,352]{2,1,0:T(8,128)(2,1)S(1)}, u32[]{:S(2)}, u32[]{:S(2)}) collective-permute-start(bf16[4,96,352]{2,1,0:T(8,128)(2,1)} %all_to_all.25), channel_id=1, source_target_pairs={{0,448},{32,96},{64,0},{96,160},{128,64},{160,224},{192,128},{224,... | collective-permute-start | bytes 811016 | tf_op jit(solution)/shard_map/ppermute | solution.py:177
  55.4 41.7 %all-to-all-start.2 = ((bf16[4,4,96,352]{3,2,1,0:T(8,128)(2,1)}), bf16[4,4,96,352]{3,2,1,0:T(8,128)(2,1)}, u32[]{:S(2)}, u32[]{:S(2)}) async-start(bf16[4,4,96,352]{3,2,1,0:T(8,128)(2,1)} %broadcast_in_dim.11), calls=%async_computation.2 | async-start | bytes 2359296 | tf_op jit(solution)/shard_map/all_to_all | solution.py:24
  59.7 17.3 %copy-start = (bf16[128,2048]{1,0:T(8,128)(2,1)S(1)}, bf16[128,2048]{1,0:T(8,128)(2,1)}, u32[]{:S(2)}) copy-start(bf16[128,2048]{1,0:T(8,128)(2,1)} %bt.5) | copy-start | bytes 1572868
  59.7 17.3 %copy-start.4 = (f32[2048]{0:T(1024)S(1)}, f32[2048]{0:T(1024)}, u32[]{:S(2)}) copy-start(f32[2048]{0:T(1024)} %param.11) | copy-start | bytes 24580
  61.0 36.1 %collective-permute-start.3 = (bf16[3,4,96,352]{3,2,1,0:T(8,128)(2,1)}, bf16[3,4,96,352]{3,2,1,0:T(8,128)(2,1)}, u32[]{:S(2)}, u32[]{:S(2)}) collective-permute-start(bf16[3,4,96,352]{3,2,1,0:T(8,128)(2,1)} %fusion), channel_id=1, source_target_pairs={{0,480},{32,0},{64,32},{96,64},{128,96},{160,128},{192,160},{224,1... | collective-permute-start | bytes 2433032 | tf_op jit(solution)/shard_map/ppermute | solution.py:19
  65.2 31.9 %collective-permute-start.4 = (bf16[3,4,96,352]{3,2,1,0:T(8,128)(2,1)}, bf16[3,4,96,352]{3,2,1,0:T(8,128)(2,1)}, u32[]{:S(2)}, u32[]{:S(2)}) collective-permute-start(bf16[3,4,96,352]{3,2,1,0:T(8,128)(2,1)} %fusion), channel_id=1, source_target_pairs={{0,32},{32,64},{64,96},{96,128},{128,160},{160,192},{192,224},{224... | collective-permute-start | bytes 2433032 | tf_op jit(solution)/shard_map/ppermute | solution.py:19
  71.6 21.9 %collective-permute-start = (bf16[4,96,352]{2,1,0:T(8,128)(2,1)}, bf16[4,96,352]{2,1,0:T(8,128)(2,1)}, u32[]{:S(2)}, u32[]{:S(2)}) collective-permute-start(bf16[4,96,352]{2,1,0:T(8,128)(2,1)} %all_to_all.25), channel_id=1, source_target_pairs={{0,480},{32,0},{64,32},{96,64},{128,96},{160,128},{192,160},{224,1... | collective-permute-start | bytes 811016 | tf_op jit(solution)/shard_map/ppermute | solution.py:19
  74.6 22.5 %collective-permute-start.1 = (bf16[4,96,352]{2,1,0:T(8,128)(2,1)}, bf16[4,96,352]{2,1,0:T(8,128)(2,1)}, u32[]{:S(2)}, u32[]{:S(2)}) collective-permute-start(bf16[4,96,352]{2,1,0:T(8,128)(2,1)} %all_to_all.25), channel_id=1, source_target_pairs={{0,32},{32,64},{64,96},{96,128},{128,160},{160,192},{192,224},{224... | collective-permute-start | bytes 811016 | tf_op jit(solution)/shard_map/ppermute | solution.py:19
  77.0 1.0 copy-start.1
  78.0 1.0 copy-start.2
  103.6 0.7 copy-start.3
  104.4 31.1 %collective-permute-start.5 = (bf16[2,64,4096]{2,1,0:T(8,128)(2,1)}, bf16[2,64,4096]{2,1,0:T(8,128)(2,1)S(1)}, u32[]{:S(2)}, u32[]{:S(2)}) collective-permute-start(bf16[2,64,4096]{2,1,0:T(8,128)(2,1)} %get-tuple-element.13.keep), channel_id=1, source_target_pairs={{0,1},{1,0},{2,3},{3,2},{4,5},{5,4},{6,7},{7,6},{8,9},{9,8},{10,11... | collective-permute-start | bytes 3145736 | tf_op jit(solution)/shard_map/ppermute | solution.py:19
  109.1 19.4 %all-to-all-start.3 = ((bf16[4,4,32,352]{3,2,1,0:T(8,128)(2,1)}), bf16[4,4,32,352]{3,2,1,0:T(8,128)(2,1)S(1)}, u32[]{:S(2)}, u32[]{:S(2)}) async-start(bf16[4,4,32,352]{3,2,1,0:T(8,128)(2,1)} %copy-done.3), calls=%async_computation.3 | async-start | bytes 786432 | tf_op jit(solution)/shard_map/all_to_all | solution.py:164
  114.5 10.8 %collective-permute-start.10 = (bf16[128,512]{1,0:T(8,128)(2,1)S(1)}, bf16[128,512]{1,0:T(8,128)(2,1)S(1)}, u32[]{:S(2)}, u32[]{:S(2)}) collective-permute-start(bf16[128,512]{1,0:T(8,128)(2,1)S(1)} %get-tuple-element.19), channel_id=1, source_target_pairs={{0,8},{8,16},{16,24},{24,0},{1,9},{9,17},{17,25},{25,1},{2,10},{10... | collective-permute-start | bytes 393224 | tf_op jit(solution)/shard_map/ppermute | solution.py:19
  117.9 9.1 %collective-permute-start.11 = (bf16[128,512]{1,0:T(8,128)(2,1)S(1)}, bf16[128,512]{1,0:T(8,128)(2,1)S(1)}, u32[]{:S(2)}, u32[]{:S(2)}) collective-permute-start(bf16[128,512]{1,0:T(8,128)(2,1)S(1)} %get-tuple-element.20), channel_id=1, source_target_pairs={{0,16},{8,24},{16,0},{24,8},{1,17},{9,25},{17,1},{25,9},{2,18},{10... | collective-permute-start | bytes 393224 | tf_op jit(solution)/shard_map/ppermute | solution.py:19
  122.2 5.7 %collective-permute-start.12 = (bf16[128,512]{1,0:T(8,128)(2,1)S(1)}, bf16[128,512]{1,0:T(8,128)(2,1)S(1)}, u32[]{:S(2)}, u32[]{:S(2)}) collective-permute-start(bf16[128,512]{1,0:T(8,128)(2,1)S(1)} %get-tuple-element.21), channel_id=1, source_target_pairs={{0,24},{8,0},{16,8},{24,16},{1,25},{9,1},{17,9},{25,17},{2,26},{10... | collective-permute-start | bytes 393224 | tf_op jit(solution)/shard_map/ppermute | solution.py:19
  130.4 40.1 %all-to-all-start.4 = ((bf16[16,32,352]{2,1,0:T(8,128)(2,1)}), bf16[16,32,352]{2,1,0:T(8,128)(2,1)S(1)}, u32[]{:S(2)}, u32[]{:S(2)}) async-start(bf16[16,32,352]{2,1,0:T(8,128)(2,1)} %shard_map.109), calls=%async_computation.4 | async-start | bytes 786432 | tf_op jit(solution)/shard_map/all_to_all | solution.py:164
  136.9 33.7 %copy-start.5 = (f32[32,352]{1,0:T(8,128)S(1)}, f32[32,352]{1,0:T(8,128)}, u32[]{:S(2)}) copy-start(f32[32,352]{1,0:T(8,128)} %param.15) | copy-start | bytes 135172
  136.9 10.7 %collective-permute-start.6 = (bf16[16,4096]{1,0:T(8,128)(2,1)S(1)}, bf16[16,4096]{1,0:T(8,128)(2,1)S(1)}, u32[]{:S(2)}, u32[]{:S(2)}) collective-permute-start(bf16[16,4096]{1,0:T(8,128)(2,1)S(1)} %get-tuple-element.15), channel_id=1, source_target_pairs={{0,2},{2,4},{4,6},{6,0},{1,3},{3,5},{5,7},{7,1},{8,10},{10,12},{12... | collective-permute-start | bytes 393224 | tf_op jit(solution)/shard_map/ppermute | solution.py:19
  140.2 8.3 %collective-permute-start.7 = (bf16[16,4096]{1,0:T(8,128)(2,1)S(1)}, bf16[16,4096]{1,0:T(8,128)(2,1)S(1)}, u32[]{:S(2)}, u32[]{:S(2)}) collective-permute-start(bf16[16,4096]{1,0:T(8,128)(2,1)S(1)} %get-tuple-element.16), channel_id=1, source_target_pairs={{0,4},{2,6},{4,0},{6,2},{1,5},{3,7},{5,1},{7,3},{8,12},{10,14},{12... | collective-permute-start | bytes 393224 | tf_op jit(solution)/shard_map/ppermute | solution.py:19
  144.5 6.9 %collective-permute-start.8 = (bf16[16,4096]{1,0:T(8,128)(2,1)S(1)}, bf16[16,4096]{1,0:T(8,128)(2,1)S(1)}, u32[]{:S(2)}, u32[]{:S(2)}) collective-permute-start(bf16[16,4096]{1,0:T(8,128)(2,1)S(1)} %get-tuple-element.17), channel_id=1, source_target_pairs={{0,6},{2,0},{4,2},{6,4},{1,7},{3,1},{5,3},{7,5},{8,14},{10,8},{12,... | collective-permute-start | bytes 393224 | tf_op jit(solution)/shard_map/ppermute | solution.py:19
  162.8 9.2 %collective-permute-start.9 = (bf16[64,4096]{1,0:T(8,128)(2,1)S(1)}, bf16[64,4096]{1,0:T(8,128)(2,1)S(1)}, u32[]{:S(2)}, u32[]{:S(2)}) collective-permute-start(bf16[64,4096]{1,0:T(8,128)(2,1)S(1)} %all_gather.3), channel_id=1, source_target_pairs={{0,1},{1,0},{2,3},{3,2},{4,5},{5,4},{6,7},{7,6},{8,9},{9,8},{10,11... | collective-permute-start | bytes 1572872 | tf_op jit(solution)/shard_map/ppermute | solution.py:19

commit v5 on v4

--- a/solution.py
+++ b/solution.py
@@ -77,9 +77,10 @@
 
 
 def products(at, tok, *refs):
-    pieces, (gds, both, wg, wu, wd, parts, sems) = refs[:6], refs[6:]
+    pieces, (gds, both, wg, wu, wd, own, parts, sems, outs) = refs[:6], refs[6:]
     assemble(at, pieces, (wg, wu, wd), sems)
     ready = [False] * 3
+    stores = []
 
     def weight(m):
         whole = (wg, wu, wd)[m]
@@ -88,23 +89,34 @@
             ready[m] = True
         return whole[...].reshape(2048, 352)
 
+    def store(source, target):
+        copy = pltpu.make_async_copy(source, target, outs.at[len(stores)])
+        copy.start()
+        stores.append(copy)
+
+    def store_parts(columns):
+        for k, half in enumerate((at[2], 1 - at[2])):
+            rows = pl.ds(pl.multiple_of(half * 64, 64), 64)
+            store(parts.at[rows, columns], both.at[k, :, columns])
+
     gate = dot(tok[0], weight(0), 1, 0)
     up = dot(tok[0], weight(1), 1, 0)
     hid = 0.5 * dot(tok[1], weight(2), 1, 0)
     s = jax.nn.sigmoid(gate)
     gd = (hid * up * s * (1.0 + gate * (1.0 - s))).astype(BF)
     ud = (hid * gate * s).astype(BF)
+    own[...] = gd.reshape(4, 32, 352)
     for k in range(4):
-        for j in range(4):
-            gds[k, j] = gd[j * 32 : (j + 1) * 32, :]
+        store(own, gds.at[k])
     parts[:, 2048:4096] = (dot(gd, weight(0), 1, 1) + dot(ud, weight(1), 1, 1)).astype(BF)
+    store_parts(pl.ds(2048, 2048))
     gate = dot(tok[2], weight(0), 1, 0)
     up = dot(tok[2], weight(1), 1, 0)
     hidden = (gate * jax.nn.sigmoid(gate) * up).astype(BF)
     parts[:, 0:2048] = dot(hidden, weight(2), 1, 1).astype(BF)
-    c = at[2]
-    both[0] = parts[pl.ds(pl.multiple_of(c * 64, 64), 64), :]
-    both[1] = parts[pl.ds(pl.multiple_of((1 - c) * 64, 64), 64), :]
+    store_parts(pl.ds(0, 2048))
+    for copy in stores:
+        copy.wait()
 
 
 def merge(at, b0, b1, b2, b3, out):
@@ -141,14 +153,17 @@
 
 VM = pl.BlockSpec(memory_space=pltpu.VMEM)
 SM = pl.BlockSpec(memory_space=pltpu.SMEM)
-
-
-def call(body, outs, scratch, *args, ins=None):
+ANY = pl.BlockSpec(memory_space=pl.ANY)
+DMA = pltpu.SemaphoreType.DMA
+
+
+def call(body, outs, scratch, *args, ins=None, to=None):
+    shape = (lambda o: pltpu.HBM(o, BF)) if to else (lambda o: jax.ShapeDtypeStruct(o, BF))
     return pl.pallas_call(
         body,
-        out_shape=tuple(jax.ShapeDtypeStruct(o, BF) for o in outs),
+        out_shape=tuple(shape(o) for o in outs),
         in_specs=[SM] + (ins or [VM] * (len(args) - 1)),
-        out_specs=(VM,) * len(outs),
+        out_specs=(to or VM,) * len(outs),
         scratch_shapes=[pltpu.VMEM(o, BF) if isinstance(o, tuple) else o for o in scratch],
         compiler_params=pltpu.CompilerParams(vmem_limit_bytes=LIMIT),
     )(*args)
@@ -189,16 +204,19 @@
     gds, both = call(
         products,
         ((4, 4, 32, 352), (2, 64, 4096)),
-        (W, W, W, (128, 4096), pltpu.SemaphoreType.DMA((3,))),
+        (W, W, W, (4, 32, 352), (128, 4096), DMA((3,)), DMA((8,))),
         at, tok, *pieces,
-        ins=[VM] + [pl.BlockSpec(memory_space=pl.ANY)] * 6,
+        ins=[VM] + [ANY] * 6,
+        to=ANY,
     )
     gds = exchange(gds, "y")
     (grads,) = call(outer, ((16, 32, 352),), (), at, cols, gds)
     gz = exchange(grads, Z)
     other = shift(both, "c", 1)
     p0, p1, p2, p3 = call(pair, ((16, 4096),) * 4, (), at, both, other)
-    p1, p2, p3 = shift(p1, "x", 1), shift(p2, "x", 2), shift(p3, "x", -1)
+    p1 = shift(p1, "x", 1)
+    p2 = shift(p2, "x", 2)
+    p3 = shift(p3, "x", -1)
     (done,) = call(finish, ((16, 4096),), (), at, p0, p1, p2, p3, bt, gain)
     half = lax.all_gather(done, "x", axis=0, tiled=True)
     other = shift(half, "c", 1)

time: 174 us -> 173 us (level)
  no operation moved by 1% of the time
where the time goes in v5:
time: 173 us; the launch traced here: 172 us
  starting transfers between devices  77.6 us (45%)
  blocking collectives  40.7 us (24%)
  waiting for transfers between devices  30.5 us (18%)
  Pallas kernels  13.1 us (8%)
  local copies, waits for them, and re-layouts  5.38 us (3%)
  other arithmetic  4.07 us (2%)
    ppermute x12, starting transfers between devices, shift(): return lax.ppermute(array, axis, [(k, (k + by) % n) for k in range(n)])  49.7 us
    all_to_all x1, blocking collectives, copies_to_all(): return lax.all_to_all(copies, axis, split_axis=0, concat_axis=0, tiled=True)  30 us
    ppermute x12, waiting for transfers between devices, shift(): return lax.ppermute(array, axis, [(k, (k + by) % n) for k in range(n)])  24.3 us
    pallas_call x7, Pallas kernels, call(): pl.pallas_call(body, out_shape=tuple((shape(o) for o in outs)), in_specs=...  13.1 us
    all_gather x1, blocking collectives, shards(): half = lax.all_gather(done, 'x', axis=0, tiled=True)  10.6 us
    ppermute x1, starting transfers between devices, shards(): lax.ppermute(a, Z, [(k, (k + (2 if k % 2 else -2)) % 16) for k in range(1...  10.3 us
    all_to_all x2, starting transfers between devices, exchange(): return lax.all_to_all(array, axis, split_axis=0, concat_axis=0, tiled=True)  9.24 us
    all_to_all x2, starting transfers between devices, copies_to_all(): return lax.all_to_all(copies, axis, split_axis=0, concat_axis=0, tiled=True)  8.46 us
  transfers between devices with their start and end apart: 17, of which 8 were waited for; matrix products, arithmetic and copies ran while one was open for 1% of the time, Pallas kernels for 4%

profile of v5, /device:TPU:1, one launch (start us, length us, event | category | flops | bytes accessed | tf_op | source)
XLA Modules:
  0.0 172.3 jit_solution(15725710858559338613)
XLA Ops:
  0.6 0.8 pad_maximum_fusion.1
  1.5 30.0 %all_to_all.25 = bf16[4,96,352]{2,1,0:T(8,128)(2,1)} all-to-all(bf16[4,96,352]{2,1,0:T(8,128)(2,1)S(1)} %broadcast_in_dim.9), channel_id=1, replica_groups=mesh['za'=4,'zb'=4,'y'=4,'x'=4,'c'=2] {'za'}, dimensions={0} | all-to-all | bytes 540672 | tf_op jit(solution)/shard_map/all_to_all | solution.py:24
  31.5 2.1 %broadcast_in_dim.10 = bf16[4,4,96,352]{3,2,1,0:T(8,128)(2,1)} broadcast(bf16[4,96,352]{2,1,0:T(8,128)(2,1)} %all_to_all.25), dimensions={1,2,3} | broadcast | bytes 1351680 | tf_op jit(solution)/shard_map/broadcast_in_dim | solution.py:23
  33.6 4.2 %all-to-all-start.1 = ((bf16[4,4,96,352]{3,2,1,0:T(8,128)(2,1)}), bf16[4,4,96,352]{3,2,1,0:T(8,128)(2,1)S(1)}, u32[]{:S(2)}, u32[]{:S(2)}) async-start(bf16[4,4,96,352]{3,2,1,0:T(8,128)(2,1)} %broadcast_in_dim.10), calls=%async_computation.1 | async-start | bytes 2359296 | tf_op jit(solution)/shard_map/all_to_all | solution.py:24
  37.8 10.3 %collective-permute-start.2 = (bf16[4,96,352]{2,1,0:T(8,128)(2,1)}, bf16[4,96,352]{2,1,0:T(8,128)(2,1)S(1)}, u32[]{:S(2)}, u32[]{:S(2)}) collective-permute-start(bf16[4,96,352]{2,1,0:T(8,128)(2,1)} %all_to_all.25), channel_id=1, source_target_pairs={{0,448},{32,96},{64,0},{96,160},{128,64},{160,224},{192,128},{224,... | collective-permute-start | bytes 811016 | tf_op jit(solution)/shard_map/ppermute | solution.py:192
  48.1 6.2 %collective-permute-done.2 = bf16[4,96,352]{2,1,0:T(8,128)(2,1)S(1)} collective-permute-done((bf16[4,96,352]{2,1,0:T(8,128)(2,1)}, bf16[4,96,352]{2,1,0:T(8,128)(2,1)S(1)}, u32[]{:S(2)}, u32[]{:S(2)}) %collective-permute-start.2) | collective-permute-done | bytes 270368 | tf_op jit(solution)/shard_map/ppermute | solution.py:192
  54.2 0.0 all-to-all-done.1.refs_0_
  54.3 1.1 broadcast_in_dim.11
  55.4 4.3 %all-to-all-start.2 = ((bf16[4,4,96,352]{3,2,1,0:T(8,128)(2,1)}), bf16[4,4,96,352]{3,2,1,0:T(8,128)(2,1)}, u32[]{:S(2)}, u32[]{:S(2)}) async-start(bf16[4,4,96,352]{3,2,1,0:T(8,128)(2,1)} %broadcast_in_dim.11), calls=%async_computation.2 | async-start | bytes 2359296 | tf_op jit(solution)/shard_map/all_to_all | solution.py:24
  59.7 0.0 copy-start
  59.7 0.0 copy-start.4
  59.7 1.3 fusion
  61.0 4.1 %collective-permute-start.3 = (bf16[3,4,96,352]{3,2,1,0:T(8,128)(2,1)}, bf16[3,4,96,352]{3,2,1,0:T(8,128)(2,1)}, u32[]{:S(2)}, u32[]{:S(2)}) collective-permute-start(bf16[3,4,96,352]{3,2,1,0:T(8,128)(2,1)} %fusion), channel_id=1, source_target_pairs={{0,480},{32,0},{64,32},{96,64},{128,96},{160,128},{192,160},{224,1... | collective-permute-start | bytes 2433032 | tf_op jit(solution)/shard_map/ppermute | solution.py:19
  65.2 6.4 %collective-permute-start.4 = (bf16[3,4,96,352]{3,2,1,0:T(8,128)(2,1)}, bf16[3,4,96,352]{3,2,1,0:T(8,128)(2,1)}, u32[]{:S(2)}, u32[]{:S(2)}) collective-permute-start(bf16[3,4,96,352]{3,2,1,0:T(8,128)(2,1)} %fusion), channel_id=1, source_target_pairs={{0,32},{32,64},{64,96},{96,128},{128,160},{160,192},{192,224},{224... | collective-permute-start | bytes 2433032 | tf_op jit(solution)/shard_map/ppermute | solution.py:19
  71.6 3.1 %collective-permute-start = (bf16[4,96,352]{2,1,0:T(8,128)(2,1)}, bf16[4,96,352]{2,1,0:T(8,128)(2,1)}, u32[]{:S(2)}, u32[]{:S(2)}) collective-permute-start(bf16[4,96,352]{2,1,0:T(8,128)(2,1)} %all_to_all.25), channel_id=1, source_target_pairs={{0,480},{32,0},{64,32},{96,64},{128,96},{160,128},{192,160},{224,1... | collective-permute-start | bytes 811016 | tf_op jit(solution)/shard_map/ppermute | solution.py:19
  74.6 2.2 %collective-permute-start.1 = (bf16[4,96,352]{2,1,0:T(8,128)(2,1)}, bf16[4,96,352]{2,1,0:T(8,128)(2,1)}, u32[]{:S(2)}, u32[]{:S(2)}) collective-permute-start(bf16[4,96,352]{2,1,0:T(8,128)(2,1)} %all_to_all.25), channel_id=1, source_target_pairs={{0,32},{32,64},{64,96},{96,128},{128,160},{160,192},{192,224},{224... | collective-permute-start | bytes 811016 | tf_op jit(solution)/shard_map/ppermute | solution.py:19
  76.9 0.1 pad_add_fusion.at
  77.0 0.0 copy-done
  77.0 0.0 copy-done.4
  77.0 0.0 copy-start.2
  77.0 1.0 copy-done.2
  78.0 0.0 copy-start.3
  78.0 1.0 copy-done.3
  79.0 1.0 shard_map.103.tok
  80.0 13.4 %collective-permute-done.refs_1_ = bf16[4,96,352]{2,1,0:T(8,128)(2,1)} collective-permute-done((bf16[4,96,352]{2,1,0:T(8,128)(2,1)}, bf16[4,96,352]{2,1,0:T(8,128)(2,1)}, u32[]{:S(2)}, u32[]{:S(2)}) %collective-permute-start) | collective-permute-done | bytes 270368 | tf_op jit(solution)/shard_map/ppermute | solution.py:19
  93.4 3.7 %collective-permute-done.1.refs_2_ = bf16[4,96,352]{2,1,0:T(8,128)(2,1)} collective-permute-done((bf16[4,96,352]{2,1,0:T(8,128)(2,1)}, bf16[4,96,352]{2,1,0:T(8,128)(2,1)}, u32[]{:S(2)}, u32[]{:S(2)}) %collective-permute-start.1) | collective-permute-done | bytes 270368 | tf_op jit(solution)/shard_map/ppermute | solution.py:19
  97.1 0.0 all-to-all-done.2.refs_3_
  97.1 0.0 collective-permute-done.3.refs_4_
  97.1 0.0 collective-permute-done.4.refs_5_
  97.1 6.4 %shard_map.104 = (bf16[4,4,32,352]{3,2,1,0:T(8,128)(2,1)}, bf16[2,64,4096]{2,1,0:T(8,128)(2,1)}) custom-call(s32[4]{0:T(128)S(1)} %pad_add_fusion.at, bf16[3,128,2048]{2,1,0:T(8,128)(2,1)S(1)} %shard_map.103.tok, bf16[4,4,96,352]{3,2,1,0:T(8,128)(2,1)S(1)} %all-to-all-done.1.refs_0_, bf16[4,96,352]{2,1,0:T(8,128)(2,1)} %collective-permute-done.refs_1_, ...), custom_call_target="tpu_custom_call" | custom-call | tf_op jit(solution)/shard_map/pallas_call | solution.py:162
  103.5 4.7 %collective-permute-start.5 = (bf16[2,64,4096]{2,1,0:T(8,128)(2,1)}, bf16[2,64,4096]{2,1,0:T(8,128)(2,1)}, u32[]{:S(2)}, u32[]{:S(2)}) collective-permute-start(bf16[2,64,4096]{2,1,0:T(8,128)(2,1)} %get-tuple-element.13.keep), channel_id=1, source_target_pairs={{0,1},{1,0},{2,3},{3,2},{4,5},{5,4},{6,7},{7,6},{8,9},{9,8},{10,11... | collective-permute-start | bytes 3145736 | tf_op jit(solution)/shard_map/ppermute | solution.py:19
  108.2 4.2 %all-to-all-start.3 = ((bf16[4,4,32,352]{3,2,1,0:T(8,128)(2,1)}), bf16[4,4,32,352]{3,2,1,0:T(8,128)(2,1)S(1)}, u32[]{:S(2)}, u32[]{:S(2)}) async-start(bf16[4,4,32,352]{3,2,1,0:T(8,128)(2,1)} %get-tuple-element.22), calls=%async_computation.3 | async-start | bytes 786432 | tf_op jit(solution)/shard_map/all_to_all | solution.py:179
  112.4 1.2 shard_map.107
  113.6 3.4 %collective-permute-start.10 = (bf16[128,512]{1,0:T(8,128)(2,1)S(1)}, bf16[128,512]{1,0:T(8,128)(2,1)S(1)}, u32[]{:S(2)}, u32[]{:S(2)}) collective-permute-start(bf16[128,512]{1,0:T(8,128)(2,1)S(1)} %get-tuple-element.19), channel_id=1, source_target_pairs={{0,8},{8,16},{16,24},{24,0},{1,9},{9,17},{17,25},{25,1},{2,10},{10... | collective-permute-start | bytes 393224 | tf_op jit(solution)/shard_map/ppermute | solution.py:19
  117.0 4.3 %collective-permute-start.11 = (bf16[128,512]{1,0:T(8,128)(2,1)S(1)}, bf16[128,512]{1,0:T(8,128)(2,1)S(1)}, u32[]{:S(2)}, u32[]{:S(2)}) collective-permute-start(bf16[128,512]{1,0:T(8,128)(2,1)S(1)} %get-tuple-element.20), channel_id=1, source_target_pairs={{0,16},{8,24},{16,0},{24,8},{1,17},{9,25},{17,1},{25,9},{2,18},{10... | collective-permute-start | bytes 393224 | tf_op jit(solution)/shard_map/ppermute | solution.py:19
  121.3 3.1 %collective-permute-start.12 = (bf16[128,512]{1,0:T(8,128)(2,1)S(1)}, bf16[128,512]{1,0:T(8,128)(2,1)S(1)}, u32[]{:S(2)}, u32[]{:S(2)}) collective-permute-start(bf16[128,512]{1,0:T(8,128)(2,1)S(1)} %get-tuple-element.21), channel_id=1, source_target_pairs={{0,24},{8,0},{16,8},{24,16},{1,25},{9,1},{17,9},{25,17},{2,26},{10... | collective-permute-start | bytes 393224 | tf_op jit(solution)/shard_map/ppermute | solution.py:19
  124.4 0.0 collective-permute-done.10.b1
  124.4 1.6 collective-permute-done.11.b2
  126.1 1.0 collective-permute-done.12.b3
  127.0 0.6 shard_map.108.cols
  127.6 0.0 copy-start.1
  127.6 0.0 all-to-all-done.3.gds
  127.6 1.9 %shard_map.109 = bf16[16,32,352]{2,1,0:T(8,128)(2,1)} custom-call(s32[4]{0:T(128)S(1)} %pad_add_fusion.at, bf16[4,128,512]{2,1,0:T(8,128)(2,1)S(1)} %shard_map.108.cols, bf16[4,4,32,352]{3,2,1,0:T(8,128)(2,1)S(1)} %all-to-all-done.3.gds), custom_call_target="tpu_custom_call" | custom-call | tf_op jit(solution)/shard_map/pallas_call | solution.py:162
  129.5 5.1 %all-to-all-start.4 = ((bf16[16,32,352]{2,1,0:T(8,128)(2,1)}), bf16[16,32,352]{2,1,0:T(8,128)(2,1)S(1)}, u32[]{:S(2)}, u32[]{:S(2)}) async-start(bf16[16,32,352]{2,1,0:T(8,128)(2,1)} %shard_map.109), calls=%async_computation.4 | async-start | bytes 786432 | tf_op jit(solution)/shard_map/all_to_all | solution.py:179
  134.6 0.0 collective-permute-done.5.other
  134.6 0.0 copy-done.1
  134.6 1.4 shard_map.105
  136.0 0.0 copy-start.5
  136.0 3.3 %collective-permute-start.6 = (bf16[16,4096]{1,0:T(8,128)(2,1)S(1)}, bf16[16,4096]{1,0:T(8,128)(2,1)S(1)}, u32[]{:S(2)}, u32[]{:S(2)}) collective-permute-start(bf16[16,4096]{1,0:T(8,128)(2,1)S(1)} %get-tuple-element.15), channel_id=1, source_target_pairs={{0,2},{2,4},{4,6},{6,0},{1,3},{3,5},{5,7},{7,1},{8,10},{10,12},{12... | collective-permute-start | bytes 393224 | tf_op jit(solution)/shard_map/ppermute | solution.py:19
  139.3 4.3 %collective-permute-start.7 = (bf16[16,4096]{1,0:T(8,128)(2,1)S(1)}, bf16[16,4096]{1,0:T(8,128)(2,1)S(1)}, u32[]{:S(2)}, u32[]{:S(2)}) collective-permute-start(bf16[16,4096]{1,0:T(8,128)(2,1)S(1)} %get-tuple-element.16), channel_id=1, source_target_pairs={{0,4},{2,6},{4,0},{6,2},{1,5},{3,7},{5,1},{7,3},{8,12},{10,14},{12... | collective-permute-start | bytes 393224 | tf_op jit(solution)/shard_map/ppermute | solution.py:19
  143.6 3.1 %collective-permute-start.8 = (bf16[16,4096]{1,0:T(8,128)(2,1)S(1)}, bf16[16,4096]{1,0:T(8,128)(2,1)S(1)}, u32[]{:S(2)}, u32[]{:S(2)}) collective-permute-start(bf16[16,4096]{1,0:T(8,128)(2,1)S(1)} %get-tuple-element.17), channel_id=1, source_target_pairs={{0,6},{2,0},{4,2},{6,4},{1,7},{3,1},{5,3},{7,5},{8,14},{10,8},{12,... | collective-permute-start | bytes 393224 | tf_op jit(solution)/shard_map/ppermute | solution.py:19
  146.7 0.0 collective-permute-done.6.p1
  146.7 0.9 collective-permute-done.7.p2
  147.6 2.9 %collective-permute-done.8.p3 = bf16[16,4096]{1,0:T(8,128)(2,1)S(1)} collective-permute-done((bf16[16,4096]{1,0:T(8,128)(2,1)S(1)}, bf16[16,4096]{1,0:T(8,128)(2,1)S(1)}, u32[]{:S(2)}, u32[]{:S(2)}) %collective-permute-start.8) | collective-permute-done | bytes 131104 | tf_op jit(solution)/shard_map/ppermute | solution.py:19
  150.6 0.7 shard_map.106
  151.3 10.6 %all_gather.3 = bf16[64,4096]{1,0:T(8,128)(2,1)S(1)} all-gather(bf16[16,4096]{1,0:T(8,128)(2,1)S(1)} %shard_map.106), channel_id=1, replica_groups=mesh['za'=4,'zb'=4,'y'=4,'x'=4,'c'=2] {'x'}, dimensions={0}, use_global_device_ids=true | all-gather | bytes 655360 | tf_op jit(solution)/shard_map/all_gather | solution.py:221
  161.9 7.7 %collective-permute-start.9 = (bf16[64,4096]{1,0:T(8,128)(2,1)S(1)}, bf16[64,4096]{1,0:T(8,128)(2,1)S(1)}, u32[]{:S(2)}, u32[]{:S(2)}) collective-permute-start(bf16[64,4096]{1,0:T(8,128)(2,1)S(1)} %all_gather.3), channel_id=1, source_target_pairs={{0,1},{1,0},{2,3},{3,2},{4,5},{5,4},{6,7},{7,6},{8,9},{9,8},{10,11... | collective-permute-start | bytes 1572872 | tf_op jit(solution)/shard_map/ppermute | solution.py:19
  169.6 0.0 all-to-all-done.4
  169.6 0.1 convert_reduce_fusion
  169.7 0.0 copy-done.5
  169.7 0.6 add.13
  170.3 0.8 collective-permute-done.9
  171.1 0.1 broadcast_select_fusion
  171.2 1.0 pad_maximum_fusion
  (1 shorter events, 0.0 us)
Async XLA Ops:
  33.6 20.7 %all-to-all-start.1 = ((bf16[4,4,96,352]{3,2,1,0:T(8,128)(2,1)}), bf16[4,4,96,352]{3,2,1,0:T(8,128)(2,1)S(1)}, u32[]{:S(2)}, u32[]{:S(2)}) async-start(bf16[4,4,96,352]{3,2,1,0:T(8,128)(2,1)} %broadcast_in_dim.10), calls=%async_computation.1 | async-start | bytes 2359296 | tf_op jit(solution)/shard_map/all_to_all | solution.py:24
  37.8 16.5 %collective-permute-start.2 = (bf16[4,96,352]{2,1,0:T(8,128)(2,1)}, bf16[4,96,352]{2,1,0:T(8,128)(2,1)S(1)}, u32[]{:S(2)}, u32[]{:S(2)}) collective-permute-start(bf16[4,96,352]{2,1,0:T(8,128)(2,1)} %all_to_all.25), channel_id=1, source_target_pairs={{0,448},{32,96},{64,0},{96,160},{128,64},{160,224},{192,128},{224,... | collective-permute-start | bytes 811016 | tf_op jit(solution)/shard_map/ppermute | solution.py:192
  55.4 41.7 %all-to-all-start.2 = ((bf16[4,4,96,352]{3,2,1,0:T(8,128)(2,1)}), bf16[4,4,96,352]{3,2,1,0:T(8,128)(2,1)}, u32[]{:S(2)}, u32[]{:S(2)}) async-start(bf16[4,4,96,352]{3,2,1,0:T(8,128)(2,1)} %broadcast_in_dim.11), calls=%async_computation.2 | async-start | bytes 2359296 | tf_op jit(solution)/shard_map/all_to_all | solution.py:24
  59.7 17.3 %copy-start = (bf16[128,2048]{1,0:T(8,128)(2,1)S(1)}, bf16[128,2048]{1,0:T(8,128)(2,1)}, u32[]{:S(2)}) copy-start(bf16[128,2048]{1,0:T(8,128)(2,1)} %bt.5) | copy-start | bytes 1572868
  59.7 17.3 %copy-start.4 = (f32[2048]{0:T(1024)S(1)}, f32[2048]{0:T(1024)}, u32[]{:S(2)}) copy-start(f32[2048]{0:T(1024)} %param.11) | copy-start | bytes 24580
  61.0 36.1 %collective-permute-start.3 = (bf16[3,4,96,352]{3,2,1,0:T(8,128)(2,1)}, bf16[3,4,96,352]{3,2,1,0:T(8,128)(2,1)}, u32[]{:S(2)}, u32[]{:S(2)}) collective-permute-start(bf16[3,4,96,352]{3,2,1,0:T(8,128)(2,1)} %fusion), channel_id=1, source_target_pairs={{0,480},{32,0},{64,32},{96,64},{128,96},{160,128},{192,160},{224,1... | collective-permute-start | bytes 2433032 | tf_op jit(solution)/shard_map/ppermute | solution.py:19
  65.2 31.9 %collective-permute-start.4 = (bf16[3,4,96,352]{3,2,1,0:T(8,128)(2,1)}, bf16[3,4,96,352]{3,2,1,0:T(8,128)(2,1)}, u32[]{:S(2)}, u32[]{:S(2)}) collective-permute-start(bf16[3,4,96,352]{3,2,1,0:T(8,128)(2,1)} %fusion), channel_id=1, source_target_pairs={{0,32},{32,64},{64,96},{96,128},{128,160},{160,192},{192,224},{224... | collective-permute-start | bytes 2433032 | tf_op jit(solution)/shard_map/ppermute | solution.py:19
  71.6 21.9 %collective-permute-start = (bf16[4,96,352]{2,1,0:T(8,128)(2,1)}, bf16[4,96,352]{2,1,0:T(8,128)(2,1)}, u32[]{:S(2)}, u32[]{:S(2)}) collective-permute-start(bf16[4,96,352]{2,1,0:T(8,128)(2,1)} %all_to_all.25), channel_id=1, source_target_pairs={{0,480},{32,0},{64,32},{96,64},{128,96},{160,128},{192,160},{224,1... | collective-permute-start | bytes 811016 | tf_op jit(solution)/shard_map/ppermute | solution.py:19
  74.6 22.5 %collective-permute-start.1 = (bf16[4,96,352]{2,1,0:T(8,128)(2,1)}, bf16[4,96,352]{2,1,0:T(8,128)(2,1)}, u32[]{:S(2)}, u32[]{:S(2)}) collective-permute-start(bf16[4,96,352]{2,1,0:T(8,128)(2,1)} %all_to_all.25), channel_id=1, source_target_pairs={{0,32},{32,64},{64,96},{96,128},{128,160},{160,192},{192,224},{224... | collective-permute-start | bytes 811016 | tf_op jit(solution)/shard_map/ppermute | solution.py:19
  77.0 1.0 copy-start.2
  78.0 1.0 copy-start.3
  103.5 31.1 %collective-permute-start.5 = (bf16[2,64,4096]{2,1,0:T(8,128)(2,1)}, bf16[2,64,4096]{2,1,0:T(8,128)(2,1)}, u32[]{:S(2)}, u32[]{:S(2)}) collective-permute-start(bf16[2,64,4096]{2,1,0:T(8,128)(2,1)} %get-tuple-element.13.keep), channel_id=1, source_target_pairs={{0,1},{1,0},{2,3},{3,2},{4,5},{5,4},{6,7},{7,6},{8,9},{9,8},{10,11... | collective-permute-start | bytes 3145736 | tf_op jit(solution)/shard_map/ppermute | solution.py:19
  108.2 19.4 %all-to-all-start.3 = ((bf16[4,4,32,352]{3,2,1,0:T(8,128)(2,1)}), bf16[4,4,32,352]{3,2,1,0:T(8,128)(2,1)S(1)}, u32[]{:S(2)}, u32[]{:S(2)}) async-start(bf16[4,4,32,352]{3,2,1,0:T(8,128)(2,1)} %get-tuple-element.22), calls=%async_computation.3 | async-start | bytes 786432 | tf_op jit(solution)/shard_map/all_to_all | solution.py:179
  113.6 10.8 %collective-permute-start.10 = (bf16[128,512]{1,0:T(8,128)(2,1)S(1)}, bf16[128,512]{1,0:T(8,128)(2,1)S(1)}, u32[]{:S(2)}, u32[]{:S(2)}) collective-permute-start(bf16[128,512]{1,0:T(8,128)(2,1)S(1)} %get-tuple-element.19), channel_id=1, source_target_pairs={{0,8},{8,16},{16,24},{24,0},{1,9},{9,17},{17,25},{25,1},{2,10},{10... | collective-permute-start | bytes 393224 | tf_op jit(solution)/shard_map/ppermute | solution.py:19
  117.0 9.1 %collective-permute-start.11 = (bf16[128,512]{1,0:T(8,128)(2,1)S(1)}, bf16[128,512]{1,0:T(8,128)(2,1)S(1)}, u32[]{:S(2)}, u32[]{:S(2)}) collective-permute-start(bf16[128,512]{1,0:T(8,128)(2,1)S(1)} %get-tuple-element.20), channel_id=1, source_target_pairs={{0,16},{8,24},{16,0},{24,8},{1,17},{9,25},{17,1},{25,9},{2,18},{10... | collective-permute-start | bytes 393224 | tf_op jit(solution)/shard_map/ppermute | solution.py:19
  121.3 5.7 %collective-permute-start.12 = (bf16[128,512]{1,0:T(8,128)(2,1)S(1)}, bf16[128,512]{1,0:T(8,128)(2,1)S(1)}, u32[]{:S(2)}, u32[]{:S(2)}) collective-permute-start(bf16[128,512]{1,0:T(8,128)(2,1)S(1)} %get-tuple-element.21), channel_id=1, source_target_pairs={{0,24},{8,0},{16,8},{24,16},{1,25},{9,1},{17,9},{25,17},{2,26},{10... | collective-permute-start | bytes 393224 | tf_op jit(solution)/shard_map/ppermute | solution.py:19
  127.6 7.0 %copy-start.1 = (bf16[2,64,4096]{2,1,0:T(8,128)(2,1)S(1)}, bf16[2,64,4096]{2,1,0:T(8,128)(2,1)}, u32[]{:S(2)}) copy-start(bf16[2,64,4096]{2,1,0:T(8,128)(2,1)} %get-tuple-element.13.keep) | copy-start | bytes 3145732
  129.5 40.1 %all-to-all-start.4 = ((bf16[16,32,352]{2,1,0:T(8,128)(2,1)}), bf16[16,32,352]{2,1,0:T(8,128)(2,1)S(1)}, u32[]{:S(2)}, u32[]{:S(2)}) async-start(bf16[16,32,352]{2,1,0:T(8,128)(2,1)} %shard_map.109), calls=%async_computation.4 | async-start | bytes 786432 | tf_op jit(solution)/shard_map/all_to_all | solution.py:179
  136.0 33.7 %copy-start.5 = (f32[32,352]{1,0:T(8,128)S(1)}, f32[32,352]{1,0:T(8,128)}, u32[]{:S(2)}) copy-start(f32[32,352]{1,0:T(8,128)} %param.15) | copy-start | bytes 135172
  136.0 10.7 %collective-permute-start.6 = (bf16[16,4096]{1,0:T(8,128)(2,1)S(1)}, bf16[16,4096]{1,0:T(8,128)(2,1)S(1)}, u32[]{:S(2)}, u32[]{:S(2)}) collective-permute-start(bf16[16,4096]{1,0:T(8,128)(2,1)S(1)} %get-tuple-element.15), channel_id=1, source_target_pairs={{0,2},{2,4},{4,6},{6,0},{1,3},{3,5},{5,7},{7,1},{8,10},{10,12},{12... | collective-permute-start | bytes 393224 | tf_op jit(solution)/shard_map/ppermute | solution.py:19
  139.3 8.3 %collective-permute-start.7 = (bf16[16,4096]{1,0:T(8,128)(2,1)S(1)}, bf16[16,4096]{1,0:T(8,128)(2,1)S(1)}, u32[]{:S(2)}, u32[]{:S(2)}) collective-permute-start(bf16[16,4096]{1,0:T(8,128)(2,1)S(1)} %get-tuple-element.16), channel_id=1, source_target_pairs={{0,4},{2,6},{4,0},{6,2},{1,5},{3,7},{5,1},{7,3},{8,12},{10,14},{12... | collective-permute-start | bytes 393224 | tf_op jit(solution)/shard_map/ppermute | solution.py:19
  143.6 6.9 %collective-permute-start.8 = (bf16[16,4096]{1,0:T(8,128)(2,1)S(1)}, bf16[16,4096]{1,0:T(8,128)(2,1)S(1)}, u32[]{:S(2)}, u32[]{:S(2)}) collective-permute-start(bf16[16,4096]{1,0:T(8,128)(2,1)S(1)} %get-tuple-element.17), channel_id=1, source_target_pairs={{0,6},{2,0},{4,2},{6,4},{1,7},{3,1},{5,3},{7,5},{8,14},{10,8},{12,... | collective-permute-start | bytes 393224 | tf_op jit(solution)/shard_map/ppermute | solution.py:19
  161.9 9.2 %collective-permute-start.9 = (bf16[64,4096]{1,0:T(8,128)(2,1)S(1)}, bf16[64,4096]{1,0:T(8,128)(2,1)S(1)}, u32[]{:S(2)}, u32[]{:S(2)}) collective-permute-start(bf16[64,4096]{1,0:T(8,128)(2,1)S(1)} %all_gather.3), channel_id=1, source_target_pairs={{0,1},{1,0},{2,3},{3,2},{4,5},{5,4},{6,7},{7,6},{8,9},{9,8},{10,11... | collective-permute-start | bytes 1572872 | tf_op jit(solution)/shard_map/ppermute | solution.py:19

commit v6 on v5

--- a/solution.py
+++ b/solution.py
@@ -77,7 +77,10 @@
 
 
 def products(at, tok, *refs):
-    pieces, (gds, both, wg, wu, wd, own, parts, sems, outs) = refs[:6], refs[6:]
+    pieces, (gds, keep, give, wg, wu, wd, own, parts, sems, outs) = (
+        refs[:6],
+        refs[6:],
+    )
     assemble(at, pieces, (wg, wu, wd), sems)
     ready = [False] * 3
     stores = []
@@ -95,9 +98,9 @@
         stores.append(copy)
 
     def store_parts(columns):
-        for k, half in enumerate((at[2], 1 - at[2])):
+        for half, out in ((at[2], keep), (1 - at[2], give)):
             rows = pl.ds(pl.multiple_of(half * 64, 64), 64)
-            store(parts.at[rows, columns], both.at[k, :, columns])
+            store(parts.at[rows, columns], out.at[:, columns])
 
     gate = dot(tok[0], weight(0), 1, 0)
     up = dot(tok[0], weight(1), 1, 0)
@@ -136,7 +139,7 @@
 def pair(at, keep, other, *outs):
     for k, out in enumerate(outs):
         rows = pl.ds(pl.multiple_of((at[3] + k) % 4 * 16, 16), 16)
-        out[...] = (keep[0, rows, :].astype(F32) + other[1, rows, :].astype(F32)).astype(BF)
+        out[...] = (keep[rows, :].astype(F32) + other[rows, :].astype(F32)).astype(BF)
 
 
 def finish(at, p0, p1, p2, p3, bt, gain, out):
@@ -201,9 +204,9 @@
     b2 = shift(b2, "y", 2)
     b3 = shift(b3, "y", 3)
     (cols,) = call(merge, ((4, *COL),), (), at, b0, b1, b2, b3)
-    gds, both = call(
+    gds, keep, give = call(
         products,
-        ((4, 4, 32, 352), (2, 64, 4096)),
+        ((4, 4, 32, 352), (64, 4096), (64, 4096)),
         (W, W, W, (4, 32, 352), (128, 4096), DMA((3,)), DMA((8,))),
         at, tok, *pieces,
         ins=[VM] + [ANY] * 6,
@@ -212,8 +215,8 @@
     gds = exchange(gds, "y")
     (grads,) = call(outer, ((16, 32, 352),), (), at, cols, gds)
     gz = exchange(grads, Z)
-    other = shift(both, "c", 1)
-    p0, p1, p2, p3 = call(pair, ((16, 4096),) * 4, (), at, both, other)
+    other = shift(give, "c", 1)
+    p0, p1, p2, p3 = call(pair, ((16, 4096),) * 4, (), at, keep, other)
     p1 = shift(p1, "x", 1)
     p2 = shift(p2, "x", 2)
     p3 = shift(p3, "x", -1)

time: 173 us -> 196 us (1.13)
  the two profiles are of different devices: /device:TPU:1 before, /device:TPU:8 now
where the time goes in v6:
time: 196 us; the launch traced here: 194 us
  starting transfers between devices  67.6 us (34%)
  waiting for transfers between devices  55.8 us (28%)
  blocking collectives  47.4 us (24%)
  Pallas kernels  12.4 us (6%)
  local copies, waits for them, and re-layouts  6.41 us (3%)
  other arithmetic  4 us (2%)
    ppermute x12, starting transfers between devices, shift(): return lax.ppermute(array, axis, [(k, (k + by) % n) for k in range(n)])  42.3 us
    all_to_all x1, blocking collectives, copies_to_all(): return lax.all_to_all(copies, axis, split_axis=0, concat_axis=0, tiled=True)  34.3 us
    ppermute x12, waiting for transfers between devices, shift(): return lax.ppermute(array, axis, [(k, (k + by) % n) for k in range(n)])  25.7 us
    all_to_all x2, waiting for transfers between devices, exchange(): return lax.all_to_all(array, axis, split_axis=0, concat_axis=0, tiled=True)  22.8 us
    all_gather x1, blocking collectives, shards(): half = lax.all_gather(done, 'x', axis=0, tiled=True)  13.1 us
    pallas_call x7, Pallas kernels, call(): pl.pallas_call(body, out_shape=tuple((shape(o) for o in outs)), in_specs=...  12.4 us
    all_to_all x2, starting transfers between devices, exchange(): return lax.all_to_all(array, axis, split_axis=0, concat_axis=0, tiled=True)  10.2 us
    all_to_all x2, starting transfers between devices, copies_to_all(): return lax.all_to_all(copies, axis, split_axis=0, concat_axis=0, tiled=True)  9.71 us
  transfers between devices with their start and end apart: 17, of which 9 were waited for; matrix products, arithmetic and copies ran while one was open for 1% of the time, Pallas kernels for 2%

profile of v6, /device:TPU:8, one launch (start us, length us, event | category | flops | bytes accessed | tf_op | source)
XLA Modules:
  0.0 194.5 jit_solution(9798426393122786737)
XLA Ops:
  0.6 0.8 pad_maximum_fusion.1
  1.5 34.3 %all_to_all.25 = bf16[4,96,352]{2,1,0:T(8,128)(2,1)} all-to-all(bf16[4,96,352]{2,1,0:T(8,128)(2,1)S(1)} %broadcast_in_dim.9), channel_id=1, replica_groups=mesh['za'=4,'zb'=4,'y'=4,'x'=4,'c'=2] {'za'}, dimensions={0} | all-to-all | bytes 540672 | tf_op jit(solution)/shard_map/all_to_all | solution.py:24
  35.8 2.1 %broadcast_in_dim.10 = bf16[4,4,96,352]{3,2,1,0:T(8,128)(2,1)} broadcast(bf16[4,96,352]{2,1,0:T(8,128)(2,1)} %all_to_all.25), dimensions={1,2,3} | broadcast | bytes 1351680 | tf_op jit(solution)/shard_map/broadcast_in_dim | solution.py:23
  37.9 4.9 %all-to-all-start.1 = ((bf16[4,4,96,352]{3,2,1,0:T(8,128)(2,1)}), bf16[4,4,96,352]{3,2,1,0:T(8,128)(2,1)S(1)}, u32[]{:S(2)}, u32[]{:S(2)}) async-start(bf16[4,4,96,352]{3,2,1,0:T(8,128)(2,1)} %broadcast_in_dim.10), calls=%async_computation.1 | async-start | bytes 2359296 | tf_op jit(solution)/shard_map/all_to_all | solution.py:24
  42.8 5.4 %collective-permute-start.2 = (bf16[4,96,352]{2,1,0:T(8,128)(2,1)}, bf16[4,96,352]{2,1,0:T(8,128)(2,1)S(1)}, u32[]{:S(2)}, u32[]{:S(2)}) collective-permute-start(bf16[4,96,352]{2,1,0:T(8,128)(2,1)} %all_to_all.25), channel_id=1, source_target_pairs={{0,448},{32,96},{64,0},{96,160},{128,64},{160,224},{192,128},{224,... | collective-permute-start | bytes 811016 | tf_op jit(solution)/shard_map/ppermute | solution.py:195
  48.3 7.3 %collective-permute-done.2 = bf16[4,96,352]{2,1,0:T(8,128)(2,1)S(1)} collective-permute-done((bf16[4,96,352]{2,1,0:T(8,128)(2,1)}, bf16[4,96,352]{2,1,0:T(8,128)(2,1)S(1)}, u32[]{:S(2)}, u32[]{:S(2)}) %collective-permute-start.2) | collective-permute-done | bytes 270368 | tf_op jit(solution)/shard_map/ppermute | solution.py:195
  55.5 0.0 all-to-all-done.1.refs_0_
  55.5 1.1 broadcast_in_dim.11
  56.7 4.8 %all-to-all-start.2 = ((bf16[4,4,96,352]{3,2,1,0:T(8,128)(2,1)}), bf16[4,4,96,352]{3,2,1,0:T(8,128)(2,1)}, u32[]{:S(2)}, u32[]{:S(2)}) async-start(bf16[4,4,96,352]{3,2,1,0:T(8,128)(2,1)} %broadcast_in_dim.11), calls=%async_computation.2 | async-start | bytes 2359296 | tf_op jit(solution)/shard_map/all_to_all | solution.py:24
  61.5 0.0 copy-start
  61.5 0.0 copy-start.4
  61.5 1.3 fusion
  62.8 6.2 %collective-permute-start.3 = (bf16[3,4,96,352]{3,2,1,0:T(8,128)(2,1)}, bf16[3,4,96,352]{3,2,1,0:T(8,128)(2,1)}, u32[]{:S(2)}, u32[]{:S(2)}) collective-permute-start(bf16[3,4,96,352]{3,2,1,0:T(8,128)(2,1)} %fusion), channel_id=1, source_target_pairs={{0,480},{32,0},{64,32},{96,64},{128,96},{160,128},{192,160},{224,1... | collective-permute-start | bytes 2433032 | tf_op jit(solution)/shard_map/ppermute | solution.py:19
  69.0 4.6 %collective-permute-start.4 = (bf16[3,4,96,352]{3,2,1,0:T(8,128)(2,1)}, bf16[3,4,96,352]{3,2,1,0:T(8,128)(2,1)}, u32[]{:S(2)}, u32[]{:S(2)}) collective-permute-start(bf16[3,4,96,352]{3,2,1,0:T(8,128)(2,1)} %fusion), channel_id=1, source_target_pairs={{0,32},{32,64},{64,96},{96,128},{128,160},{160,192},{192,224},{224... | collective-permute-start | bytes 2433032 | tf_op jit(solution)/shard_map/ppermute | solution.py:19
  73.6 2.5 %collective-permute-start = (bf16[4,96,352]{2,1,0:T(8,128)(2,1)}, bf16[4,96,352]{2,1,0:T(8,128)(2,1)}, u32[]{:S(2)}, u32[]{:S(2)}) collective-permute-start(bf16[4,96,352]{2,1,0:T(8,128)(2,1)} %all_to_all.25), channel_id=1, source_target_pairs={{0,480},{32,0},{64,32},{96,64},{128,96},{160,128},{192,160},{224,1... | collective-permute-start | bytes 811016 | tf_op jit(solution)/shard_map/ppermute | solution.py:19
  76.1 3.4 %collective-permute-start.1 = (bf16[4,96,352]{2,1,0:T(8,128)(2,1)}, bf16[4,96,352]{2,1,0:T(8,128)(2,1)}, u32[]{:S(2)}, u32[]{:S(2)}) collective-permute-start(bf16[4,96,352]{2,1,0:T(8,128)(2,1)} %all_to_all.25), channel_id=1, source_target_pairs={{0,32},{32,64},{64,96},{96,128},{128,160},{160,192},{192,224},{224... | collective-permute-start | bytes 811016 | tf_op jit(solution)/shard_map/ppermute | solution.py:19
  79.5 0.1 pad_add_fusion.at
  79.5 0.0 copy-done
  79.5 0.0 copy-done.4
  79.5 0.0 copy-start.2
  79.5 1.0 copy-done.2
  80.6 0.0 copy-start.3
  80.6 1.0 copy-done.3
  81.6 1.0 shard_map.103.tok
  82.6 12.9 %collective-permute-done.refs_1_ = bf16[4,96,352]{2,1,0:T(8,128)(2,1)} collective-permute-done((bf16[4,96,352]{2,1,0:T(8,128)(2,1)}, bf16[4,96,352]{2,1,0:T(8,128)(2,1)}, u32[]{:S(2)}, u32[]{:S(2)}) %collective-permute-start) | collective-permute-done | bytes 270368 | tf_op jit(solution)/shard_map/ppermute | solution.py:19
  95.5 3.1 %collective-permute-done.1.refs_2_ = bf16[4,96,352]{2,1,0:T(8,128)(2,1)} collective-permute-done((bf16[4,96,352]{2,1,0:T(8,128)(2,1)}, bf16[4,96,352]{2,1,0:T(8,128)(2,1)}, u32[]{:S(2)}, u32[]{:S(2)}) %collective-permute-start.1) | collective-permute-done | bytes 270368 | tf_op jit(solution)/shard_map/ppermute | solution.py:19
  98.5 0.0 all-to-all-done.2.refs_3_
  98.5 0.0 collective-permute-done.3.refs_4_
  98.5 0.0 collective-permute-done.4.refs_5_
  98.5 6.3 %shard_map.104 = (bf16[4,4,32,352]{3,2,1,0:T(8,128)(2,1)}, bf16[64,4096]{1,0:T(8,128)(2,1)}, bf16[64,4096]{1,0:T(8,128)(2,1)}) custom-call(s32[4]{0:T(128)S(1)} %pad_add_fusion.at, bf16[3,128,2048]{2,1,0:T(8,128)(2,1)S(1)} %shard_map.103.tok, bf16[4,4,96,352]{3,2,1,0:T(8,128)(2,1)S(1)} %all-to-all-done.1.refs_0_, ...), custom_call_target="tpu_custom_call" | custom-call | tf_op jit(solution)/shard_map/pallas_call | solution.py:165
  104.9 1.9 collective-permute-start.5
  106.8 2.1 %collective-permute-done.5.other = bf16[64,4096]{1,0:T(8,128)(2,1)S(1)} collective-permute-done((bf16[64,4096]{1,0:T(8,128)(2,1)}, bf16[64,4096]{1,0:T(8,128)(2,1)S(1)}, u32[]{:S(2)}, u32[]{:S(2)}) %collective-permute-start.5) | collective-permute-done | bytes 524320 | tf_op jit(solution)/shard_map/ppermute | solution.py:19
  108.9 0.0 copy-start.1
  108.9 1.0 copy-done.1
  109.9 0.7 shard_map.105
  110.6 3.4 %collective-permute-start.6 = (bf16[16,4096]{1,0:T(8,128)(2,1)S(1)}, bf16[16,4096]{1,0:T(8,128)(2,1)S(1)}, u32[]{:S(2)}, u32[]{:S(2)}) collective-permute-start(bf16[16,4096]{1,0:T(8,128)(2,1)S(1)} %get-tuple-element.17), channel_id=1, source_target_pairs={{0,2},{2,4},{4,6},{6,0},{1,3},{3,5},{5,7},{7,1},{8,10},{10,12},{12... | collective-permute-start | bytes 393224 | tf_op jit(solution)/shard_map/ppermute | solution.py:19
  114.0 4.6 %collective-permute-start.7 = (bf16[16,4096]{1,0:T(8,128)(2,1)S(1)}, bf16[16,4096]{1,0:T(8,128)(2,1)S(1)}, u32[]{:S(2)}, u32[]{:S(2)}) collective-permute-start(bf16[16,4096]{1,0:T(8,128)(2,1)S(1)} %get-tuple-element.18), channel_id=1, source_target_pairs={{0,4},{2,6},{4,0},{6,2},{1,5},{3,7},{5,1},{7,3},{8,12},{10,14},{12... | collective-permute-start | bytes 393224 | tf_op jit(solution)/shard_map/ppermute | solution.py:19
  118.7 3.4 %collective-permute-start.8 = (bf16[16,4096]{1,0:T(8,128)(2,1)S(1)}, bf16[16,4096]{1,0:T(8,128)(2,1)S(1)}, u32[]{:S(2)}, u32[]{:S(2)}) collective-permute-start(bf16[16,4096]{1,0:T(8,128)(2,1)S(1)} %get-tuple-element.19), channel_id=1, source_target_pairs={{0,6},{2,0},{4,2},{6,4},{1,7},{3,1},{5,3},{7,5},{8,14},{10,8},{12,... | collective-permute-start | bytes 393224 | tf_op jit(solution)/shard_map/ppermute | solution.py:19
  122.0 0.0 collective-permute-done.6.p1
  122.0 1.0 collective-permute-done.7.p2
  123.1 2.5 %collective-permute-done.8.p3 = bf16[16,4096]{1,0:T(8,128)(2,1)S(1)} collective-permute-done((bf16[16,4096]{1,0:T(8,128)(2,1)S(1)}, bf16[16,4096]{1,0:T(8,128)(2,1)S(1)}, u32[]{:S(2)}, u32[]{:S(2)}) %collective-permute-start.8) | collective-permute-done | bytes 131104 | tf_op jit(solution)/shard_map/ppermute | solution.py:19
  125.5 0.7 shard_map.106
  126.2 13.1 %all_gather.3 = bf16[64,4096]{1,0:T(8,128)(2,1)S(1)} all-gather(bf16[16,4096]{1,0:T(8,128)(2,1)S(1)} %shard_map.106), channel_id=1, replica_groups=mesh['za'=4,'zb'=4,'y'=4,'x'=4,'c'=2] {'x'}, dimensions={0}, use_global_device_ids=true | all-gather | bytes 655360 | tf_op jit(solution)/shard_map/all_gather | solution.py:224
  139.3 1.9 collective-permute-start.9
  141.3 4.8 %all-to-all-start.3 = ((bf16[4,4,32,352]{3,2,1,0:T(8,128)(2,1)}), bf16[4,4,32,352]{3,2,1,0:T(8,128)(2,1)S(1)}, u32[]{:S(2)}, u32[]{:S(2)}) async-start(bf16[4,4,32,352]{3,2,1,0:T(8,128)(2,1)} %get-tuple-element.24), calls=%async_computation.3 | async-start | bytes 786432 | tf_op jit(solution)/shard_map/all_to_all | solution.py:182
  146.1 1.2 shard_map.107
  147.3 3.4 %collective-permute-start.10 = (bf16[128,512]{1,0:T(8,128)(2,1)S(1)}, bf16[128,512]{1,0:T(8,128)(2,1)S(1)}, u32[]{:S(2)}, u32[]{:S(2)}) collective-permute-start(bf16[128,512]{1,0:T(8,128)(2,1)S(1)} %get-tuple-element.21), channel_id=1, source_target_pairs={{0,8},{8,16},{16,24},{24,0},{1,9},{9,17},{17,25},{25,1},{2,10},{10... | collective-permute-start | bytes 393224 | tf_op jit(solution)/shard_map/ppermute | solution.py:19
  150.7 2.5 %collective-permute-start.11 = (bf16[128,512]{1,0:T(8,128)(2,1)S(1)}, bf16[128,512]{1,0:T(8,128)(2,1)S(1)}, u32[]{:S(2)}, u32[]{:S(2)}) collective-permute-start(bf16[128,512]{1,0:T(8,128)(2,1)S(1)} %get-tuple-element.22), channel_id=1, source_target_pairs={{0,16},{8,24},{16,0},{24,8},{1,17},{9,25},{17,1},{25,9},{2,18},{10... | collective-permute-start | bytes 393224 | tf_op jit(solution)/shard_map/ppermute | solution.py:19
  153.2 4.5 %collective-permute-start.12 = (bf16[128,512]{1,0:T(8,128)(2,1)S(1)}, bf16[128,512]{1,0:T(8,128)(2,1)S(1)}, u32[]{:S(2)}, u32[]{:S(2)}) collective-permute-start(bf16[128,512]{1,0:T(8,128)(2,1)S(1)} %get-tuple-element.23), channel_id=1, source_target_pairs={{0,24},{8,0},{16,8},{24,16},{1,25},{9,1},{17,9},{25,17},{2,26},{10... | collective-permute-start | bytes 393224 | tf_op jit(solution)/shard_map/ppermute | solution.py:19
  157.8 0.0 collective-permute-done.10.b1
  157.8 2.3 %collective-permute-done.11.b2 = bf16[128,512]{1,0:T(8,128)(2,1)S(1)} collective-permute-done((bf16[128,512]{1,0:T(8,128)(2,1)S(1)}, bf16[128,512]{1,0:T(8,128)(2,1)S(1)}, u32[]{:S(2)}, u32[]{:S(2)}) %collective-permute-start.11) | collective-permute-done | bytes 131104 | tf_op jit(solution)/shard_map/ppermute | solution.py:19
  160.0 1.9 collective-permute-done.12.b3
  162.0 0.6 shard_map.108.cols
  162.6 0.0 all-to-all-done.3.gds
  162.6 1.9 shard_map.109
  164.5 5.3 %all-to-all-start.4 = ((bf16[16,32,352]{2,1,0:T(8,128)(2,1)}), bf16[16,32,352]{2,1,0:T(8,128)(2,1)S(1)}, u32[]{:S(2)}, u32[]{:S(2)}) async-start(bf16[16,32,352]{2,1,0:T(8,128)(2,1)} %shard_map.109), calls=%async_computation.4 | async-start | bytes 786432 | tf_op jit(solution)/shard_map/all_to_all | solution.py:182
  169.8 0.0 collective-permute-done.9
  169.8 0.1 broadcast_select_fusion
  169.9 0.0 copy-start.5
  169.9 1.0 pad_maximum_fusion
  171.0 22.8 %all-to-all-done.4 = bf16[16,32,352]{2,1,0:T(8,128)(2,1)S(1)} async-done(((bf16[16,32,352]{2,1,0:T(8,128)(2,1)}), bf16[16,32,352]{2,1,0:T(8,128)(2,1)S(1)}, u32[]{:S(2)}, u32[]{:S(2)}) %all-to-all-start.4) | async-done | bytes 360480 | tf_op jit(solution)/shard_map/all_to_all | solution.py:182
  193.8 0.1 convert_reduce_fusion
  193.8 0.0 copy-done.5
  193.8 0.6 add.13
  (1 shorter events, 0.0 us)
Async XLA Ops:
  37.9 17.6 %all-to-all-start.1 = ((bf16[4,4,96,352]{3,2,1,0:T(8,128)(2,1)}), bf16[4,4,96,352]{3,2,1,0:T(8,128)(2,1)S(1)}, u32[]{:S(2)}, u32[]{:S(2)}) async-start(bf16[4,4,96,352]{3,2,1,0:T(8,128)(2,1)} %broadcast_in_dim.10), calls=%async_computation.1 | async-start | bytes 2359296 | tf_op jit(solution)/shard_map/all_to_all | solution.py:24
  42.8 12.7 %collective-permute-start.2 = (bf16[4,96,352]{2,1,0:T(8,128)(2,1)}, bf16[4,96,352]{2,1,0:T(8,128)(2,1)S(1)}, u32[]{:S(2)}, u32[]{:S(2)}) collective-permute-start(bf16[4,96,352]{2,1,0:T(8,128)(2,1)} %all_to_all.25), channel_id=1, source_target_pairs={{0,448},{32,96},{64,0},{96,160},{128,64},{160,224},{192,128},{224,... | collective-permute-start | bytes 811016 | tf_op jit(solution)/shard_map/ppermute | solution.py:195
  56.7 41.9 %all-to-all-start.2 = ((bf16[4,4,96,352]{3,2,1,0:T(8,128)(2,1)}), bf16[4,4,96,352]{3,2,1,0:T(8,128)(2,1)}, u32[]{:S(2)}, u32[]{:S(2)}) async-start(bf16[4,4,96,352]{3,2,1,0:T(8,128)(2,1)} %broadcast_in_dim.11), calls=%async_computation.2 | async-start | bytes 2359296 | tf_op jit(solution)/shard_map/all_to_all | solution.py:24
  61.5 18.1 %copy-start = (bf16[128,2048]{1,0:T(8,128)(2,1)S(1)}, bf16[128,2048]{1,0:T(8,128)(2,1)}, u32[]{:S(2)}) copy-start(bf16[128,2048]{1,0:T(8,128)(2,1)} %bt.5) | copy-start | bytes 1572868
  61.5 18.1 %copy-start.4 = (f32[2048]{0:T(1024)S(1)}, f32[2048]{0:T(1024)}, u32[]{:S(2)}) copy-start(f32[2048]{0:T(1024)} %param.11) | copy-start | bytes 24580
  62.8 35.7 %collective-permute-start.3 = (bf16[3,4,96,352]{3,2,1,0:T(8,128)(2,1)}, bf16[3,4,96,352]{3,2,1,0:T(8,128)(2,1)}, u32[]{:S(2)}, u32[]{:S(2)}) collective-permute-start(bf16[3,4,96,352]{3,2,1,0:T(8,128)(2,1)} %fusion), channel_id=1, source_target_pairs={{0,480},{32,0},{64,32},{96,64},{128,96},{160,128},{192,160},{224,1... | collective-permute-start | bytes 2433032 | tf_op jit(solution)/shard_map/ppermute | solution.py:19
  69.0 29.6 %collective-permute-start.4 = (bf16[3,4,96,352]{3,2,1,0:T(8,128)(2,1)}, bf16[3,4,96,352]{3,2,1,0:T(8,128)(2,1)}, u32[]{:S(2)}, u32[]{:S(2)}) collective-permute-start(bf16[3,4,96,352]{3,2,1,0:T(8,128)(2,1)} %fusion), channel_id=1, source_target_pairs={{0,32},{32,64},{64,96},{96,128},{128,160},{160,192},{192,224},{224... | collective-permute-start | bytes 2433032 | tf_op jit(solution)/shard_map/ppermute | solution.py:19
  73.6 21.9 %collective-permute-start = (bf16[4,96,352]{2,1,0:T(8,128)(2,1)}, bf16[4,96,352]{2,1,0:T(8,128)(2,1)}, u32[]{:S(2)}, u32[]{:S(2)}) collective-permute-start(bf16[4,96,352]{2,1,0:T(8,128)(2,1)} %all_to_all.25), channel_id=1, source_target_pairs={{0,480},{32,0},{64,32},{96,64},{128,96},{160,128},{192,160},{224,1... | collective-permute-start | bytes 811016 | tf_op jit(solution)/shard_map/ppermute | solution.py:19
  76.1 22.5 %collective-permute-start.1 = (bf16[4,96,352]{2,1,0:T(8,128)(2,1)}, bf16[4,96,352]{2,1,0:T(8,128)(2,1)}, u32[]{:S(2)}, u32[]{:S(2)}) collective-permute-start(bf16[4,96,352]{2,1,0:T(8,128)(2,1)} %all_to_all.25), channel_id=1, source_target_pairs={{0,32},{32,64},{64,96},{96,128},{128,160},{160,192},{192,224},{224... | collective-permute-start | bytes 811016 | tf_op jit(solution)/shard_map/ppermute | solution.py:19
  79.5 1.0 copy-start.2
  80.6 1.0 copy-start.3
  104.9 4.0 %collective-permute-start.5 = (bf16[64,4096]{1,0:T(8,128)(2,1)}, bf16[64,4096]{1,0:T(8,128)(2,1)S(1)}, u32[]{:S(2)}, u32[]{:S(2)}) collective-permute-start(bf16[64,4096]{1,0:T(8,128)(2,1)} %get-tuple-element.15), channel_id=1, source_target_pairs={{0,1},{1,0},{2,3},{3,2},{4,5},{5,4},{6,7},{7,6},{8,9},{9,8},{10,11... | collective-permute-start | bytes 1572872 | tf_op jit(solution)/shard_map/ppermute | solution.py:19
  108.9 1.0 copy-start.1
  110.6 11.4 %collective-permute-start.6 = (bf16[16,4096]{1,0:T(8,128)(2,1)S(1)}, bf16[16,4096]{1,0:T(8,128)(2,1)S(1)}, u32[]{:S(2)}, u32[]{:S(2)}) collective-permute-start(bf16[16,4096]{1,0:T(8,128)(2,1)S(1)} %get-tuple-element.17), channel_id=1, source_target_pairs={{0,2},{2,4},{4,6},{6,0},{1,3},{3,5},{5,7},{7,1},{8,10},{10,12},{12... | collective-permute-start | bytes 393224 | tf_op jit(solution)/shard_map/ppermute | solution.py:19
  114.0 9.0 %collective-permute-start.7 = (bf16[16,4096]{1,0:T(8,128)(2,1)S(1)}, bf16[16,4096]{1,0:T(8,128)(2,1)S(1)}, u32[]{:S(2)}, u32[]{:S(2)}) collective-permute-start(bf16[16,4096]{1,0:T(8,128)(2,1)S(1)} %get-tuple-element.18), channel_id=1, source_target_pairs={{0,4},{2,6},{4,0},{6,2},{1,5},{3,7},{5,1},{7,3},{8,12},{10,14},{12... | collective-permute-start | bytes 393224 | tf_op jit(solution)/shard_map/ppermute | solution.py:19
  118.7 6.9 %collective-permute-start.8 = (bf16[16,4096]{1,0:T(8,128)(2,1)S(1)}, bf16[16,4096]{1,0:T(8,128)(2,1)S(1)}, u32[]{:S(2)}, u32[]{:S(2)}) collective-permute-start(bf16[16,4096]{1,0:T(8,128)(2,1)S(1)} %get-tuple-element.19), channel_id=1, source_target_pairs={{0,6},{2,0},{4,2},{6,4},{1,7},{3,1},{5,3},{7,5},{8,14},{10,8},{12,... | collective-permute-start | bytes 393224 | tf_op jit(solution)/shard_map/ppermute | solution.py:19
  139.3 30.5 %collective-permute-start.9 = (bf16[64,4096]{1,0:T(8,128)(2,1)S(1)}, bf16[64,4096]{1,0:T(8,128)(2,1)S(1)}, u32[]{:S(2)}, u32[]{:S(2)}) collective-permute-start(bf16[64,4096]{1,0:T(8,128)(2,1)S(1)} %all_gather.3), channel_id=1, source_target_pairs={{0,1},{1,0},{2,3},{3,2},{4,5},{5,4},{6,7},{7,6},{8,9},{9,8},{10,11... | collective-permute-start | bytes 1572872 | tf_op jit(solution)/shard_map/ppermute | solution.py:19
  141.3 21.3 %all-to-all-start.3 = ((bf16[4,4,32,352]{3,2,1,0:T(8,128)(2,1)}), bf16[4,4,32,352]{3,2,1,0:T(8,128)(2,1)S(1)}, u32[]{:S(2)}, u32[]{:S(2)}) async-start(bf16[4,4,32,352]{3,2,1,0:T(8,128)(2,1)} %get-tuple-element.24), calls=%async_computation.3 | async-start | bytes 786432 | tf_op jit(solution)/shard_map/all_to_all | solution.py:182
  147.3 10.5 %collective-permute-start.10 = (bf16[128,512]{1,0:T(8,128)(2,1)S(1)}, bf16[128,512]{1,0:T(8,128)(2,1)S(1)}, u32[]{:S(2)}, u32[]{:S(2)}) collective-permute-start(bf16[128,512]{1,0:T(8,128)(2,1)S(1)} %get-tuple-element.21), channel_id=1, source_target_pairs={{0,8},{8,16},{16,24},{24,0},{1,9},{9,17},{17,25},{25,1},{2,10},{10... | collective-permute-start | bytes 393224 | tf_op jit(solution)/shard_map/ppermute | solution.py:19
  150.7 9.3 %collective-permute-start.11 = (bf16[128,512]{1,0:T(8,128)(2,1)S(1)}, bf16[128,512]{1,0:T(8,128)(2,1)S(1)}, u32[]{:S(2)}, u32[]{:S(2)}) collective-permute-start(bf16[128,512]{1,0:T(8,128)(2,1)S(1)} %get-tuple-element.22), channel_id=1, source_target_pairs={{0,16},{8,24},{16,0},{24,8},{1,17},{9,25},{17,1},{25,9},{2,18},{10... | collective-permute-start | bytes 393224 | tf_op jit(solution)/shard_map/ppermute | solution.py:19
  153.2 8.7 %collective-permute-start.12 = (bf16[128,512]{1,0:T(8,128)(2,1)S(1)}, bf16[128,512]{1,0:T(8,128)(2,1)S(1)}, u32[]{:S(2)}, u32[]{:S(2)}) collective-permute-start(bf16[128,512]{1,0:T(8,128)(2,1)S(1)} %get-tuple-element.23), channel_id=1, source_target_pairs={{0,24},{8,0},{16,8},{24,16},{1,25},{9,1},{17,9},{25,17},{2,26},{10... | collective-permute-start | bytes 393224 | tf_op jit(solution)/shard_map/ppermute | solution.py:19
  164.5 29.3 %all-to-all-start.4 = ((bf16[16,32,352]{2,1,0:T(8,128)(2,1)}), bf16[16,32,352]{2,1,0:T(8,128)(2,1)S(1)}, u32[]{:S(2)}, u32[]{:S(2)}) async-start(bf16[16,32,352]{2,1,0:T(8,128)(2,1)} %shard_map.109), calls=%async_computation.4 | async-start | bytes 786432 | tf_op jit(solution)/shard_map/all_to_all | solution.py:182
  169.9 23.9 %copy-start.5 = (f32[32,352]{1,0:T(8,128)S(1)}, f32[32,352]{1,0:T(8,128)}, u32[]{:S(2)}) copy-start(f32[32,352]{1,0:T(8,128)} %param.15) | copy-start | bytes 135172

commit v7 on v6

--- a/solution.py
+++ b/solution.py
@@ -52,6 +52,22 @@
             ).start()
 
 
+def move(pairs, sems):
+    copies = [pltpu.make_async_copy(a, b, sems.at[k]) for k, (a, b) in enumerate(pairs)]
+    for copy in copies:
+        copy.start()
+    for copy in copies:
+        copy.wait()
+
+
+def spread(at, piece, out, sems):
+    move([(piece, out.at[k]) for k in range(4)], sems)
+
+
+def turn(at, near, out, sems):
+    move([(near.at[(at[1] + k) % 4], out.at[k - 1]) for k in range(1, 4)], sems)
+
+
 def columns(at, bt, gain, b0, b1, b2, b3, split):
     y = at[1]
     normed = normalize(bt[...], gain[...])
@@ -103,9 +119,12 @@
             store(parts.at[rows, columns], out.at[:, columns])
 
     gate = dot(tok[0], weight(0), 1, 0)
+    fwd_gate = dot(tok[2], weight(0), 1, 0)
     up = dot(tok[0], weight(1), 1, 0)
+    fwd_up = dot(tok[2], weight(1), 1, 0)
+    s = jax.nn.sigmoid(gate)
+    hidden = (fwd_gate * jax.nn.sigmoid(fwd_gate) * fwd_up).astype(BF)
     hid = 0.5 * dot(tok[1], weight(2), 1, 0)
-    s = jax.nn.sigmoid(gate)
     gd = (hid * up * s * (1.0 + gate * (1.0 - s))).astype(BF)
     ud = (hid * gate * s).astype(BF)
     own[...] = gd.reshape(4, 32, 352)
@@ -113,9 +132,6 @@
         store(own, gds.at[k])
     parts[:, 2048:4096] = (dot(gd, weight(0), 1, 1) + dot(ud, weight(1), 1, 1)).astype(BF)
     store_parts(pl.ds(2048, 2048))
-    gate = dot(tok[2], weight(0), 1, 0)
-    up = dot(tok[2], weight(1), 1, 0)
-    hidden = (gate * jax.nn.sigmoid(gate) * up).astype(BF)
     parts[:, 0:2048] = dot(hidden, weight(2), 1, 1).astype(BF)
     store_parts(pl.ds(0, 2048))
     for copy in stores:
@@ -174,6 +190,7 @@
 
 LIMIT = 24 * 1024 * 1024
 W = (4, 4, 4, 32, 352)
+SETS = (4, 4, 96, 352)
 TOK = (128, 2048)
 COL = (128, 512)
 
@@ -184,19 +201,21 @@
 
 def shards(ft, bt, og, gain, gw, uw, dw, gsum):
     spots = [lax.axis_index(n) for n in ("zb", "y", "c", "x")]
-    y, c = spots[1], spots[2]
+    c = spots[2]
     at = jnp.stack(spots).astype(jnp.int32)
     gain = gain.reshape(1, 2048)
     own = jnp.concatenate([gw, uw, dw], axis=0)
     a = copies_to_all(own, "za")
-    near = copies_to_all(a, "y")
+    (copies,) = call(spread, (SETS,), (DMA((4,)),), at, a, ins=[ANY], to=ANY)
+    near = exchange(copies, "y")
     a1 = shift(a, Z, -1)
     a3 = shift(a, Z, 1)
     a2 = lax.ppermute(a, Z, [(k, (k + (2 if k % 2 else -2)) % 16) for k in range(16)])
-    others = lax.dynamic_slice_in_dim(jnp.concatenate([near, near]), y + 1, 3)
+    (others,) = call(turn, ((3, 4, 96, 352),), (DMA((3,)),), at, near, ins=[ANY], to=ANY)
     z1 = shift(others, Z, -1)
     z3 = shift(others, Z, 1)
-    far = copies_to_all(a2, "y")
+    (copies,) = call(spread, (SETS,), (DMA((4,)),), at, a2, ins=[ANY], to=ANY)
+    far = exchange(copies, "y")
     pieces = (near, a1, a3, far, z1, z3)
     b0, b1, b2, b3 = call(columns, (COL,) * 4, ((4, *COL),), at, bt, gain)
     (tok,) = call(tokens, ((3, *TOK),), (), at, bt, ft, og, gain)

time: 196 us -> 233 us (1.19)
  Pallas kernels: 12.4 us -> 52.8 us
  blocking collectives: 47.4 us -> 13.1 us
  waiting for transfers between devices: 55.8 us -> 75.6 us
  starting transfers between devices: 67.6 us -> 81.3 us
    pallas_call x7 -> x10, Pallas kernels: 12.4 us -> 52.8 us  [call(): pl.pallas_call(body, out_shape=tuple((shape(o) for o in outs)), in_specs=...]
    all_to_all x1 -> x0, blocking collectives: 34.3 us -> none  [copies_to_all(): return lax.all_to_all(copies, axis, split_axis=0, concat_axis=0, tiled=True)]
    all_to_all x2 -> x1, waiting for transfers between devices: 0.01 us -> 19 us  [copies_to_all(): return lax.all_to_all(copies, axis, split_axis=0, concat_axis=0, tiled=True)]
    all_to_all x2 -> x4, starting transfers between devices: 10.2 us -> 19.8 us  [exchange(): return lax.all_to_all(array, axis, split_axis=0, concat_axis=0, tiled=True)]
    all_to_all x2 -> x1, starting transfers between devices: 9.71 us -> 15.1 us  [copies_to_all(): return lax.all_to_all(copies, axis, split_axis=0, concat_axis=0, tiled=True)]
    broadcast_in_dim x3 -> x1, local copies, waits for them, and re-layouts: 3.28 us -> 0.74 us  [copies_to_all(): copies = jnp.broadcast_to(array, (lax.axis_size(axis), *array.shape))]
    all_to_all x2 -> x4, waiting for transfers between devices: 22.8 us -> 22.8 us  [exchange(): return lax.all_to_all(array, axis, split_axis=0, concat_axis=0, tiled=True)]
  transfers between devices with their start and end apart: 17 -> 18, of which waited for: 9 -> 10; matrix products, arithmetic and copies ran while one was open for 1% -> 1% of each run, Pallas kernels for 2% -> 3%
where the time goes in v7:
time: 233 us; the launch traced here: 232 us
  starting transfers between devices  81.3 us (35%)
  waiting for transfers between devices  75.6 us (32%)
  Pallas kernels  52.8 us (23%)
  blocking collectives  13.1 us (6%)
  local copies, waits for them, and re-layouts  5.14 us (2%)
  other arithmetic  2.66 us (1%)
    pallas_call x10, Pallas kernels, call(): pl.pallas_call(body, out_shape=tuple((shape(o) for o in outs)), in_specs=...  52.8 us
    ppermute x12, starting transfers between devices, shift(): return lax.ppermute(array, axis, [(k, (k + by) % n) for k in range(n)])  40.6 us
    ppermute x12, waiting for transfers between devices, shift(): return lax.ppermute(array, axis, [(k, (k + by) % n) for k in range(n)])  27.1 us
    all_to_all x4, waiting for transfers between devices, exchange(): return lax.all_to_all(array, axis, split_axis=0, concat_axis=0, tiled=True)  22.8 us
    all_to_all x4, starting transfers between devices, exchange(): return lax.all_to_all(array, axis, split_axis=0, concat_axis=0, tiled=True)  19.8 us
    all_to_all x1, waiting for transfers between devices, copies_to_all(): return lax.all_to_all(copies, axis, split_axis=0, concat_axis=0, tiled=True)  19 us
    all_to_all x1, starting transfers between devices, copies_to_all(): return lax.all_to_all(copies, axis, split_axis=0, concat_axis=0, tiled=True)  15.1 us
    all_gather x1, blocking collectives, shards(): half = lax.all_gather(done, 'x', axis=0, tiled=True)  13.1 us
  transfers between devices with their start and end apart: 18, of which 10 were waited for; matrix products, arithmetic and copies ran while one was open for 1% of the time, Pallas kernels for 3%

profile of v7, /device:TPU:8, one launch (start us, length us, event | category | flops | bytes accessed | tf_op | source)
XLA Modules:
  0.0 231.6 jit_solution(13577610506541009924)
XLA Ops:
  0.6 0.8 pad_maximum_fusion.1
  1.4 0.7 broadcast_in_dim.3
  2.2 15.1 %all-to-all-start = ((bf16[4,96,352]{2,1,0:T(8,128)(2,1)}), bf16[4,96,352]{2,1,0:T(8,128)(2,1)}, u32[]{:S(2)}, u32[]{:S(2)}) async-start(bf16[4,96,352]{2,1,0:T(8,128)(2,1)} %broadcast_in_dim.3), calls=%async_computation | async-start | bytes 589824 | tf_op jit(solution)/shard_map/all_to_all | solution.py:24
  17.2 0.1 pad_add_fusion.at
  17.3 19.0 %all-to-all-done.piece = bf16[4,96,352]{2,1,0:T(8,128)(2,1)} async-done(((bf16[4,96,352]{2,1,0:T(8,128)(2,1)}), bf16[4,96,352]{2,1,0:T(8,128)(2,1)}, u32[]{:S(2)}, u32[]{:S(2)}) %all-to-all-start) | async-done | bytes 270368 | tf_op jit(solution)/shard_map/all_to_all | solution.py:24
  36.3 37.4 %shard_map.104 = bf16[4,4,96,352]{3,2,1,0:T(8,128)(2,1)} custom-call(s32[4]{0:T(128)S(1)} %pad_add_fusion.at, bf16[4,96,352]{2,1,0:T(8,128)(2,1)} %all-to-all-done.piece), custom_call_target="tpu_custom_call" | custom-call | tf_op jit(solution)/shard_map/pallas_call | solution.py:181
  73.7 4.9 %all-to-all-start.1 = ((bf16[4,4,96,352]{3,2,1,0:T(8,128)(2,1)}), bf16[4,4,96,352]{3,2,1,0:T(8,128)(2,1)S(1)}, u32[]{:S(2)}, u32[]{:S(2)}) async-start(bf16[4,4,96,352]{3,2,1,0:T(8,128)(2,1)} %shard_map.104), calls=%async_computation.1 | async-start | bytes 2359296 | tf_op jit(solution)/shard_map/all_to_all | solution.py:199
  78.6 5.9 %collective-permute-start.2 = (bf16[4,96,352]{2,1,0:T(8,128)(2,1)}, bf16[4,96,352]{2,1,0:T(8,128)(2,1)S(1)}, u32[]{:S(2)}, u32[]{:S(2)}) collective-permute-start(bf16[4,96,352]{2,1,0:T(8,128)(2,1)} %all-to-all-done.piece), channel_id=1, source_target_pairs={{0,448},{32,96},{64,0},{96,160},{128,64},{160,224},{192,128},{224,... | collective-permute-start | bytes 811016 | tf_op jit(solution)/shard_map/ppermute | solution.py:213
  84.5 6.7 %collective-permute-done.2.piece = bf16[4,96,352]{2,1,0:T(8,128)(2,1)S(1)} collective-permute-done((bf16[4,96,352]{2,1,0:T(8,128)(2,1)}, bf16[4,96,352]{2,1,0:T(8,128)(2,1)S(1)}, u32[]{:S(2)}, u32[]{:S(2)}) %collective-permute-start.2) | collective-permute-done | bytes 270368 | tf_op jit(solution)/shard_map/ppermute | solution.py:213
  91.2 1.6 shard_map.105
  92.8 0.0 all-to-all-done.1.near.refs_0_
  92.8 4.8 %all-to-all-start.2 = ((bf16[4,4,96,352]{3,2,1,0:T(8,128)(2,1)}), bf16[4,4,96,352]{3,2,1,0:T(8,128)(2,1)}, u32[]{:S(2)}, u32[]{:S(2)}) async-start(bf16[4,4,96,352]{3,2,1,0:T(8,128)(2,1)} %shard_map.105), calls=%async_computation.2 | async-start | bytes 2359296 | tf_op jit(solution)/shard_map/all_to_all | solution.py:199
  97.7 1.5 shard_map.106
  99.2 5.2 %collective-permute-start.3 = (bf16[3,4,96,352]{3,2,1,0:T(8,128)(2,1)}, bf16[3,4,96,352]{3,2,1,0:T(8,128)(2,1)}, u32[]{:S(2)}, u32[]{:S(2)}) collective-permute-start(bf16[3,4,96,352]{3,2,1,0:T(8,128)(2,1)} %shard_map.106), channel_id=1, source_target_pairs={{0,480},{32,0},{64,32},{96,64},{128,96},{160,128},{192,160},{224,1... | collective-permute-start | bytes 2433032 | tf_op jit(solution)/shard_map/ppermute | solution.py:19
  104.4 3.9 %collective-permute-start.4 = (bf16[3,4,96,352]{3,2,1,0:T(8,128)(2,1)}, bf16[3,4,96,352]{3,2,1,0:T(8,128)(2,1)}, u32[]{:S(2)}, u32[]{:S(2)}) collective-permute-start(bf16[3,4,96,352]{3,2,1,0:T(8,128)(2,1)} %shard_map.106), channel_id=1, source_target_pairs={{0,32},{32,64},{64,96},{96,128},{128,160},{160,192},{192,224},{224... | collective-permute-start | bytes 2433032 | tf_op jit(solution)/shard_map/ppermute | solution.py:19
  108.3 3.2 %collective-permute-start = (bf16[4,96,352]{2,1,0:T(8,128)(2,1)}, bf16[4,96,352]{2,1,0:T(8,128)(2,1)S(1)}, u32[]{:S(2)}, u32[]{:S(2)}) collective-permute-start(bf16[4,96,352]{2,1,0:T(8,128)(2,1)} %all-to-all-done.piece), channel_id=1, source_target_pairs={{0,480},{32,0},{64,32},{96,64},{128,96},{160,128},{192,160},{224,1... | collective-permute-start | bytes 811016 | tf_op jit(solution)/shard_map/ppermute | solution.py:19
  111.5 2.7 %collective-permute-start.1 = (bf16[4,96,352]{2,1,0:T(8,128)(2,1)}, bf16[4,96,352]{2,1,0:T(8,128)(2,1)S(1)}, u32[]{:S(2)}, u32[]{:S(2)}) collective-permute-start(bf16[4,96,352]{2,1,0:T(8,128)(2,1)} %all-to-all-done.piece), channel_id=1, source_target_pairs={{0,32},{32,64},{64,96},{96,128},{128,160},{160,192},{192,224},{224... | collective-permute-start | bytes 811016 | tf_op jit(solution)/shard_map/ppermute | solution.py:19
  114.2 0.0 copy-done
  114.2 0.0 copy-done.2
  114.2 0.0 copy-done.3
  114.2 1.0 shard_map.103.tok
  115.2 15.4 %collective-permute-done.refs_1_ = bf16[4,96,352]{2,1,0:T(8,128)(2,1)S(1)} collective-permute-done((bf16[4,96,352]{2,1,0:T(8,128)(2,1)}, bf16[4,96,352]{2,1,0:T(8,128)(2,1)S(1)}, u32[]{:S(2)}, u32[]{:S(2)}) %collective-permute-start) | collective-permute-done | bytes 270368 | tf_op jit(solution)/shard_map/ppermute | solution.py:19
  130.6 0.7 copy-done.4
  131.3 1.9 collective-permute-done.1.refs_2_
  133.1 0.7 copy-done.6
  133.9 0.0 all-to-all-done.2.refs_3_
  133.9 0.0 collective-permute-done.3.refs_4_
  133.9 0.0 collective-permute-done.4.refs_5_
  133.9 0.0 copy-start.5
  133.9 1.0 copy-done.5
  134.8 1.0 copy-done.7
  135.8 6.3 %shard_map.107 = (bf16[4,4,32,352]{3,2,1,0:T(8,128)(2,1)}, bf16[64,4096]{1,0:T(8,128)(2,1)}, bf16[64,4096]{1,0:T(8,128)(2,1)}) custom-call(s32[4]{0:T(128)S(1)} %pad_add_fusion.at, bf16[3,128,2048]{2,1,0:T(8,128)(2,1)S(1)} %shard_map.103.tok, bf16[4,4,96,352]{3,2,1,0:T(8,128)(2,1)S(1)} %all-to-all-done.1.near.refs_0_, bf16[4,96,352]{2,1,0:T(8,128)(2,1)S(1)} %copy-done.5, ...), custom_call_target="tpu_custom_call" | custom-call | tf_op jit(solution)/shard_map/pallas_call | solution.py:181
  142.1 1.9 collective-permute-start.5
  144.0 2.1 collective-permute-done.5.other
  146.1 1.0 copy-done.1
  147.1 0.7 shard_map.108
  147.8 3.4 %collective-permute-start.6 = (bf16[16,4096]{1,0:T(8,128)(2,1)S(1)}, bf16[16,4096]{1,0:T(8,128)(2,1)S(1)}, u32[]{:S(2)}, u32[]{:S(2)}) collective-permute-start(bf16[16,4096]{1,0:T(8,128)(2,1)S(1)} %get-tuple-element.17), channel_id=1, source_target_pairs={{0,2},{2,4},{4,6},{6,0},{1,3},{3,5},{5,7},{7,1},{8,10},{10,12},{12... | collective-permute-start | bytes 393224 | tf_op jit(solution)/shard_map/ppermute | solution.py:19
  151.2 4.7 %collective-permute-start.7 = (bf16[16,4096]{1,0:T(8,128)(2,1)S(1)}, bf16[16,4096]{1,0:T(8,128)(2,1)S(1)}, u32[]{:S(2)}, u32[]{:S(2)}) collective-permute-start(bf16[16,4096]{1,0:T(8,128)(2,1)S(1)} %get-tuple-element.18), channel_id=1, source_target_pairs={{0,4},{2,6},{4,0},{6,2},{1,5},{3,7},{5,1},{7,3},{8,12},{10,14},{12... | collective-permute-start | bytes 393224 | tf_op jit(solution)/shard_map/ppermute | solution.py:19
  155.9 3.3 %collective-permute-start.8 = (bf16[16,4096]{1,0:T(8,128)(2,1)S(1)}, bf16[16,4096]{1,0:T(8,128)(2,1)S(1)}, u32[]{:S(2)}, u32[]{:S(2)}) collective-permute-start(bf16[16,4096]{1,0:T(8,128)(2,1)S(1)} %get-tuple-element.19), channel_id=1, source_target_pairs={{0,6},{2,0},{4,2},{6,4},{1,7},{3,1},{5,3},{7,5},{8,14},{10,8},{12,... | collective-permute-start | bytes 393224 | tf_op jit(solution)/shard_map/ppermute | solution.py:19
  159.2 0.0 collective-permute-done.6.p1
  159.2 1.0 collective-permute-done.7.p2
  160.3 2.5 %collective-permute-done.8.p3 = bf16[16,4096]{1,0:T(8,128)(2,1)S(1)} collective-permute-done((bf16[16,4096]{1,0:T(8,128)(2,1)S(1)}, bf16[16,4096]{1,0:T(8,128)(2,1)S(1)}, u32[]{:S(2)}, u32[]{:S(2)}) %collective-permute-start.8) | collective-permute-done | bytes 131104 | tf_op jit(solution)/shard_map/ppermute | solution.py:19
  162.7 0.7 shard_map.109
  163.4 13.1 %all_gather.3 = bf16[64,4096]{1,0:T(8,128)(2,1)S(1)} all-gather(bf16[16,4096]{1,0:T(8,128)(2,1)S(1)} %shard_map.109), channel_id=1, replica_groups=mesh['za'=4,'zb'=4,'y'=4,'x'=4,'c'=2] {'x'}, dimensions={0}, use_global_device_ids=true | all-gather | bytes 655360 | tf_op jit(solution)/shard_map/all_gather | solution.py:243
  176.6 1.9 collective-permute-start.9
  178.5 4.8 %all-to-all-start.3 = ((bf16[4,4,32,352]{3,2,1,0:T(8,128)(2,1)}), bf16[4,4,32,352]{3,2,1,0:T(8,128)(2,1)S(1)}, u32[]{:S(2)}, u32[]{:S(2)}) async-start(bf16[4,4,32,352]{3,2,1,0:T(8,128)(2,1)} %get-tuple-element.24), calls=%async_computation.3 | async-start | bytes 786432 | tf_op jit(solution)/shard_map/all_to_all | solution.py:199
  183.3 1.2 shard_map.110
  184.5 3.4 %collective-permute-start.10 = (bf16[128,512]{1,0:T(8,128)(2,1)S(1)}, bf16[128,512]{1,0:T(8,128)(2,1)S(1)}, u32[]{:S(2)}, u32[]{:S(2)}) collective-permute-start(bf16[128,512]{1,0:T(8,128)(2,1)S(1)} %get-tuple-element.21), channel_id=1, source_target_pairs={{0,8},{8,16},{16,24},{24,0},{1,9},{9,17},{17,25},{25,1},{2,10},{10... | collective-permute-start | bytes 393224 | tf_op jit(solution)/shard_map/ppermute | solution.py:19
  187.9 2.5 %collective-permute-start.11 = (bf16[128,512]{1,0:T(8,128)(2,1)S(1)}, bf16[128,512]{1,0:T(8,128)(2,1)S(1)}, u32[]{:S(2)}, u32[]{:S(2)}) collective-permute-start(bf16[128,512]{1,0:T(8,128)(2,1)S(1)} %get-tuple-element.22), channel_id=1, source_target_pairs={{0,16},{8,24},{16,0},{24,8},{1,17},{9,25},{17,1},{25,9},{2,18},{10... | collective-permute-start | bytes 393224 | tf_op jit(solution)/shard_map/ppermute | solution.py:19
  190.5 4.5 %collective-permute-start.12 = (bf16[128,512]{1,0:T(8,128)(2,1)S(1)}, bf16[128,512]{1,0:T(8,128)(2,1)S(1)}, u32[]{:S(2)}, u32[]{:S(2)}) collective-permute-start(bf16[128,512]{1,0:T(8,128)(2,1)S(1)} %get-tuple-element.23), channel_id=1, source_target_pairs={{0,24},{8,0},{16,8},{24,16},{1,25},{9,1},{17,9},{25,17},{2,26},{10... | collective-permute-start | bytes 393224 | tf_op jit(solution)/shard_map/ppermute | solution.py:19
  195.0 0.0 collective-permute-done.10.b1
  195.0 2.3 collective-permute-done.11.b2
  197.3 1.9 collective-permute-done.12.b3
  199.2 0.6 shard_map.111.cols
  199.8 0.0 all-to-all-done.3.gds
  199.8 1.9 shard_map.112
  201.7 5.2 %all-to-all-start.4 = ((bf16[16,32,352]{2,1,0:T(8,128)(2,1)}), bf16[16,32,352]{2,1,0:T(8,128)(2,1)S(1)}, u32[]{:S(2)}, u32[]{:S(2)}) async-start(bf16[16,32,352]{2,1,0:T(8,128)(2,1)} %shard_map.112), calls=%async_computation.4 | async-start | bytes 786432 | tf_op jit(solution)/shard_map/all_to_all | solution.py:199
  206.9 0.0 collective-permute-done.9
  207.0 0.1 broadcast_select_fusion
  207.0 0.0 copy-start.9
  207.0 1.0 pad_maximum_fusion
  208.1 22.8 %all-to-all-done.4 = bf16[16,32,352]{2,1,0:T(8,128)(2,1)S(1)} async-done(((bf16[16,32,352]{2,1,0:T(8,128)(2,1)}), bf16[16,32,352]{2,1,0:T(8,128)(2,1)S(1)}, u32[]{:S(2)}, u32[]{:S(2)}) %all-to-all-start.4) | async-done | bytes 360480 | tf_op jit(solution)/shard_map/all_to_all | solution.py:199
  230.9 0.1 convert_reduce_fusion
  230.9 0.6 add.3
  (10 shorter events, 0.0 us)
Async XLA Ops:
  2.2 34.1 %all-to-all-start = ((bf16[4,96,352]{2,1,0:T(8,128)(2,1)}), bf16[4,96,352]{2,1,0:T(8,128)(2,1)}, u32[]{:S(2)}, u32[]{:S(2)}) async-start(bf16[4,96,352]{2,1,0:T(8,128)(2,1)} %broadcast_in_dim.3), calls=%async_computation | async-start | bytes 589824 | tf_op jit(solution)/shard_map/all_to_all | solution.py:24
  73.7 19.1 %all-to-all-start.1 = ((bf16[4,4,96,352]{3,2,1,0:T(8,128)(2,1)}), bf16[4,4,96,352]{3,2,1,0:T(8,128)(2,1)S(1)}, u32[]{:S(2)}, u32[]{:S(2)}) async-start(bf16[4,4,96,352]{3,2,1,0:T(8,128)(2,1)} %shard_map.104), calls=%async_computation.1 | async-start | bytes 2359296 | tf_op jit(solution)/shard_map/all_to_all | solution.py:199
  78.6 12.6 %collective-permute-start.2 = (bf16[4,96,352]{2,1,0:T(8,128)(2,1)}, bf16[4,96,352]{2,1,0:T(8,128)(2,1)S(1)}, u32[]{:S(2)}, u32[]{:S(2)}) collective-permute-start(bf16[4,96,352]{2,1,0:T(8,128)(2,1)} %all-to-all-done.piece), channel_id=1, source_target_pairs={{0,448},{32,96},{64,0},{96,160},{128,64},{160,224},{192,128},{224,... | collective-permute-start | bytes 811016 | tf_op jit(solution)/shard_map/ppermute | solution.py:213
  92.8 41.0 %all-to-all-start.2 = ((bf16[4,4,96,352]{3,2,1,0:T(8,128)(2,1)}), bf16[4,4,96,352]{3,2,1,0:T(8,128)(2,1)}, u32[]{:S(2)}, u32[]{:S(2)}) async-start(bf16[4,4,96,352]{3,2,1,0:T(8,128)(2,1)} %shard_map.105), calls=%async_computation.2 | async-start | bytes 2359296 | tf_op jit(solution)/shard_map/all_to_all | solution.py:199
  97.6 16.5 %copy-start = (bf16[128,2048]{1,0:T(8,128)(2,1)S(1)}, bf16[128,2048]{1,0:T(8,128)(2,1)}, u32[]{:S(2)}) copy-start(bf16[128,2048]{1,0:T(8,128)(2,1)} %bt.5) | copy-start | bytes 1572868
  97.7 16.5 %copy-start.2 = (bf16[128,2048]{1,0:T(8,128)(2,1)S(1)}, bf16[128,2048]{1,0:T(8,128)(2,1)}, u32[]{:S(2)}) copy-start(bf16[128,2048]{1,0:T(8,128)(2,1)} %ft.1) | copy-start | bytes 1572868
  97.7 16.5 %copy-start.3 = (bf16[128,2048]{1,0:T(8,128)(2,1)S(1)}, bf16[128,2048]{1,0:T(8,128)(2,1)}, u32[]{:S(2)}) copy-start(bf16[128,2048]{1,0:T(8,128)(2,1)} %og.1) | copy-start | bytes 1572868
  97.7 16.5 %copy-start.8 = (f32[2048]{0:T(1024)S(1)}, f32[2048]{0:T(1024)}, u32[]{:S(2)}) copy-start(f32[2048]{0:T(1024)} %param.11) | copy-start | bytes 24580
  99.2 34.7 %collective-permute-start.3 = (bf16[3,4,96,352]{3,2,1,0:T(8,128)(2,1)}, bf16[3,4,96,352]{3,2,1,0:T(8,128)(2,1)}, u32[]{:S(2)}, u32[]{:S(2)}) collective-permute-start(bf16[3,4,96,352]{3,2,1,0:T(8,128)(2,1)} %shard_map.106), channel_id=1, source_target_pairs={{0,480},{32,0},{64,32},{96,64},{128,96},{160,128},{192,160},{224,1... | collective-permute-start | bytes 2433032 | tf_op jit(solution)/shard_map/ppermute | solution.py:19
  104.4 29.4 %collective-permute-start.4 = (bf16[3,4,96,352]{3,2,1,0:T(8,128)(2,1)}, bf16[3,4,96,352]{3,2,1,0:T(8,128)(2,1)}, u32[]{:S(2)}, u32[]{:S(2)}) collective-permute-start(bf16[3,4,96,352]{3,2,1,0:T(8,128)(2,1)} %shard_map.106), channel_id=1, source_target_pairs={{0,32},{32,64},{64,96},{96,128},{128,160},{160,192},{192,224},{224... | collective-permute-start | bytes 2433032 | tf_op jit(solution)/shard_map/ppermute | solution.py:19
  108.3 22.3 %collective-permute-start = (bf16[4,96,352]{2,1,0:T(8,128)(2,1)}, bf16[4,96,352]{2,1,0:T(8,128)(2,1)S(1)}, u32[]{:S(2)}, u32[]{:S(2)}) collective-permute-start(bf16[4,96,352]{2,1,0:T(8,128)(2,1)} %all-to-all-done.piece), channel_id=1, source_target_pairs={{0,480},{32,0},{64,32},{96,64},{128,96},{160,128},{192,160},{224,1... | collective-permute-start | bytes 811016 | tf_op jit(solution)/shard_map/ppermute | solution.py:19
  111.5 21.6 %collective-permute-start.1 = (bf16[4,96,352]{2,1,0:T(8,128)(2,1)}, bf16[4,96,352]{2,1,0:T(8,128)(2,1)S(1)}, u32[]{:S(2)}, u32[]{:S(2)}) collective-permute-start(bf16[4,96,352]{2,1,0:T(8,128)(2,1)} %all-to-all-done.piece), channel_id=1, source_target_pairs={{0,32},{32,64},{64,96},{96,128},{128,160},{160,192},{192,224},{224... | collective-permute-start | bytes 811016 | tf_op jit(solution)/shard_map/ppermute | solution.py:19
  130.6 0.7 copy-start.4
  133.1 0.7 copy-start.6
  133.9 1.0 copy-start.5
  134.8 1.0 copy-start.7
  142.1 4.0 %collective-permute-start.5 = (bf16[64,4096]{1,0:T(8,128)(2,1)}, bf16[64,4096]{1,0:T(8,128)(2,1)S(1)}, u32[]{:S(2)}, u32[]{:S(2)}) collective-permute-start(bf16[64,4096]{1,0:T(8,128)(2,1)} %get-tuple-element.15), channel_id=1, source_target_pairs={{0,1},{1,0},{2,3},{3,2},{4,5},{5,4},{6,7},{7,6},{8,9},{9,8},{10,11... | collective-permute-start | bytes 1572872 | tf_op jit(solution)/shard_map/ppermute | solution.py:19
  146.1 1.0 copy-start.1
  147.8 11.4 %collective-permute-start.6 = (bf16[16,4096]{1,0:T(8,128)(2,1)S(1)}, bf16[16,4096]{1,0:T(8,128)(2,1)S(1)}, u32[]{:S(2)}, u32[]{:S(2)}) collective-permute-start(bf16[16,4096]{1,0:T(8,128)(2,1)S(1)} %get-tuple-element.17), channel_id=1, source_target_pairs={{0,2},{2,4},{4,6},{6,0},{1,3},{3,5},{5,7},{7,1},{8,10},{10,12},{12... | collective-permute-start | bytes 393224 | tf_op jit(solution)/shard_map/ppermute | solution.py:19
  151.2 9.0 %collective-permute-start.7 = (bf16[16,4096]{1,0:T(8,128)(2,1)S(1)}, bf16[16,4096]{1,0:T(8,128)(2,1)S(1)}, u32[]{:S(2)}, u32[]{:S(2)}) collective-permute-start(bf16[16,4096]{1,0:T(8,128)(2,1)S(1)} %get-tuple-element.18), channel_id=1, source_target_pairs={{0,4},{2,6},{4,0},{6,2},{1,5},{3,7},{5,1},{7,3},{8,12},{10,14},{12... | collective-permute-start | bytes 393224 | tf_op jit(solution)/shard_map/ppermute | solution.py:19
  155.9 6.9 %collective-permute-start.8 = (bf16[16,4096]{1,0:T(8,128)(2,1)S(1)}, bf16[16,4096]{1,0:T(8,128)(2,1)S(1)}, u32[]{:S(2)}, u32[]{:S(2)}) collective-permute-start(bf16[16,4096]{1,0:T(8,128)(2,1)S(1)} %get-tuple-element.19), channel_id=1, source_target_pairs={{0,6},{2,0},{4,2},{6,4},{1,7},{3,1},{5,3},{7,5},{8,14},{10,8},{12,... | collective-permute-start | bytes 393224 | tf_op jit(solution)/shard_map/ppermute | solution.py:19
  176.6 30.4 %collective-permute-start.9 = (bf16[64,4096]{1,0:T(8,128)(2,1)S(1)}, bf16[64,4096]{1,0:T(8,128)(2,1)S(1)}, u32[]{:S(2)}, u32[]{:S(2)}) collective-permute-start(bf16[64,4096]{1,0:T(8,128)(2,1)S(1)} %all_gather.3), channel_id=1, source_target_pairs={{0,1},{1,0},{2,3},{3,2},{4,5},{5,4},{6,7},{7,6},{8,9},{9,8},{10,11... | collective-permute-start | bytes 1572872 | tf_op jit(solution)/shard_map/ppermute | solution.py:19
  178.5 21.3 %all-to-all-start.3 = ((bf16[4,4,32,352]{3,2,1,0:T(8,128)(2,1)}), bf16[4,4,32,352]{3,2,1,0:T(8,128)(2,1)S(1)}, u32[]{:S(2)}, u32[]{:S(2)}) async-start(bf16[4,4,32,352]{3,2,1,0:T(8,128)(2,1)} %get-tuple-element.24), calls=%async_computation.3 | async-start | bytes 786432 | tf_op jit(solution)/shard_map/all_to_all | solution.py:199
  184.5 10.5 %collective-permute-start.10 = (bf16[128,512]{1,0:T(8,128)(2,1)S(1)}, bf16[128,512]{1,0:T(8,128)(2,1)S(1)}, u32[]{:S(2)}, u32[]{:S(2)}) collective-permute-start(bf16[128,512]{1,0:T(8,128)(2,1)S(1)} %get-tuple-element.21), channel_id=1, source_target_pairs={{0,8},{8,16},{16,24},{24,0},{1,9},{9,17},{17,25},{25,1},{2,10},{10... | collective-permute-start | bytes 393224 | tf_op jit(solution)/shard_map/ppermute | solution.py:19
  187.9 9.3 %collective-permute-start.11 = (bf16[128,512]{1,0:T(8,128)(2,1)S(1)}, bf16[128,512]{1,0:T(8,128)(2,1)S(1)}, u32[]{:S(2)}, u32[]{:S(2)}) collective-permute-start(bf16[128,512]{1,0:T(8,128)(2,1)S(1)} %get-tuple-element.22), channel_id=1, source_target_pairs={{0,16},{8,24},{16,0},{24,8},{1,17},{9,25},{17,1},{25,9},{2,18},{10... | collective-permute-start | bytes 393224 | tf_op jit(solution)/shard_map/ppermute | solution.py:19
  190.5 8.7 %collective-permute-start.12 = (bf16[128,512]{1,0:T(8,128)(2,1)S(1)}, bf16[128,512]{1,0:T(8,128)(2,1)S(1)}, u32[]{:S(2)}, u32[]{:S(2)}) collective-permute-start(bf16[128,512]{1,0:T(8,128)(2,1)S(1)} %get-tuple-element.23), channel_id=1, source_target_pairs={{0,24},{8,0},{16,8},{24,16},{1,25},{9,1},{17,9},{25,17},{2,26},{10... | collective-permute-start | bytes 393224 | tf_op jit(solution)/shard_map/ppermute | solution.py:19
  201.7 29.2 %all-to-all-start.4 = ((bf16[16,32,352]{2,1,0:T(8,128)(2,1)}), bf16[16,32,352]{2,1,0:T(8,128)(2,1)S(1)}, u32[]{:S(2)}, u32[]{:S(2)}) async-start(bf16[16,32,352]{2,1,0:T(8,128)(2,1)} %shard_map.112), calls=%async_computation.4 | async-start | bytes 786432 | tf_op jit(solution)/shard_map/all_to_all | solution.py:199
  207.0 23.9 %copy-start.9 = (f32[32,352]{1,0:T(8,128)S(1)}, f32[32,352]{1,0:T(8,128)}, u32[]{:S(2)}) copy-start(f32[32,352]{1,0:T(8,128)} %param.15) | copy-start | bytes 135172

commit v8 on v7

--- a/solution.py
+++ b/solution.py
@@ -34,7 +34,7 @@
     return lax.dot_general(a, b, (((ca,), (cb,)), ((), ())), preferred_element_type=F32)
 
 
-def assemble(at, pieces, wholes, sems):
+def assemble(at, pieces, whole, sem):
     zb, y = at[0], at[1]
     near, a1, a3, far, z1, z3 = pieces
     todo = []
@@ -45,11 +45,9 @@
         todo.append((mine, r, y))
         for dy in range(1, 4):
             todo.append((other.at[dy - 1], r, (y + dy) % 4))
-    for m, whole in enumerate(wholes):
-        for piece, r, yy in todo:
-            pltpu.make_async_copy(
-                piece.at[:, pl.ds(m * 32, 32), :], whole.at[:, (zb + r) % 4, yy], sems.at[m]
-            ).start()
+    for piece, r, yy in todo:
+        pltpu.make_async_copy(piece, whole.at[:, (zb + r) % 4, yy], sem).start()
+    pltpu.make_async_copy(whole, whole, sem).wait()
 
 
 def move(pairs, sems):
@@ -93,20 +91,15 @@
 
 
 def products(at, tok, *refs):
-    pieces, (gds, keep, give, wg, wu, wd, own, parts, sems, outs) = (
+    pieces, (gds, keep, give, whole, own, parts, sem, outs) = (
         refs[:6],
         refs[6:],
     )
-    assemble(at, pieces, (wg, wu, wd), sems)
-    ready = [False] * 3
+    assemble(at, pieces, whole, sem)
     stores = []
 
     def weight(m):
-        whole = (wg, wu, wd)[m]
-        if not ready[m]:
-            pltpu.make_async_copy(whole, whole, sems.at[m]).wait()
-            ready[m] = True
-        return whole[...].reshape(2048, 352)
+        return whole[:, :, :, m * 32 : (m + 1) * 32, :].reshape(2048, 352)
 
     def store(source, target):
         copy = pltpu.make_async_copy(source, target, outs.at[len(stores)])
@@ -140,14 +133,12 @@
 
 def merge(at, b0, b1, b2, b3, out):
     for k, piece in enumerate((b0, b1, b2, b3)):
-        out[(at[1] + 4 - k) % 4] = piece[...]
+        spot = pl.multiple_of((at[1] + 4 - k) % 4 * 128, 128)
+        out[:, pl.ds(spot, 128)] = piece[...].astype(F32).T.astype(BF)
 
 
 def outer(at, cols, gds, grads):
-    total = dot(cols[0], gds[0].reshape(128, 352), 0, 0)
-    for k in range(1, 4):
-        total = total + dot(cols[k], gds[k].reshape(128, 352), 0, 0)
-    total = total.astype(BF)
+    total = dot(cols[...], gds[...].reshape(512, 352), 1, 0).astype(BF)
     for z in range(16):
         grads[z] = total[z * 32 : (z + 1) * 32, :]
 
@@ -189,7 +180,7 @@
 
 
 LIMIT = 24 * 1024 * 1024
-W = (4, 4, 4, 32, 352)
+W = (4, 4, 4, 96, 352)
 SETS = (4, 4, 96, 352)
 TOK = (128, 2048)
 COL = (128, 512)
@@ -222,11 +213,11 @@
     b1 = shift(b1, "y", 1)
     b2 = shift(b2, "y", 2)
     b3 = shift(b3, "y", 3)
-    (cols,) = call(merge, ((4, *COL),), (), at, b0, b1, b2, b3)
+    (cols,) = call(merge, ((512, 512),), (), at, b0, b1, b2, b3)
     gds, keep, give = call(
         products,
         ((4, 4, 32, 352), (64, 4096), (64, 4096)),
-        (W, W, W, (4, 32, 352), (128, 4096), DMA((3,)), DMA((8,))),
+        (W, (4, 32, 352), (128, 4096), DMA, DMA((8,))),
         at, tok, *pieces,
         ins=[VM] + [ANY] * 6,
         to=ANY,

time: 233 us -> 233 us (level)
  no operation moved by 1% of the time
where the time goes in v8:
time: 233 us; the launch traced here: 232 us
  starting transfers between devices  81.4 us (35%)
  waiting for transfers between devices  75.5 us (32%)
  Pallas kernels  52.9 us (23%)
  blocking collectives  13.1 us (6%)
  local copies, waits for them, and re-layouts  5.14 us (2%)
  other arithmetic  2.66 us (1%)
    pallas_call x10, Pallas kernels, call(): pl.pallas_call(body, out_shape=tuple((shape(o) for o in outs)), in_specs=...  52.9 us
    ppermute x12, starting transfers between devices, shift(): return lax.ppermute(array, axis, [(k, (k + by) % n) for k in range(n)])  40.6 us
    ppermute x12, waiting for transfers between devices, shift(): return lax.ppermute(array, axis, [(k, (k + by) % n) for k in range(n)])  27.1 us
    all_to_all x4, waiting for transfers between devices, exchange(): return lax.all_to_all(array, axis, split_axis=0, concat_axis=0, tiled=True)  22.8 us
    all_to_all x4, starting transfers between devices, exchange(): return lax.all_to_all(array, axis, split_axis=0, concat_axis=0, tiled=True)  19.8 us
    all_to_all x1, waiting for transfers between devices, copies_to_all(): return lax.all_to_all(copies, axis, split_axis=0, concat_axis=0, tiled=True)  19 us
    all_to_all x1, starting transfers between devices, copies_to_all(): return lax.all_to_all(copies, axis, split_axis=0, concat_axis=0, tiled=True)  15.1 us
    all_gather x1, blocking collectives, shards(): half = lax.all_gather(done, 'x', axis=0, tiled=True)  13.1 us
  transfers between devices with their start and end apart: 18, of which 10 were waited for; matrix products, arithmetic and copies ran while one was open for 1% of the time, Pallas kernels for 3%

profile of v8, /device:TPU:8, one launch (start us, length us, event | category | flops | bytes accessed | tf_op | source)
XLA Modules:
  0.0 231.6 jit_solution(11593150567506073143)
XLA Ops:
  0.6 0.8 pad_maximum_fusion.1
  1.4 0.7 broadcast_in_dim.3
  2.2 15.1 %all-to-all-start = ((bf16[4,96,352]{2,1,0:T(8,128)(2,1)}), bf16[4,96,352]{2,1,0:T(8,128)(2,1)}, u32[]{:S(2)}, u32[]{:S(2)}) async-start(bf16[4,96,352]{2,1,0:T(8,128)(2,1)} %broadcast_in_dim.3), calls=%async_computation | async-start | bytes 589824 | tf_op jit(solution)/shard_map/all_to_all | solution.py:24
  17.2 0.1 pad_add_fusion.at
  17.3 19.0 %all-to-all-done.piece = bf16[4,96,352]{2,1,0:T(8,128)(2,1)} async-done(((bf16[4,96,352]{2,1,0:T(8,128)(2,1)}), bf16[4,96,352]{2,1,0:T(8,128)(2,1)}, u32[]{:S(2)}, u32[]{:S(2)}) %all-to-all-start) | async-done | bytes 270368 | tf_op jit(solution)/shard_map/all_to_all | solution.py:24
  36.3 37.4 %shard_map.104 = bf16[4,4,96,352]{3,2,1,0:T(8,128)(2,1)} custom-call(s32[4]{0:T(128)S(1)} %pad_add_fusion.at, bf16[4,96,352]{2,1,0:T(8,128)(2,1)} %all-to-all-done.piece), custom_call_target="tpu_custom_call" | custom-call | tf_op jit(solution)/shard_map/pallas_call | solution.py:172
  73.7 4.9 %all-to-all-start.1 = ((bf16[4,4,96,352]{3,2,1,0:T(8,128)(2,1)}), bf16[4,4,96,352]{3,2,1,0:T(8,128)(2,1)S(1)}, u32[]{:S(2)}, u32[]{:S(2)}) async-start(bf16[4,4,96,352]{3,2,1,0:T(8,128)(2,1)} %shard_map.104), calls=%async_computation.1 | async-start | bytes 2359296 | tf_op jit(solution)/shard_map/all_to_all | solution.py:190
  78.6 5.9 %collective-permute-start.2 = (bf16[4,96,352]{2,1,0:T(8,128)(2,1)}, bf16[4,96,352]{2,1,0:T(8,128)(2,1)S(1)}, u32[]{:S(2)}, u32[]{:S(2)}) collective-permute-start(bf16[4,96,352]{2,1,0:T(8,128)(2,1)} %all-to-all-done.piece), channel_id=1, source_target_pairs={{0,448},{32,96},{64,0},{96,160},{128,64},{160,224},{192,128},{224,... | collective-permute-start | bytes 811016 | tf_op jit(solution)/shard_map/ppermute | solution.py:204
  84.5 6.7 %collective-permute-done.2.piece = bf16[4,96,352]{2,1,0:T(8,128)(2,1)S(1)} collective-permute-done((bf16[4,96,352]{2,1,0:T(8,128)(2,1)}, bf16[4,96,352]{2,1,0:T(8,128)(2,1)S(1)}, u32[]{:S(2)}, u32[]{:S(2)}) %collective-permute-start.2) | collective-permute-done | bytes 270368 | tf_op jit(solution)/shard_map/ppermute | solution.py:204
  91.2 1.6 shard_map.105
  92.8 0.0 all-to-all-done.1.near.refs_0_
  92.8 4.8 %all-to-all-start.2 = ((bf16[4,4,96,352]{3,2,1,0:T(8,128)(2,1)}), bf16[4,4,96,352]{3,2,1,0:T(8,128)(2,1)}, u32[]{:S(2)}, u32[]{:S(2)}) async-start(bf16[4,4,96,352]{3,2,1,0:T(8,128)(2,1)} %shard_map.105), calls=%async_computation.2 | async-start | bytes 2359296 | tf_op jit(solution)/shard_map/all_to_all | solution.py:190
  97.7 1.5 shard_map.106
  99.2 5.2 %collective-permute-start.3 = (bf16[3,4,96,352]{3,2,1,0:T(8,128)(2,1)}, bf16[3,4,96,352]{3,2,1,0:T(8,128)(2,1)}, u32[]{:S(2)}, u32[]{:S(2)}) collective-permute-start(bf16[3,4,96,352]{3,2,1,0:T(8,128)(2,1)} %shard_map.106), channel_id=1, source_target_pairs={{0,480},{32,0},{64,32},{96,64},{128,96},{160,128},{192,160},{224,1... | collective-permute-start | bytes 2433032 | tf_op jit(solution)/shard_map/ppermute | solution.py:19
  104.4 3.9 %collective-permute-start.4 = (bf16[3,4,96,352]{3,2,1,0:T(8,128)(2,1)}, bf16[3,4,96,352]{3,2,1,0:T(8,128)(2,1)}, u32[]{:S(2)}, u32[]{:S(2)}) collective-permute-start(bf16[3,4,96,352]{3,2,1,0:T(8,128)(2,1)} %shard_map.106), channel_id=1, source_target_pairs={{0,32},{32,64},{64,96},{96,128},{128,160},{160,192},{192,224},{224... | collective-permute-start | bytes 2433032 | tf_op jit(solution)/shard_map/ppermute | solution.py:19
  108.3 3.2 %collective-permute-start = (bf16[4,96,352]{2,1,0:T(8,128)(2,1)}, bf16[4,96,352]{2,1,0:T(8,128)(2,1)S(1)}, u32[]{:S(2)}, u32[]{:S(2)}) collective-permute-start(bf16[4,96,352]{2,1,0:T(8,128)(2,1)} %all-to-all-done.piece), channel_id=1, source_target_pairs={{0,480},{32,0},{64,32},{96,64},{128,96},{160,128},{192,160},{224,1... | collective-permute-start | bytes 811016 | tf_op jit(solution)/shard_map/ppermute | solution.py:19
  111.5 2.7 %collective-permute-start.1 = (bf16[4,96,352]{2,1,0:T(8,128)(2,1)}, bf16[4,96,352]{2,1,0:T(8,128)(2,1)S(1)}, u32[]{:S(2)}, u32[]{:S(2)}) collective-permute-start(bf16[4,96,352]{2,1,0:T(8,128)(2,1)} %all-to-all-done.piece), channel_id=1, source_target_pairs={{0,32},{32,64},{64,96},{96,128},{128,160},{160,192},{192,224},{224... | collective-permute-start | bytes 811016 | tf_op jit(solution)/shard_map/ppermute | solution.py:19
  114.2 0.0 copy-done
  114.2 0.0 copy-done.2
  114.2 0.0 copy-done.3
  114.2 1.0 shard_map.103.tok
  115.2 15.4 %collective-permute-done.refs_1_ = bf16[4,96,352]{2,1,0:T(8,128)(2,1)S(1)} collective-permute-done((bf16[4,96,352]{2,1,0:T(8,128)(2,1)}, bf16[4,96,352]{2,1,0:T(8,128)(2,1)S(1)}, u32[]{:S(2)}, u32[]{:S(2)}) %collective-permute-start) | collective-permute-done | bytes 270368 | tf_op jit(solution)/shard_map/ppermute | solution.py:19
  130.6 0.7 copy-done.4
  131.3 1.9 collective-permute-done.1.refs_2_
  133.1 0.7 copy-done.6
  133.9 0.0 all-to-all-done.2.refs_3_
  133.9 0.0 collective-permute-done.3.refs_4_
  133.9 0.0 collective-permute-done.4.refs_5_
  133.9 0.0 copy-start.5
  133.9 1.0 copy-done.5
  134.8 1.0 copy-done.7
  135.8 6.3 %shard_map.107 = (bf16[4,4,32,352]{3,2,1,0:T(8,128)(2,1)}, bf16[64,4096]{1,0:T(8,128)(2,1)}, bf16[64,4096]{1,0:T(8,128)(2,1)}) custom-call(s32[4]{0:T(128)S(1)} %pad_add_fusion.at, bf16[3,128,2048]{2,1,0:T(8,128)(2,1)S(1)} %shard_map.103.tok, bf16[4,4,96,352]{3,2,1,0:T(8,128)(2,1)S(1)} %all-to-all-done.1.near.refs_0_, bf16[4,96,352]{2,1,0:T(8,128)(2,1)S(1)} %copy-done.5, ...), custom_call_target="tpu_custom_call" | custom-call | tf_op jit(solution)/shard_map/pallas_call | solution.py:172
  142.1 1.9 collective-permute-start.5
  144.1 2.1 collective-permute-done.5.other
  146.1 1.0 copy-done.1
  147.2 0.7 shard_map.108
  147.9 3.4 %collective-permute-start.6 = (bf16[16,4096]{1,0:T(8,128)(2,1)S(1)}, bf16[16,4096]{1,0:T(8,128)(2,1)S(1)}, u32[]{:S(2)}, u32[]{:S(2)}) collective-permute-start(bf16[16,4096]{1,0:T(8,128)(2,1)S(1)} %get-tuple-element.17), channel_id=1, source_target_pairs={{0,2},{2,4},{4,6},{6,0},{1,3},{3,5},{5,7},{7,1},{8,10},{10,12},{12... | collective-permute-start | bytes 393224 | tf_op jit(solution)/shard_map/ppermute | solution.py:19
  151.3 4.6 %collective-permute-start.7 = (bf16[16,4096]{1,0:T(8,128)(2,1)S(1)}, bf16[16,4096]{1,0:T(8,128)(2,1)S(1)}, u32[]{:S(2)}, u32[]{:S(2)}) collective-permute-start(bf16[16,4096]{1,0:T(8,128)(2,1)S(1)} %get-tuple-element.18), channel_id=1, source_target_pairs={{0,4},{2,6},{4,0},{6,2},{1,5},{3,7},{5,1},{7,3},{8,12},{10,14},{12... | collective-permute-start | bytes 393224 | tf_op jit(solution)/shard_map/ppermute | solution.py:19
  155.9 3.3 %collective-permute-start.8 = (bf16[16,4096]{1,0:T(8,128)(2,1)S(1)}, bf16[16,4096]{1,0:T(8,128)(2,1)S(1)}, u32[]{:S(2)}, u32[]{:S(2)}) collective-permute-start(bf16[16,4096]{1,0:T(8,128)(2,1)S(1)} %get-tuple-element.19), channel_id=1, source_target_pairs={{0,6},{2,0},{4,2},{6,4},{1,7},{3,1},{5,3},{7,5},{8,14},{10,8},{12,... | collective-permute-start | bytes 393224 | tf_op jit(solution)/shard_map/ppermute | solution.py:19
  159.3 0.0 collective-permute-done.6.p1
  159.3 1.0 collective-permute-done.7.p2
  160.3 2.5 %collective-permute-done.8.p3 = bf16[16,4096]{1,0:T(8,128)(2,1)S(1)} collective-permute-done((bf16[16,4096]{1,0:T(8,128)(2,1)S(1)}, bf16[16,4096]{1,0:T(8,128)(2,1)S(1)}, u32[]{:S(2)}, u32[]{:S(2)}) %collective-permute-start.8) | collective-permute-done | bytes 131104 | tf_op jit(solution)/shard_map/ppermute | solution.py:19
  162.8 0.7 shard_map.109
  163.5 13.1 %all_gather.3 = bf16[64,4096]{1,0:T(8,128)(2,1)S(1)} all-gather(bf16[16,4096]{1,0:T(8,128)(2,1)S(1)} %shard_map.109), channel_id=1, replica_groups=mesh['za'=4,'zb'=4,'y'=4,'x'=4,'c'=2] {'x'}, dimensions={0}, use_global_device_ids=true | all-gather | bytes 655360 | tf_op jit(solution)/shard_map/all_gather | solution.py:234
  176.6 1.9 collective-permute-start.9
  178.5 4.8 %all-to-all-start.3 = ((bf16[4,4,32,352]{3,2,1,0:T(8,128)(2,1)}), bf16[4,4,32,352]{3,2,1,0:T(8,128)(2,1)S(1)}, u32[]{:S(2)}, u32[]{:S(2)}) async-start(bf16[4,4,32,352]{3,2,1,0:T(8,128)(2,1)} %get-tuple-element.24), calls=%async_computation.3 | async-start | bytes 786432 | tf_op jit(solution)/shard_map/all_to_all | solution.py:190
  183.3 1.2 shard_map.110
  184.5 3.4 %collective-permute-start.10 = (bf16[128,512]{1,0:T(8,128)(2,1)S(1)}, bf16[128,512]{1,0:T(8,128)(2,1)S(1)}, u32[]{:S(2)}, u32[]{:S(2)}) collective-permute-start(bf16[128,512]{1,0:T(8,128)(2,1)S(1)} %get-tuple-element.21), channel_id=1, source_target_pairs={{0,8},{8,16},{16,24},{24,0},{1,9},{9,17},{17,25},{25,1},{2,10},{10... | collective-permute-start | bytes 393224 | tf_op jit(solution)/shard_map/ppermute | solution.py:19
  187.9 2.5 %collective-permute-start.11 = (bf16[128,512]{1,0:T(8,128)(2,1)S(1)}, bf16[128,512]{1,0:T(8,128)(2,1)S(1)}, u32[]{:S(2)}, u32[]{:S(2)}) collective-permute-start(bf16[128,512]{1,0:T(8,128)(2,1)S(1)} %get-tuple-element.22), channel_id=1, source_target_pairs={{0,16},{8,24},{16,0},{24,8},{1,17},{9,25},{17,1},{25,9},{2,18},{10... | collective-permute-start | bytes 393224 | tf_op jit(solution)/shard_map/ppermute | solution.py:19
  190.5 4.5 %collective-permute-start.12 = (bf16[128,512]{1,0:T(8,128)(2,1)S(1)}, bf16[128,512]{1,0:T(8,128)(2,1)S(1)}, u32[]{:S(2)}, u32[]{:S(2)}) collective-permute-start(bf16[128,512]{1,0:T(8,128)(2,1)S(1)} %get-tuple-element.23), channel_id=1, source_target_pairs={{0,24},{8,0},{16,8},{24,16},{1,25},{9,1},{17,9},{25,17},{2,26},{10... | collective-permute-start | bytes 393224 | tf_op jit(solution)/shard_map/ppermute | solution.py:19
  195.0 0.0 collective-permute-done.10.b1
  195.0 2.3 collective-permute-done.11.b2
  197.3 1.9 collective-permute-done.12.b3
  199.2 0.7 shard_map.111.cols
  199.9 0.0 all-to-all-done.3.gds
  200.0 1.7 shard_map.112
  201.7 5.3 %all-to-all-start.4 = ((bf16[16,32,352]{2,1,0:T(8,128)(2,1)}), bf16[16,32,352]{2,1,0:T(8,128)(2,1)S(1)}, u32[]{:S(2)}, u32[]{:S(2)}) async-start(bf16[16,32,352]{2,1,0:T(8,128)(2,1)} %shard_map.112), calls=%async_computation.4 | async-start | bytes 786432 | tf_op jit(solution)/shard_map/all_to_all | solution.py:190
  207.0 0.0 collective-permute-done.9
  207.0 0.1 broadcast_select_fusion
  207.1 0.0 copy-start.9
  207.1 1.0 pad_maximum_fusion
  208.2 22.8 %all-to-all-done.4 = bf16[16,32,352]{2,1,0:T(8,128)(2,1)S(1)} async-done(((bf16[16,32,352]{2,1,0:T(8,128)(2,1)}), bf16[16,32,352]{2,1,0:T(8,128)(2,1)S(1)}, u32[]{:S(2)}, u32[]{:S(2)}) %all-to-all-start.4) | async-done | bytes 360480 | tf_op jit(solution)/shard_map/all_to_all | solution.py:190
  230.9 0.1 convert_reduce_fusion
  231.0 0.6 add.3
  (10 shorter events, 0.0 us)
Async XLA Ops:
  2.2 34.1 %all-to-all-start = ((bf16[4,96,352]{2,1,0:T(8,128)(2,1)}), bf16[4,96,352]{2,1,0:T(8,128)(2,1)}, u32[]{:S(2)}, u32[]{:S(2)}) async-start(bf16[4,96,352]{2,1,0:T(8,128)(2,1)} %broadcast_in_dim.3), calls=%async_computation | async-start | bytes 589824 | tf_op jit(solution)/shard_map/all_to_all | solution.py:24
  73.7 19.1 %all-to-all-start.1 = ((bf16[4,4,96,352]{3,2,1,0:T(8,128)(2,1)}), bf16[4,4,96,352]{3,2,1,0:T(8,128)(2,1)S(1)}, u32[]{:S(2)}, u32[]{:S(2)}) async-start(bf16[4,4,96,352]{3,2,1,0:T(8,128)(2,1)} %shard_map.104), calls=%async_computation.1 | async-start | bytes 2359296 | tf_op jit(solution)/shard_map/all_to_all | solution.py:190
  78.6 12.6 %collective-permute-start.2 = (bf16[4,96,352]{2,1,0:T(8,128)(2,1)}, bf16[4,96,352]{2,1,0:T(8,128)(2,1)S(1)}, u32[]{:S(2)}, u32[]{:S(2)}) collective-permute-start(bf16[4,96,352]{2,1,0:T(8,128)(2,1)} %all-to-all-done.piece), channel_id=1, source_target_pairs={{0,448},{32,96},{64,0},{96,160},{128,64},{160,224},{192,128},{224,... | collective-permute-start | bytes 811016 | tf_op jit(solution)/shard_map/ppermute | solution.py:204
  92.8 41.0 %all-to-all-start.2 = ((bf16[4,4,96,352]{3,2,1,0:T(8,128)(2,1)}), bf16[4,4,96,352]{3,2,1,0:T(8,128)(2,1)}, u32[]{:S(2)}, u32[]{:S(2)}) async-start(bf16[4,4,96,352]{3,2,1,0:T(8,128)(2,1)} %shard_map.105), calls=%async_computation.2 | async-start | bytes 2359296 | tf_op jit(solution)/shard_map/all_to_all | solution.py:190
  97.6 16.5 %copy-start = (bf16[128,2048]{1,0:T(8,128)(2,1)S(1)}, bf16[128,2048]{1,0:T(8,128)(2,1)}, u32[]{:S(2)}) copy-start(bf16[128,2048]{1,0:T(8,128)(2,1)} %bt.5) | copy-start | bytes 1572868
  97.7 16.5 %copy-start.2 = (bf16[128,2048]{1,0:T(8,128)(2,1)S(1)}, bf16[128,2048]{1,0:T(8,128)(2,1)}, u32[]{:S(2)}) copy-start(bf16[128,2048]{1,0:T(8,128)(2,1)} %ft.1) | copy-start | bytes 1572868
  97.7 16.5 %copy-start.3 = (bf16[128,2048]{1,0:T(8,128)(2,1)S(1)}, bf16[128,2048]{1,0:T(8,128)(2,1)}, u32[]{:S(2)}) copy-start(bf16[128,2048]{1,0:T(8,128)(2,1)} %og.1) | copy-start | bytes 1572868
  97.7 16.5 %copy-start.8 = (f32[2048]{0:T(1024)S(1)}, f32[2048]{0:T(1024)}, u32[]{:S(2)}) copy-start(f32[2048]{0:T(1024)} %param.11) | copy-start | bytes 24580
  99.2 34.7 %collective-permute-start.3 = (bf16[3,4,96,352]{3,2,1,0:T(8,128)(2,1)}, bf16[3,4,96,352]{3,2,1,0:T(8,128)(2,1)}, u32[]{:S(2)}, u32[]{:S(2)}) collective-permute-start(bf16[3,4,96,352]{3,2,1,0:T(8,128)(2,1)} %shard_map.106), channel_id=1, source_target_pairs={{0,480},{32,0},{64,32},{96,64},{128,96},{160,128},{192,160},{224,1... | collective-permute-start | bytes 2433032 | tf_op jit(solution)/shard_map/ppermute | solution.py:19
  104.4 29.4 %collective-permute-start.4 = (bf16[3,4,96,352]{3,2,1,0:T(8,128)(2,1)}, bf16[3,4,96,352]{3,2,1,0:T(8,128)(2,1)}, u32[]{:S(2)}, u32[]{:S(2)}) collective-permute-start(bf16[3,4,96,352]{3,2,1,0:T(8,128)(2,1)} %shard_map.106), channel_id=1, source_target_pairs={{0,32},{32,64},{64,96},{96,128},{128,160},{160,192},{192,224},{224... | collective-permute-start | bytes 2433032 | tf_op jit(solution)/shard_map/ppermute | solution.py:19
  108.3 22.3 %collective-permute-start = (bf16[4,96,352]{2,1,0:T(8,128)(2,1)}, bf16[4,96,352]{2,1,0:T(8,128)(2,1)S(1)}, u32[]{:S(2)}, u32[]{:S(2)}) collective-permute-start(bf16[4,96,352]{2,1,0:T(8,128)(2,1)} %all-to-all-done.piece), channel_id=1, source_target_pairs={{0,480},{32,0},{64,32},{96,64},{128,96},{160,128},{192,160},{224,1... | collective-permute-start | bytes 811016 | tf_op jit(solution)/shard_map/ppermute | solution.py:19
  111.5 21.6 %collective-permute-start.1 = (bf16[4,96,352]{2,1,0:T(8,128)(2,1)}, bf16[4,96,352]{2,1,0:T(8,128)(2,1)S(1)}, u32[]{:S(2)}, u32[]{:S(2)}) collective-permute-start(bf16[4,96,352]{2,1,0:T(8,128)(2,1)} %all-to-all-done.piece), channel_id=1, source_target_pairs={{0,32},{32,64},{64,96},{96,128},{128,160},{160,192},{192,224},{224... | collective-permute-start | bytes 811016 | tf_op jit(solution)/shard_map/ppermute | solution.py:19
  130.6 0.7 copy-start.4
  133.1 0.7 copy-start.6
  133.9 1.0 copy-start.5
  134.8 1.0 copy-start.7
  142.1 4.0 %collective-permute-start.5 = (bf16[64,4096]{1,0:T(8,128)(2,1)}, bf16[64,4096]{1,0:T(8,128)(2,1)S(1)}, u32[]{:S(2)}, u32[]{:S(2)}) collective-permute-start(bf16[64,4096]{1,0:T(8,128)(2,1)} %get-tuple-element.15), channel_id=1, source_target_pairs={{0,1},{1,0},{2,3},{3,2},{4,5},{5,4},{6,7},{7,6},{8,9},{9,8},{10,11... | collective-permute-start | bytes 1572872 | tf_op jit(solution)/shard_map/ppermute | solution.py:19
  146.1 1.0 copy-start.1
  147.9 11.4 %collective-permute-start.6 = (bf16[16,4096]{1,0:T(8,128)(2,1)S(1)}, bf16[16,4096]{1,0:T(8,128)(2,1)S(1)}, u32[]{:S(2)}, u32[]{:S(2)}) collective-permute-start(bf16[16,4096]{1,0:T(8,128)(2,1)S(1)} %get-tuple-element.17), channel_id=1, source_target_pairs={{0,2},{2,4},{4,6},{6,0},{1,3},{3,5},{5,7},{7,1},{8,10},{10,12},{12... | collective-permute-start | bytes 393224 | tf_op jit(solution)/shard_map/ppermute | solution.py:19
  151.3 9.0 %collective-permute-start.7 = (bf16[16,4096]{1,0:T(8,128)(2,1)S(1)}, bf16[16,4096]{1,0:T(8,128)(2,1)S(1)}, u32[]{:S(2)}, u32[]{:S(2)}) collective-permute-start(bf16[16,4096]{1,0:T(8,128)(2,1)S(1)} %get-tuple-element.18), channel_id=1, source_target_pairs={{0,4},{2,6},{4,0},{6,2},{1,5},{3,7},{5,1},{7,3},{8,12},{10,14},{12... | collective-permute-start | bytes 393224 | tf_op jit(solution)/shard_map/ppermute | solution.py:19
  155.9 6.9 %collective-permute-start.8 = (bf16[16,4096]{1,0:T(8,128)(2,1)S(1)}, bf16[16,4096]{1,0:T(8,128)(2,1)S(1)}, u32[]{:S(2)}, u32[]{:S(2)}) collective-permute-start(bf16[16,4096]{1,0:T(8,128)(2,1)S(1)} %get-tuple-element.19), channel_id=1, source_target_pairs={{0,6},{2,0},{4,2},{6,4},{1,7},{3,1},{5,3},{7,5},{8,14},{10,8},{12,... | collective-permute-start | bytes 393224 | tf_op jit(solution)/shard_map/ppermute | solution.py:19
  176.6 30.4 %collective-permute-start.9 = (bf16[64,4096]{1,0:T(8,128)(2,1)S(1)}, bf16[64,4096]{1,0:T(8,128)(2,1)S(1)}, u32[]{:S(2)}, u32[]{:S(2)}) collective-permute-start(bf16[64,4096]{1,0:T(8,128)(2,1)S(1)} %all_gather.3), channel_id=1, source_target_pairs={{0,1},{1,0},{2,3},{3,2},{4,5},{5,4},{6,7},{7,6},{8,9},{9,8},{10,11... | collective-permute-start | bytes 1572872 | tf_op jit(solution)/shard_map/ppermute | solution.py:19
  178.5 21.4 %all-to-all-start.3 = ((bf16[4,4,32,352]{3,2,1,0:T(8,128)(2,1)}), bf16[4,4,32,352]{3,2,1,0:T(8,128)(2,1)S(1)}, u32[]{:S(2)}, u32[]{:S(2)}) async-start(bf16[4,4,32,352]{3,2,1,0:T(8,128)(2,1)} %get-tuple-element.24), calls=%async_computation.3 | async-start | bytes 786432 | tf_op jit(solution)/shard_map/all_to_all | solution.py:190
  184.5 10.5 %collective-permute-start.10 = (bf16[128,512]{1,0:T(8,128)(2,1)S(1)}, bf16[128,512]{1,0:T(8,128)(2,1)S(1)}, u32[]{:S(2)}, u32[]{:S(2)}) collective-permute-start(bf16[128,512]{1,0:T(8,128)(2,1)S(1)} %get-tuple-element.21), channel_id=1, source_target_pairs={{0,8},{8,16},{16,24},{24,0},{1,9},{9,17},{17,25},{25,1},{2,10},{10... | collective-permute-start | bytes 393224 | tf_op jit(solution)/shard_map/ppermute | solution.py:19
  187.9 9.3 %collective-permute-start.11 = (bf16[128,512]{1,0:T(8,128)(2,1)S(1)}, bf16[128,512]{1,0:T(8,128)(2,1)S(1)}, u32[]{:S(2)}, u32[]{:S(2)}) collective-permute-start(bf16[128,512]{1,0:T(8,128)(2,1)S(1)} %get-tuple-element.22), channel_id=1, source_target_pairs={{0,16},{8,24},{16,0},{24,8},{1,17},{9,25},{17,1},{25,9},{2,18},{10... | collective-permute-start | bytes 393224 | tf_op jit(solution)/shard_map/ppermute | solution.py:19
  190.5 8.7 %collective-permute-start.12 = (bf16[128,512]{1,0:T(8,128)(2,1)S(1)}, bf16[128,512]{1,0:T(8,128)(2,1)S(1)}, u32[]{:S(2)}, u32[]{:S(2)}) collective-permute-start(bf16[128,512]{1,0:T(8,128)(2,1)S(1)} %get-tuple-element.23), channel_id=1, source_target_pairs={{0,24},{8,0},{16,8},{24,16},{1,25},{9,1},{17,9},{25,17},{2,26},{10... | collective-permute-start | bytes 393224 | tf_op jit(solution)/shard_map/ppermute | solution.py:19
  201.7 29.3 %all-to-all-start.4 = ((bf16[16,32,352]{2,1,0:T(8,128)(2,1)}), bf16[16,32,352]{2,1,0:T(8,128)(2,1)S(1)}, u32[]{:S(2)}, u32[]{:S(2)}) async-start(bf16[16,32,352]{2,1,0:T(8,128)(2,1)} %shard_map.112), calls=%async_computation.4 | async-start | bytes 786432 | tf_op jit(solution)/shard_map/all_to_all | solution.py:190
  207.1 23.9 %copy-start.9 = (f32[32,352]{1,0:T(8,128)S(1)}, f32[32,352]{1,0:T(8,128)}, u32[]{:S(2)}) copy-start(f32[32,352]{1,0:T(8,128)} %param.15) | copy-start | bytes 135172

commit v9 on v7

--- a/solution.py
+++ b/solution.py
@@ -66,6 +66,15 @@
 
 def turn(at, near, out, sems):
     move([(near.at[(at[1] + k) % 4], out.at[k - 1]) for k in range(1, 4)], sems)
+
+
+def place(at, half, other, fwd, back, sems):
+    pairs = []
+    for part, c in ((half, at[2]), (other, 1 - at[2])):
+        rows = pl.ds(pl.multiple_of(c * 64, 64), 64)
+        pairs.append((part.at[:, pl.ds(0, 2048)], fwd.at[rows, :]))
+        pairs.append((part.at[:, pl.ds(2048, 2048)], back.at[rows, :]))
+    move(pairs, sems)
 
 
 def columns(at, bt, gain, b0, b1, b2, b3, split):
@@ -140,14 +149,12 @@
 
 def merge(at, b0, b1, b2, b3, out):
     for k, piece in enumerate((b0, b1, b2, b3)):
-        out[(at[1] + 4 - k) % 4] = piece[...]
+        spot = pl.multiple_of((at[1] + 4 - k) % 4 * 128, 128)
+        out[:, pl.ds(spot, 128)] = piece[...].astype(F32).T.astype(BF)
 
 
 def outer(at, cols, gds, grads):
-    total = dot(cols[0], gds[0].reshape(128, 352), 0, 0)
-    for k in range(1, 4):
-        total = total + dot(cols[k], gds[k].reshape(128, 352), 0, 0)
-    total = total.astype(BF)
+    total = dot(cols[...], gds[...].reshape(512, 352), 1, 0).astype(BF)
     for z in range(16):
         grads[z] = total[z * 32 : (z + 1) * 32, :]
 
@@ -201,7 +208,6 @@
 
 def shards(ft, bt, og, gain, gw, uw, dw, gsum):
     spots = [lax.axis_index(n) for n in ("zb", "y", "c", "x")]
-    c = spots[2]
     at = jnp.stack(spots).astype(jnp.int32)
     gain = gain.reshape(1, 2048)
     own = jnp.concatenate([gw, uw, dw], axis=0)
@@ -222,7 +228,7 @@
     b1 = shift(b1, "y", 1)
     b2 = shift(b2, "y", 2)
     b3 = shift(b3, "y", 3)
-    (cols,) = call(merge, ((4, *COL),), (), at, b0, b1, b2, b3)
+    (cols,) = call(merge, ((512, 512),), (), at, b0, b1, b2, b3)
     gds, keep, give = call(
         products,
         ((4, 4, 32, 352), (64, 4096), (64, 4096)),
@@ -242,11 +248,9 @@
     (done,) = call(finish, ((16, 4096),), (), at, p0, p1, p2, p3, bt, gain)
     half = lax.all_gather(done, "x", axis=0, tiled=True)
     other = shift(half, "c", 1)
-    first = jnp.where(c == 0, half, other)
-    second = jnp.where(c == 0, other, half)
-    whole = jnp.concatenate([first, second], axis=0)
+    fwd, back = call(place, (TOK, TOK), (DMA((4,)),), at, half, other, ins=[ANY] * 2, to=ANY)
     grad = gsum + gz.astype(F32).sum(axis=0)
-    return whole[:, :2048], whole[:, 2048:], grad
+    return fwd, back, grad
 
 
 def solution(mesh):

time: 233 us -> 209 us (0.90)
  the two profiles are of different devices: /device:TPU:8 before, /device:TPU:1 now
where the time goes in v9:
time: 209 us; the launch traced here: 208 us
  starting transfers between devices  93.7 us (45%)
  Pallas kernels  54.4 us (26%)
  waiting for transfers between devices  42.5 us (20%)
  blocking collectives  10.8 us (5%)
  local copies, waits for them, and re-layouts  4.12 us (2%)
    pallas_call x11, Pallas kernels, call(): pl.pallas_call(body, out_shape=tuple((shape(o) for o in outs)), in_specs=...  54.4 us
    ppermute x12, starting transfers between devices, shift(): return lax.ppermute(array, axis, [(k, (k + by) % n) for k in range(n)])  50.3 us
    ppermute x12, waiting for transfers between devices, shift(): return lax.ppermute(array, axis, [(k, (k + by) % n) for k in range(n)])  21.9 us
    all_to_all x4, starting transfers between devices, exchange(): return lax.all_to_all(array, axis, split_axis=0, concat_axis=0, tiled=True)  17.5 us
    all_to_all x1, starting transfers between devices, copies_to_all(): return lax.all_to_all(copies, axis, split_axis=0, concat_axis=0, tiled=True)  15.6 us
    all_to_all x1, waiting for transfers between devices, copies_to_all(): return lax.all_to_all(copies, axis, split_axis=0, concat_axis=0, tiled=True)  14.2 us
    all_gather x1, blocking collectives, shards(): half = lax.all_gather(done, 'x', axis=0, tiled=True)  10.8 us
    ppermute x1, starting transfers between devices, shards(): lax.ppermute(a, Z, [(k, (k + (2 if k % 2 else -2)) % 16) for k in range(1...  10.3 us
  transfers between devices with their start and end apart: 18, of which 7 were waited for; matrix products, arithmetic and copies ran while one was open for 0% of the time, Pallas kernels for 5%

profile of v9, /device:TPU:1, one launch (start us, length us, event | category | flops | bytes accessed | tf_op | source)
XLA Modules:
  0.0 208.0 jit_solution(7265374391063315774)
XLA Ops:
  0.6 0.8 pad_maximum_fusion
  1.4 0.7 broadcast_in_dim.3
  2.2 15.6 %all-to-all-start = ((bf16[4,96,352]{2,1,0:T(8,128)(2,1)}), bf16[4,96,352]{2,1,0:T(8,128)(2,1)}, u32[]{:S(2)}, u32[]{:S(2)}) async-start(bf16[4,96,352]{2,1,0:T(8,128)(2,1)} %broadcast_in_dim.3), calls=%async_computation | async-start | bytes 589824 | tf_op jit(solution)/shard_map/all_to_all | solution.py:24
  17.8 0.1 pad_add_fusion.at
  17.9 14.2 %all-to-all-done.piece = bf16[4,96,352]{2,1,0:T(8,128)(2,1)} async-done(((bf16[4,96,352]{2,1,0:T(8,128)(2,1)}), bf16[4,96,352]{2,1,0:T(8,128)(2,1)}, u32[]{:S(2)}, u32[]{:S(2)}) %all-to-all-start) | async-done | bytes 270368 | tf_op jit(solution)/shard_map/all_to_all | solution.py:24
  32.1 37.4 %shard_map.104 = bf16[4,4,96,352]{3,2,1,0:T(8,128)(2,1)} custom-call(s32[4]{0:T(128)S(1)} %pad_add_fusion.at, bf16[4,96,352]{2,1,0:T(8,128)(2,1)} %all-to-all-done.piece), custom_call_target="tpu_custom_call" | custom-call | tf_op jit(solution)/shard_map/pallas_call | solution.py:188
  69.5 4.2 %all-to-all-start.1 = ((bf16[4,4,96,352]{3,2,1,0:T(8,128)(2,1)}), bf16[4,4,96,352]{3,2,1,0:T(8,128)(2,1)S(1)}, u32[]{:S(2)}, u32[]{:S(2)}) async-start(bf16[4,4,96,352]{3,2,1,0:T(8,128)(2,1)} %shard_map.104), calls=%async_computation.1 | async-start | bytes 2359296 | tf_op jit(solution)/shard_map/all_to_all | solution.py:206
  73.7 10.3 %collective-permute-start.2 = (bf16[4,96,352]{2,1,0:T(8,128)(2,1)}, bf16[4,96,352]{2,1,0:T(8,128)(2,1)S(1)}, u32[]{:S(2)}, u32[]{:S(2)}) collective-permute-start(bf16[4,96,352]{2,1,0:T(8,128)(2,1)} %all-to-all-done.piece), channel_id=1, source_target_pairs={{0,448},{32,96},{64,0},{96,160},{128,64},{160,224},{192,128},{224,... | collective-permute-start | bytes 811016 | tf_op jit(solution)/shard_map/ppermute | solution.py:219
  84.0 6.3 %collective-permute-done.2.piece = bf16[4,96,352]{2,1,0:T(8,128)(2,1)S(1)} collective-permute-done((bf16[4,96,352]{2,1,0:T(8,128)(2,1)}, bf16[4,96,352]{2,1,0:T(8,128)(2,1)S(1)}, u32[]{:S(2)}, u32[]{:S(2)}) %collective-permute-start.2) | collective-permute-done | bytes 270368 | tf_op jit(solution)/shard_map/ppermute | solution.py:219
  90.4 1.6 shard_map.105
  92.0 0.0 all-to-all-done.1.near.refs_0_
  92.0 4.3 %all-to-all-start.2 = ((bf16[4,4,96,352]{3,2,1,0:T(8,128)(2,1)}), bf16[4,4,96,352]{3,2,1,0:T(8,128)(2,1)}, u32[]{:S(2)}, u32[]{:S(2)}) async-start(bf16[4,4,96,352]{3,2,1,0:T(8,128)(2,1)} %shard_map.105), calls=%async_computation.2 | async-start | bytes 2359296 | tf_op jit(solution)/shard_map/all_to_all | solution.py:206
  96.3 0.0 copy-start
  96.3 0.0 copy-start.2
  96.3 0.0 copy-start.3
  96.3 0.0 copy-start.8
  96.3 1.5 shard_map.106
  97.8 3.0 %collective-permute-start.3 = (bf16[3,4,96,352]{3,2,1,0:T(8,128)(2,1)}, bf16[3,4,96,352]{3,2,1,0:T(8,128)(2,1)}, u32[]{:S(2)}, u32[]{:S(2)}) collective-permute-start(bf16[3,4,96,352]{3,2,1,0:T(8,128)(2,1)} %shard_map.106), channel_id=1, source_target_pairs={{0,480},{32,0},{64,32},{96,64},{128,96},{160,128},{192,160},{224,1... | collective-permute-start | bytes 2433032 | tf_op jit(solution)/shard_map/ppermute | solution.py:19
  100.8 5.9 %collective-permute-start.4 = (bf16[3,4,96,352]{3,2,1,0:T(8,128)(2,1)}, bf16[3,4,96,352]{3,2,1,0:T(8,128)(2,1)}, u32[]{:S(2)}, u32[]{:S(2)}) collective-permute-start(bf16[3,4,96,352]{3,2,1,0:T(8,128)(2,1)} %shard_map.106), channel_id=1, source_target_pairs={{0,32},{32,64},{64,96},{96,128},{128,160},{160,192},{192,224},{224... | collective-permute-start | bytes 2433032 | tf_op jit(solution)/shard_map/ppermute | solution.py:19
  106.8 2.6 %collective-permute-start = (bf16[4,96,352]{2,1,0:T(8,128)(2,1)}, bf16[4,96,352]{2,1,0:T(8,128)(2,1)S(1)}, u32[]{:S(2)}, u32[]{:S(2)}) collective-permute-start(bf16[4,96,352]{2,1,0:T(8,128)(2,1)} %all-to-all-done.piece), channel_id=1, source_target_pairs={{0,480},{32,0},{64,32},{96,64},{128,96},{160,128},{192,160},{224,1... | collective-permute-start | bytes 811016 | tf_op jit(solution)/shard_map/ppermute | solution.py:19
  109.4 2.7 %collective-permute-start.1 = (bf16[4,96,352]{2,1,0:T(8,128)(2,1)}, bf16[4,96,352]{2,1,0:T(8,128)(2,1)S(1)}, u32[]{:S(2)}, u32[]{:S(2)}) collective-permute-start(bf16[4,96,352]{2,1,0:T(8,128)(2,1)} %all-to-all-done.piece), channel_id=1, source_target_pairs={{0,32},{32,64},{64,96},{96,128},{128,160},{160,192},{192,224},{224... | collective-permute-start | bytes 811016 | tf_op jit(solution)/shard_map/ppermute | solution.py:19
  112.1 0.0 copy-done
  112.1 1.0 shard_map.103.tok
  113.1 16.0 %collective-permute-done.refs_1_ = bf16[4,96,352]{2,1,0:T(8,128)(2,1)S(1)} collective-permute-done((bf16[4,96,352]{2,1,0:T(8,128)(2,1)}, bf16[4,96,352]{2,1,0:T(8,128)(2,1)S(1)}, u32[]{:S(2)}, u32[]{:S(2)}) %collective-permute-start) | collective-permute-done | bytes 270368 | tf_op jit(solution)/shard_map/ppermute | solution.py:19
  129.1 0.7 copy-done.4
  129.9 1.2 collective-permute-done.1.refs_2_
  131.1 0.7 copy-done.6
  131.8 0.0 all-to-all-done.2.refs_3_
  131.8 0.0 collective-permute-done.3.refs_4_
  131.8 0.0 collective-permute-done.4.refs_5_
  131.8 1.0 copy-done.5
  132.8 1.0 copy-done.7
  133.8 6.3 %shard_map.107 = (bf16[4,4,32,352]{3,2,1,0:T(8,128)(2,1)}, bf16[64,4096]{1,0:T(8,128)(2,1)}, bf16[64,4096]{1,0:T(8,128)(2,1)}) custom-call(s32[4]{0:T(128)S(1)} %pad_add_fusion.at, bf16[3,128,2048]{2,1,0:T(8,128)(2,1)S(1)} %shard_map.103.tok, bf16[4,4,96,352]{3,2,1,0:T(8,128)(2,1)S(1)} %all-to-all-done.1.near.refs_0_, bf16[4,96,352]{2,1,0:T(8,128)(2,1)S(1)} %copy-done.5, ...), custom_call_target="tpu_custom_call" | custom-call | tf_op jit(solution)/shard_map/pallas_call | solution.py:188
  140.0 0.0 copy-start.10
  140.0 4.0 %all-to-all-start.3 = ((bf16[4,4,32,352]{3,2,1,0:T(8,128)(2,1)}), bf16[4,4,32,352]{3,2,1,0:T(8,128)(2,1)S(1)}, u32[]{:S(2)}, u32[]{:S(2)}) async-start(bf16[4,4,32,352]{3,2,1,0:T(8,128)(2,1)} %get-tuple-element.28), calls=%async_computation.3 | async-start | bytes 786432 | tf_op jit(solution)/shard_map/all_to_all | solution.py:206
  144.1 1.2 shard_map.111
  145.3 3.4 %collective-permute-start.10 = (bf16[128,512]{1,0:T(8,128)(2,1)S(1)}, bf16[128,512]{1,0:T(8,128)(2,1)S(1)}, u32[]{:S(2)}, u32[]{:S(2)}) collective-permute-start(bf16[128,512]{1,0:T(8,128)(2,1)S(1)} %get-tuple-element.25), channel_id=1, source_target_pairs={{0,8},{8,16},{16,24},{24,0},{1,9},{9,17},{17,25},{25,1},{2,10},{10... | collective-permute-start | bytes 393224 | tf_op jit(solution)/shard_map/ppermute | solution.py:19
  148.7 4.3 %collective-permute-start.11 = (bf16[128,512]{1,0:T(8,128)(2,1)S(1)}, bf16[128,512]{1,0:T(8,128)(2,1)S(1)}, u32[]{:S(2)}, u32[]{:S(2)}) collective-permute-start(bf16[128,512]{1,0:T(8,128)(2,1)S(1)} %get-tuple-element.26), channel_id=1, source_target_pairs={{0,16},{8,24},{16,0},{24,8},{1,17},{9,25},{17,1},{25,9},{2,18},{10... | collective-permute-start | bytes 393224 | tf_op jit(solution)/shard_map/ppermute | solution.py:19
  153.0 3.1 %collective-permute-start.12 = (bf16[128,512]{1,0:T(8,128)(2,1)S(1)}, bf16[128,512]{1,0:T(8,128)(2,1)S(1)}, u32[]{:S(2)}, u32[]{:S(2)}) collective-permute-start(bf16[128,512]{1,0:T(8,128)(2,1)S(1)} %get-tuple-element.27), channel_id=1, source_target_pairs={{0,24},{8,0},{16,8},{24,16},{1,25},{9,1},{17,9},{25,17},{2,26},{10... | collective-permute-start | bytes 393224 | tf_op jit(solution)/shard_map/ppermute | solution.py:19
  156.1 7.1 %collective-permute-start.5 = (bf16[64,4096]{1,0:T(8,128)(2,1)S(1)}, bf16[64,4096]{1,0:T(8,128)(2,1)S(1)}, u32[]{:S(2)}, u32[]{:S(2)}) collective-permute-start(bf16[64,4096]{1,0:T(8,128)(2,1)S(1)} %copy-done.10), channel_id=1, source_target_pairs={{0,1},{1,0},{2,3},{3,2},{4,5},{5,4},{6,7},{7,6},{8,9},{9,8},{10,11... | collective-permute-start | bytes 1572872 | tf_op jit(solution)/shard_map/ppermute | solution.py:19
  163.2 0.0 collective-permute-done.10.b1
  163.2 0.0 collective-permute-done.11.b2
  163.2 0.0 collective-permute-done.12.b3
  163.2 0.7 shard_map.112.cols
  163.9 0.0 copy-start.1
  164.0 0.0 all-to-all-done.3.gds
  164.0 1.7 shard_map.113
  165.7 5.0 %all-to-all-start.4 = ((bf16[16,32,352]{2,1,0:T(8,128)(2,1)}), bf16[16,32,352]{2,1,0:T(8,128)(2,1)S(1)}, u32[]{:S(2)}, u32[]{:S(2)}) async-start(bf16[16,32,352]{2,1,0:T(8,128)(2,1)} %shard_map.113), calls=%async_computation.4 | async-start | bytes 786432 | tf_op jit(solution)/shard_map/all_to_all | solution.py:206
  170.7 0.0 collective-permute-done.5.other
  170.7 0.7 shard_map.108
  171.4 3.1 %collective-permute-start.6 = (bf16[16,4096]{1,0:T(8,128)(2,1)S(1)}, bf16[16,4096]{1,0:T(8,128)(2,1)S(1)}, u32[]{:S(2)}, u32[]{:S(2)}) collective-permute-start(bf16[16,4096]{1,0:T(8,128)(2,1)S(1)} %get-tuple-element.19), channel_id=1, source_target_pairs={{0,2},{2,4},{4,6},{6,0},{1,3},{3,5},{5,7},{7,1},{8,10},{10,12},{12... | collective-permute-start | bytes 393224 | tf_op jit(solution)/shard_map/ppermute | solution.py:19
  174.5 4.4 %collective-permute-start.7 = (bf16[16,4096]{1,0:T(8,128)(2,1)S(1)}, bf16[16,4096]{1,0:T(8,128)(2,1)S(1)}, u32[]{:S(2)}, u32[]{:S(2)}) collective-permute-start(bf16[16,4096]{1,0:T(8,128)(2,1)S(1)} %get-tuple-element.20), channel_id=1, source_target_pairs={{0,4},{2,6},{4,0},{6,2},{1,5},{3,7},{5,1},{7,3},{8,12},{10,14},{12... | collective-permute-start | bytes 393224 | tf_op jit(solution)/shard_map/ppermute | solution.py:19
  178.9 3.1 %collective-permute-start.8 = (bf16[16,4096]{1,0:T(8,128)(2,1)S(1)}, bf16[16,4096]{1,0:T(8,128)(2,1)S(1)}, u32[]{:S(2)}, u32[]{:S(2)}) collective-permute-start(bf16[16,4096]{1,0:T(8,128)(2,1)S(1)} %get-tuple-element.21), channel_id=1, source_target_pairs={{0,6},{2,0},{4,2},{6,4},{1,7},{3,1},{5,3},{7,5},{8,14},{10,8},{12,... | collective-permute-start | bytes 393224 | tf_op jit(solution)/shard_map/ppermute | solution.py:19
  182.0 0.0 collective-permute-done.6.p1
  182.0 1.4 collective-permute-done.7.p2
  183.4 1.7 collective-permute-done.8.p3
  185.1 0.7 shard_map.109
  185.7 10.8 %all_gather.3.half = bf16[64,4096]{1,0:T(8,128)(2,1)S(1)} all-gather(bf16[16,4096]{1,0:T(8,128)(2,1)S(1)} %shard_map.109), channel_id=1, replica_groups=mesh['za'=4,'zb'=4,'y'=4,'x'=4,'c'=2] {'x'}, dimensions={0}, use_global_device_ids=true | all-gather | bytes 655360 | tf_op jit(solution)/shard_map/all_gather | solution.py:249
  196.5 7.7 %collective-permute-start.9 = (bf16[64,4096]{1,0:T(8,128)(2,1)S(1)}, bf16[64,4096]{1,0:T(8,128)(2,1)S(1)}, u32[]{:S(2)}, u32[]{:S(2)}) collective-permute-start(bf16[64,4096]{1,0:T(8,128)(2,1)S(1)} %all_gather.3.half), channel_id=1, source_target_pairs={{0,1},{1,0},{2,3},{3,2},{4,5},{5,4},{6,7},{7,6},{8,9},{9,8},{10,11... | collective-permute-start | bytes 1572872 | tf_op jit(solution)/shard_map/ppermute | solution.py:19
  204.2 1.5 collective-permute-done.9.other
  205.7 1.5 shard_map.110
  207.3 0.0 all-to-all-done.4
  207.3 0.1 convert_reduce_fusion
  207.4 0.6 add.3
  (11 shorter events, 0.0 us)
Async XLA Ops:
  2.2 29.9 %all-to-all-start = ((bf16[4,96,352]{2,1,0:T(8,128)(2,1)}), bf16[4,96,352]{2,1,0:T(8,128)(2,1)}, u32[]{:S(2)}, u32[]{:S(2)}) async-start(bf16[4,96,352]{2,1,0:T(8,128)(2,1)} %broadcast_in_dim.3), calls=%async_computation | async-start | bytes 589824 | tf_op jit(solution)/shard_map/all_to_all | solution.py:24
  69.5 22.5 %all-to-all-start.1 = ((bf16[4,4,96,352]{3,2,1,0:T(8,128)(2,1)}), bf16[4,4,96,352]{3,2,1,0:T(8,128)(2,1)S(1)}, u32[]{:S(2)}, u32[]{:S(2)}) async-start(bf16[4,4,96,352]{3,2,1,0:T(8,128)(2,1)} %shard_map.104), calls=%async_computation.1 | async-start | bytes 2359296 | tf_op jit(solution)/shard_map/all_to_all | solution.py:206
  73.7 16.7 %collective-permute-start.2 = (bf16[4,96,352]{2,1,0:T(8,128)(2,1)}, bf16[4,96,352]{2,1,0:T(8,128)(2,1)S(1)}, u32[]{:S(2)}, u32[]{:S(2)}) collective-permute-start(bf16[4,96,352]{2,1,0:T(8,128)(2,1)} %all-to-all-done.piece), channel_id=1, source_target_pairs={{0,448},{32,96},{64,0},{96,160},{128,64},{160,224},{192,128},{224,... | collective-permute-start | bytes 811016 | tf_op jit(solution)/shard_map/ppermute | solution.py:219
  92.0 39.8 %all-to-all-start.2 = ((bf16[4,4,96,352]{3,2,1,0:T(8,128)(2,1)}), bf16[4,4,96,352]{3,2,1,0:T(8,128)(2,1)}, u32[]{:S(2)}, u32[]{:S(2)}) async-start(bf16[4,4,96,352]{3,2,1,0:T(8,128)(2,1)} %shard_map.105), calls=%async_computation.2 | async-start | bytes 2359296 | tf_op jit(solution)/shard_map/all_to_all | solution.py:206
  96.3 15.8 %copy-start = (bf16[128,2048]{1,0:T(8,128)(2,1)S(1)}, bf16[128,2048]{1,0:T(8,128)(2,1)}, u32[]{:S(2)}) copy-start(bf16[128,2048]{1,0:T(8,128)(2,1)} %bt.5) | copy-start | bytes 1572868
  96.3 15.8 %copy-start.2 = (bf16[128,2048]{1,0:T(8,128)(2,1)S(1)}, bf16[128,2048]{1,0:T(8,128)(2,1)}, u32[]{:S(2)}) copy-start(bf16[128,2048]{1,0:T(8,128)(2,1)} %ft.1) | copy-start | bytes 1572868
  96.3 15.8 %copy-start.3 = (bf16[128,2048]{1,0:T(8,128)(2,1)S(1)}, bf16[128,2048]{1,0:T(8,128)(2,1)}, u32[]{:S(2)}) copy-start(bf16[128,2048]{1,0:T(8,128)(2,1)} %og.1) | copy-start | bytes 1572868
  96.3 15.8 %copy-start.8 = (f32[2048]{0:T(1024)S(1)}, f32[2048]{0:T(1024)}, u32[]{:S(2)}) copy-start(f32[2048]{0:T(1024)} %param.11) | copy-start | bytes 24580
  97.8 34.0 %collective-permute-start.3 = (bf16[3,4,96,352]{3,2,1,0:T(8,128)(2,1)}, bf16[3,4,96,352]{3,2,1,0:T(8,128)(2,1)}, u32[]{:S(2)}, u32[]{:S(2)}) collective-permute-start(bf16[3,4,96,352]{3,2,1,0:T(8,128)(2,1)} %shard_map.106), channel_id=1, source_target_pairs={{0,480},{32,0},{64,32},{96,64},{128,96},{160,128},{192,160},{224,1... | collective-permute-start | bytes 2433032 | tf_op jit(solution)/shard_map/ppermute | solution.py:19
  100.8 31.0 %collective-permute-start.4 = (bf16[3,4,96,352]{3,2,1,0:T(8,128)(2,1)}, bf16[3,4,96,352]{3,2,1,0:T(8,128)(2,1)}, u32[]{:S(2)}, u32[]{:S(2)}) collective-permute-start(bf16[3,4,96,352]{3,2,1,0:T(8,128)(2,1)} %shard_map.106), channel_id=1, source_target_pairs={{0,32},{32,64},{64,96},{96,128},{128,160},{160,192},{192,224},{224... | collective-permute-start | bytes 2433032 | tf_op jit(solution)/shard_map/ppermute | solution.py:19
  106.8 22.4 %collective-permute-start = (bf16[4,96,352]{2,1,0:T(8,128)(2,1)}, bf16[4,96,352]{2,1,0:T(8,128)(2,1)S(1)}, u32[]{:S(2)}, u32[]{:S(2)}) collective-permute-start(bf16[4,96,352]{2,1,0:T(8,128)(2,1)} %all-to-all-done.piece), channel_id=1, source_target_pairs={{0,480},{32,0},{64,32},{96,64},{128,96},{160,128},{192,160},{224,1... | collective-permute-start | bytes 811016 | tf_op jit(solution)/shard_map/ppermute | solution.py:19
  109.4 21.7 %collective-permute-start.1 = (bf16[4,96,352]{2,1,0:T(8,128)(2,1)}, bf16[4,96,352]{2,1,0:T(8,128)(2,1)S(1)}, u32[]{:S(2)}, u32[]{:S(2)}) collective-permute-start(bf16[4,96,352]{2,1,0:T(8,128)(2,1)} %all-to-all-done.piece), channel_id=1, source_target_pairs={{0,32},{32,64},{64,96},{96,128},{128,160},{160,192},{192,224},{224... | collective-permute-start | bytes 811016 | tf_op jit(solution)/shard_map/ppermute | solution.py:19
  129.1 0.7 copy-start.4
  131.1 0.7 copy-start.6
  131.8 1.0 copy-start.5
  132.8 1.0 copy-start.7
  140.0 16.0 %copy-start.10 = (bf16[64,4096]{1,0:T(8,128)(2,1)S(1)}, bf16[64,4096]{1,0:T(8,128)(2,1)}, u32[]{:S(2)}) copy-start(bf16[64,4096]{1,0:T(8,128)(2,1)} %get-tuple-element.17) | copy-start | bytes 1572868
  140.0 23.9 %all-to-all-start.3 = ((bf16[4,4,32,352]{3,2,1,0:T(8,128)(2,1)}), bf16[4,4,32,352]{3,2,1,0:T(8,128)(2,1)S(1)}, u32[]{:S(2)}, u32[]{:S(2)}) async-start(bf16[4,4,32,352]{3,2,1,0:T(8,128)(2,1)} %get-tuple-element.28), calls=%async_computation.3 | async-start | bytes 786432 | tf_op jit(solution)/shard_map/all_to_all | solution.py:206
  145.3 17.9 %collective-permute-start.10 = (bf16[128,512]{1,0:T(8,128)(2,1)S(1)}, bf16[128,512]{1,0:T(8,128)(2,1)S(1)}, u32[]{:S(2)}, u32[]{:S(2)}) collective-permute-start(bf16[128,512]{1,0:T(8,128)(2,1)S(1)} %get-tuple-element.25), channel_id=1, source_target_pairs={{0,8},{8,16},{16,24},{24,0},{1,9},{9,17},{17,25},{25,1},{2,10},{10... | collective-permute-start | bytes 393224 | tf_op jit(solution)/shard_map/ppermute | solution.py:19
  148.7 14.5 %collective-permute-start.11 = (bf16[128,512]{1,0:T(8,128)(2,1)S(1)}, bf16[128,512]{1,0:T(8,128)(2,1)S(1)}, u32[]{:S(2)}, u32[]{:S(2)}) collective-permute-start(bf16[128,512]{1,0:T(8,128)(2,1)S(1)} %get-tuple-element.26), channel_id=1, source_target_pairs={{0,16},{8,24},{16,0},{24,8},{1,17},{9,25},{17,1},{25,9},{2,18},{10... | collective-permute-start | bytes 393224 | tf_op jit(solution)/shard_map/ppermute | solution.py:19
  153.0 10.2 %collective-permute-start.12 = (bf16[128,512]{1,0:T(8,128)(2,1)S(1)}, bf16[128,512]{1,0:T(8,128)(2,1)S(1)}, u32[]{:S(2)}, u32[]{:S(2)}) collective-permute-start(bf16[128,512]{1,0:T(8,128)(2,1)S(1)} %get-tuple-element.27), channel_id=1, source_target_pairs={{0,24},{8,0},{16,8},{24,16},{1,25},{9,1},{17,9},{25,17},{2,26},{10... | collective-permute-start | bytes 393224 | tf_op jit(solution)/shard_map/ppermute | solution.py:19
  156.1 14.6 %collective-permute-start.5 = (bf16[64,4096]{1,0:T(8,128)(2,1)S(1)}, bf16[64,4096]{1,0:T(8,128)(2,1)S(1)}, u32[]{:S(2)}, u32[]{:S(2)}) collective-permute-start(bf16[64,4096]{1,0:T(8,128)(2,1)S(1)} %copy-done.10), channel_id=1, source_target_pairs={{0,1},{1,0},{2,3},{3,2},{4,5},{5,4},{6,7},{7,6},{8,9},{9,8},{10,11... | collective-permute-start | bytes 1572872 | tf_op jit(solution)/shard_map/ppermute | solution.py:19
  163.9 6.8 %copy-start.1 = (bf16[64,4096]{1,0:T(8,128)(2,1)S(1)}, bf16[64,4096]{1,0:T(8,128)(2,1)}, u32[]{:S(2)}) copy-start(bf16[64,4096]{1,0:T(8,128)(2,1)} %get-tuple-element.16.keep) | copy-start | bytes 1572868
  165.7 41.6 %all-to-all-start.4 = ((bf16[16,32,352]{2,1,0:T(8,128)(2,1)}), bf16[16,32,352]{2,1,0:T(8,128)(2,1)S(1)}, u32[]{:S(2)}, u32[]{:S(2)}) async-start(bf16[16,32,352]{2,1,0:T(8,128)(2,1)} %shard_map.113), calls=%async_computation.4 | async-start | bytes 786432 | tf_op jit(solution)/shard_map/all_to_all | solution.py:206
  171.4 10.6 %collective-permute-start.6 = (bf16[16,4096]{1,0:T(8,128)(2,1)S(1)}, bf16[16,4096]{1,0:T(8,128)(2,1)S(1)}, u32[]{:S(2)}, u32[]{:S(2)}) collective-permute-start(bf16[16,4096]{1,0:T(8,128)(2,1)S(1)} %get-tuple-element.19), channel_id=1, source_target_pairs={{0,2},{2,4},{4,6},{6,0},{1,3},{3,5},{5,7},{7,1},{8,10},{10,12},{12... | collective-permute-start | bytes 393224 | tf_op jit(solution)/shard_map/ppermute | solution.py:19
  174.5 8.8 %collective-permute-start.7 = (bf16[16,4096]{1,0:T(8,128)(2,1)S(1)}, bf16[16,4096]{1,0:T(8,128)(2,1)S(1)}, u32[]{:S(2)}, u32[]{:S(2)}) collective-permute-start(bf16[16,4096]{1,0:T(8,128)(2,1)S(1)} %get-tuple-element.20), channel_id=1, source_target_pairs={{0,4},{2,6},{4,0},{6,2},{1,5},{3,7},{5,1},{7,3},{8,12},{10,14},{12... | collective-permute-start | bytes 393224 | tf_op jit(solution)/shard_map/ppermute | solution.py:19
  178.9 6.2 %collective-permute-start.8 = (bf16[16,4096]{1,0:T(8,128)(2,1)S(1)}, bf16[16,4096]{1,0:T(8,128)(2,1)S(1)}, u32[]{:S(2)}, u32[]{:S(2)}) collective-permute-start(bf16[16,4096]{1,0:T(8,128)(2,1)S(1)} %get-tuple-element.21), channel_id=1, source_target_pairs={{0,6},{2,0},{4,2},{6,4},{1,7},{3,1},{5,3},{7,5},{8,14},{10,8},{12,... | collective-permute-start | bytes 393224 | tf_op jit(solution)/shard_map/ppermute | solution.py:19
  185.7 21.6 %copy-start.9 = (f32[32,352]{1,0:T(8,128)S(1)}, f32[32,352]{1,0:T(8,128)}, u32[]{:S(2)}) copy-start(f32[32,352]{1,0:T(8,128)} %param.15) | copy-start | bytes 135172
  196.5 9.2 %collective-permute-start.9 = (bf16[64,4096]{1,0:T(8,128)(2,1)S(1)}, bf16[64,4096]{1,0:T(8,128)(2,1)S(1)}, u32[]{:S(2)}, u32[]{:S(2)}) collective-permute-start(bf16[64,4096]{1,0:T(8,128)(2,1)S(1)} %all_gather.3.half), channel_id=1, source_target_pairs={{0,1},{1,0},{2,3},{3,2},{4,5},{5,4},{6,7},{7,6},{8,9},{9,8},{10,11... | collective-permute-start | bytes 1572872 | tf_op jit(solution)/shard_map/ppermute | solution.py:19

commit v10 on v7

--- a/solution.py
+++ b/solution.py
@@ -140,14 +140,12 @@
 
 def merge(at, b0, b1, b2, b3, out):
     for k, piece in enumerate((b0, b1, b2, b3)):
-        out[(at[1] + 4 - k) % 4] = piece[...]
+        spot = pl.multiple_of((at[1] + 4 - k) % 4 * 128, 128)
+        out[:, pl.ds(spot, 128)] = piece[...].astype(F32).T.astype(BF)
 
 
 def outer(at, cols, gds, grads):
-    total = dot(cols[0], gds[0].reshape(128, 352), 0, 0)
-    for k in range(1, 4):
-        total = total + dot(cols[k], gds[k].reshape(128, 352), 0, 0)
-    total = total.astype(BF)
+    total = dot(cols[...], gds[...].reshape(512, 352), 1, 0).astype(BF)
     for z in range(16):
         grads[z] = total[z * 32 : (z + 1) * 32, :]
 
@@ -222,7 +220,7 @@
     b1 = shift(b1, "y", 1)
     b2 = shift(b2, "y", 2)
     b3 = shift(b3, "y", 3)
-    (cols,) = call(merge, ((4, *COL),), (), at, b0, b1, b2, b3)
+    (cols,) = call(merge, ((512, 512),), (), at, b0, b1, b2, b3)
     gds, keep, give = call(
         products,
         ((4, 4, 32, 352), (64, 4096), (64, 4096)),

time: 233 us -> 233 us (level)
  no operation moved by 1% of the time
where the time goes in v10:
time: 233 us; the launch traced here: 232 us
  starting transfers between devices  81.3 us (35%)
  waiting for transfers between devices  75.5 us (32%)
  Pallas kernels  52.8 us (23%)
  blocking collectives  13.1 us (6%)
  local copies, waits for them, and re-layouts  5.14 us (2%)
  other arithmetic  2.66 us (1%)
    pallas_call x10, Pallas kernels, call(): pl.pallas_call(body, out_shape=tuple((shape(o) for o in outs)), in_specs=...  52.8 us
    ppermute x12, starting transfers between devices, shift(): return lax.ppermute(array, axis, [(k, (k + by) % n) for k in range(n)])  40.6 us
    ppermute x12, waiting for transfers between devices, shift(): return lax.ppermute(array, axis, [(k, (k + by) % n) for k in range(n)])  27.1 us
    all_to_all x4, waiting for transfers between devices, exchange(): return lax.all_to_all(array, axis, split_axis=0, concat_axis=0, tiled=True)  22.8 us
    all_to_all x4, starting transfers between devices, exchange(): return lax.all_to_all(array, axis, split_axis=0, concat_axis=0, tiled=True)  19.8 us
    all_to_all x1, waiting for transfers between devices, copies_to_all(): return lax.all_to_all(copies, axis, split_axis=0, concat_axis=0, tiled=True)  19 us
    all_to_all x1, starting transfers between devices, copies_to_all(): return lax.all_to_all(copies, axis, split_axis=0, concat_axis=0, tiled=True)  15.1 us
    all_gather x1, blocking collectives, shards(): half = lax.all_gather(done, 'x', axis=0, tiled=True)  13.1 us
  transfers between devices with their start and end apart: 18, of which 10 were waited for; matrix products, arithmetic and copies ran while one was open for 1% of the time, Pallas kernels for 3%

profile of v10, /device:TPU:8, one launch (start us, length us, event | category | flops | bytes accessed | tf_op | source)
XLA Modules:
  0.0 231.6 jit_solution(16780269011025363519)
XLA Ops:
  0.6 0.8 pad_maximum_fusion.1
  1.4 0.7 broadcast_in_dim.3
  2.2 15.1 %all-to-all-start = ((bf16[4,96,352]{2,1,0:T(8,128)(2,1)}), bf16[4,96,352]{2,1,0:T(8,128)(2,1)}, u32[]{:S(2)}, u32[]{:S(2)}) async-start(bf16[4,96,352]{2,1,0:T(8,128)(2,1)} %broadcast_in_dim.3), calls=%async_computation | async-start | bytes 589824 | tf_op jit(solution)/shard_map/all_to_all | solution.py:24
  17.2 0.1 pad_add_fusion.at
  17.3 19.0 %all-to-all-done.piece = bf16[4,96,352]{2,1,0:T(8,128)(2,1)} async-done(((bf16[4,96,352]{2,1,0:T(8,128)(2,1)}), bf16[4,96,352]{2,1,0:T(8,128)(2,1)}, u32[]{:S(2)}, u32[]{:S(2)}) %all-to-all-start) | async-done | bytes 270368 | tf_op jit(solution)/shard_map/all_to_all | solution.py:24
  36.3 37.4 %shard_map.104 = bf16[4,4,96,352]{3,2,1,0:T(8,128)(2,1)} custom-call(s32[4]{0:T(128)S(1)} %pad_add_fusion.at, bf16[4,96,352]{2,1,0:T(8,128)(2,1)} %all-to-all-done.piece), custom_call_target="tpu_custom_call" | custom-call | tf_op jit(solution)/shard_map/pallas_call | solution.py:179
  73.7 4.9 %all-to-all-start.1 = ((bf16[4,4,96,352]{3,2,1,0:T(8,128)(2,1)}), bf16[4,4,96,352]{3,2,1,0:T(8,128)(2,1)S(1)}, u32[]{:S(2)}, u32[]{:S(2)}) async-start(bf16[4,4,96,352]{3,2,1,0:T(8,128)(2,1)} %shard_map.104), calls=%async_computation.1 | async-start | bytes 2359296 | tf_op jit(solution)/shard_map/all_to_all | solution.py:197
  78.6 5.9 %collective-permute-start.2 = (bf16[4,96,352]{2,1,0:T(8,128)(2,1)}, bf16[4,96,352]{2,1,0:T(8,128)(2,1)S(1)}, u32[]{:S(2)}, u32[]{:S(2)}) collective-permute-start(bf16[4,96,352]{2,1,0:T(8,128)(2,1)} %all-to-all-done.piece), channel_id=1, source_target_pairs={{0,448},{32,96},{64,0},{96,160},{128,64},{160,224},{192,128},{224,... | collective-permute-start | bytes 811016 | tf_op jit(solution)/shard_map/ppermute | solution.py:211
  84.5 6.7 %collective-permute-done.2.piece = bf16[4,96,352]{2,1,0:T(8,128)(2,1)S(1)} collective-permute-done((bf16[4,96,352]{2,1,0:T(8,128)(2,1)}, bf16[4,96,352]{2,1,0:T(8,128)(2,1)S(1)}, u32[]{:S(2)}, u32[]{:S(2)}) %collective-permute-start.2) | collective-permute-done | bytes 270368 | tf_op jit(solution)/shard_map/ppermute | solution.py:211
  91.2 1.6 shard_map.105
  92.8 0.0 all-to-all-done.1.near.refs_0_
  92.8 4.8 %all-to-all-start.2 = ((bf16[4,4,96,352]{3,2,1,0:T(8,128)(2,1)}), bf16[4,4,96,352]{3,2,1,0:T(8,128)(2,1)}, u32[]{:S(2)}, u32[]{:S(2)}) async-start(bf16[4,4,96,352]{3,2,1,0:T(8,128)(2,1)} %shard_map.105), calls=%async_computation.2 | async-start | bytes 2359296 | tf_op jit(solution)/shard_map/all_to_all | solution.py:197
  97.7 1.5 shard_map.106
  99.2 5.2 %collective-permute-start.3 = (bf16[3,4,96,352]{3,2,1,0:T(8,128)(2,1)}, bf16[3,4,96,352]{3,2,1,0:T(8,128)(2,1)}, u32[]{:S(2)}, u32[]{:S(2)}) collective-permute-start(bf16[3,4,96,352]{3,2,1,0:T(8,128)(2,1)} %shard_map.106), channel_id=1, source_target_pairs={{0,480},{32,0},{64,32},{96,64},{128,96},{160,128},{192,160},{224,1... | collective-permute-start | bytes 2433032 | tf_op jit(solution)/shard_map/ppermute | solution.py:19
  104.4 3.9 %collective-permute-start.4 = (bf16[3,4,96,352]{3,2,1,0:T(8,128)(2,1)}, bf16[3,4,96,352]{3,2,1,0:T(8,128)(2,1)}, u32[]{:S(2)}, u32[]{:S(2)}) collective-permute-start(bf16[3,4,96,352]{3,2,1,0:T(8,128)(2,1)} %shard_map.106), channel_id=1, source_target_pairs={{0,32},{32,64},{64,96},{96,128},{128,160},{160,192},{192,224},{224... | collective-permute-start | bytes 2433032 | tf_op jit(solution)/shard_map/ppermute | solution.py:19
  108.3 3.2 %collective-permute-start = (bf16[4,96,352]{2,1,0:T(8,128)(2,1)}, bf16[4,96,352]{2,1,0:T(8,128)(2,1)S(1)}, u32[]{:S(2)}, u32[]{:S(2)}) collective-permute-start(bf16[4,96,352]{2,1,0:T(8,128)(2,1)} %all-to-all-done.piece), channel_id=1, source_target_pairs={{0,480},{32,0},{64,32},{96,64},{128,96},{160,128},{192,160},{224,1... | collective-permute-start | bytes 811016 | tf_op jit(solution)/shard_map/ppermute | solution.py:19
  111.5 2.7 %collective-permute-start.1 = (bf16[4,96,352]{2,1,0:T(8,128)(2,1)}, bf16[4,96,352]{2,1,0:T(8,128)(2,1)S(1)}, u32[]{:S(2)}, u32[]{:S(2)}) collective-permute-start(bf16[4,96,352]{2,1,0:T(8,128)(2,1)} %all-to-all-done.piece), channel_id=1, source_target_pairs={{0,32},{32,64},{64,96},{96,128},{128,160},{160,192},{192,224},{224... | collective-permute-start | bytes 811016 | tf_op jit(solution)/shard_map/ppermute | solution.py:19
  114.2 0.0 copy-done
  114.2 0.0 copy-done.2
  114.2 1.0 shard_map.103.tok
  115.2 15.4 %collective-permute-done.refs_1_ = bf16[4,96,352]{2,1,0:T(8,128)(2,1)S(1)} collective-permute-done((bf16[4,96,352]{2,1,0:T(8,128)(2,1)}, bf16[4,96,352]{2,1,0:T(8,128)(2,1)S(1)}, u32[]{:S(2)}, u32[]{:S(2)}) %collective-permute-start) | collective-permute-done | bytes 270368 | tf_op jit(solution)/shard_map/ppermute | solution.py:19
  130.6 0.7 copy-done.4
  131.3 1.9 collective-permute-done.1.refs_2_
  133.1 0.7 copy-done.6
  133.9 0.0 all-to-all-done.2.refs_3_
  133.9 0.0 collective-permute-done.3.refs_4_
  133.9 0.0 collective-permute-done.4.refs_5_
  133.9 0.0 copy-start.5
  133.9 1.0 copy-done.5
  134.8 1.0 copy-done.7
  135.8 6.3 %shard_map.107 = (bf16[4,4,32,352]{3,2,1,0:T(8,128)(2,1)}, bf16[64,4096]{1,0:T(8,128)(2,1)}, bf16[64,4096]{1,0:T(8,128)(2,1)}) custom-call(s32[4]{0:T(128)S(1)} %pad_add_fusion.at, bf16[3,128,2048]{2,1,0:T(8,128)(2,1)S(1)} %shard_map.103.tok, bf16[4,4,96,352]{3,2,1,0:T(8,128)(2,1)S(1)} %all-to-all-done.1.near.refs_0_, bf16[4,96,352]{2,1,0:T(8,128)(2,1)S(1)} %copy-done.5, ...), custom_call_target="tpu_custom_call" | custom-call | tf_op jit(solution)/shard_map/pallas_call | solution.py:179
  142.1 1.9 collective-permute-start.5
  144.0 2.1 collective-permute-done.5.other
  146.1 1.0 copy-done.1
  147.1 0.7 shard_map.108
  147.8 3.4 %collective-permute-start.6 = (bf16[16,4096]{1,0:T(8,128)(2,1)S(1)}, bf16[16,4096]{1,0:T(8,128)(2,1)S(1)}, u32[]{:S(2)}, u32[]{:S(2)}) collective-permute-start(bf16[16,4096]{1,0:T(8,128)(2,1)S(1)} %get-tuple-element.17), channel_id=1, source_target_pairs={{0,2},{2,4},{4,6},{6,0},{1,3},{3,5},{5,7},{7,1},{8,10},{10,12},{12... | collective-permute-start | bytes 393224 | tf_op jit(solution)/shard_map/ppermute | solution.py:19
  151.2 4.7 %collective-permute-start.7 = (bf16[16,4096]{1,0:T(8,128)(2,1)S(1)}, bf16[16,4096]{1,0:T(8,128)(2,1)S(1)}, u32[]{:S(2)}, u32[]{:S(2)}) collective-permute-start(bf16[16,4096]{1,0:T(8,128)(2,1)S(1)} %get-tuple-element.18), channel_id=1, source_target_pairs={{0,4},{2,6},{4,0},{6,2},{1,5},{3,7},{5,1},{7,3},{8,12},{10,14},{12... | collective-permute-start | bytes 393224 | tf_op jit(solution)/shard_map/ppermute | solution.py:19
  155.9 3.3 %collective-permute-start.8 = (bf16[16,4096]{1,0:T(8,128)(2,1)S(1)}, bf16[16,4096]{1,0:T(8,128)(2,1)S(1)}, u32[]{:S(2)}, u32[]{:S(2)}) collective-permute-start(bf16[16,4096]{1,0:T(8,128)(2,1)S(1)} %get-tuple-element.19), channel_id=1, source_target_pairs={{0,6},{2,0},{4,2},{6,4},{1,7},{3,1},{5,3},{7,5},{8,14},{10,8},{12,... | collective-permute-start | bytes 393224 | tf_op jit(solution)/shard_map/ppermute | solution.py:19
  159.2 0.0 collective-permute-done.6.p1
  159.2 1.0 collective-permute-done.7.p2
  160.3 2.5 %collective-permute-done.8.p3 = bf16[16,4096]{1,0:T(8,128)(2,1)S(1)} collective-permute-done((bf16[16,4096]{1,0:T(8,128)(2,1)S(1)}, bf16[16,4096]{1,0:T(8,128)(2,1)S(1)}, u32[]{:S(2)}, u32[]{:S(2)}) %collective-permute-start.8) | collective-permute-done | bytes 131104 | tf_op jit(solution)/shard_map/ppermute | solution.py:19
  162.7 0.7 shard_map.109
  163.4 13.1 %all_gather.3 = bf16[64,4096]{1,0:T(8,128)(2,1)S(1)} all-gather(bf16[16,4096]{1,0:T(8,128)(2,1)S(1)} %shard_map.109), channel_id=1, replica_groups=mesh['za'=4,'zb'=4,'y'=4,'x'=4,'c'=2] {'x'}, dimensions={0}, use_global_device_ids=true | all-gather | bytes 655360 | tf_op jit(solution)/shard_map/all_gather | solution.py:241
  176.6 1.9 collective-permute-start.9
  178.5 4.8 %all-to-all-start.3 = ((bf16[4,4,32,352]{3,2,1,0:T(8,128)(2,1)}), bf16[4,4,32,352]{3,2,1,0:T(8,128)(2,1)S(1)}, u32[]{:S(2)}, u32[]{:S(2)}) async-start(bf16[4,4,32,352]{3,2,1,0:T(8,128)(2,1)} %get-tuple-element.24), calls=%async_computation.3 | async-start | bytes 786432 | tf_op jit(solution)/shard_map/all_to_all | solution.py:197
  183.3 1.2 shard_map.110
  184.5 3.4 %collective-permute-start.10 = (bf16[128,512]{1,0:T(8,128)(2,1)S(1)}, bf16[128,512]{1,0:T(8,128)(2,1)S(1)}, u32[]{:S(2)}, u32[]{:S(2)}) collective-permute-start(bf16[128,512]{1,0:T(8,128)(2,1)S(1)} %get-tuple-element.21), channel_id=1, source_target_pairs={{0,8},{8,16},{16,24},{24,0},{1,9},{9,17},{17,25},{25,1},{2,10},{10... | collective-permute-start | bytes 393224 | tf_op jit(solution)/shard_map/ppermute | solution.py:19
  187.9 2.5 %collective-permute-start.11 = (bf16[128,512]{1,0:T(8,128)(2,1)S(1)}, bf16[128,512]{1,0:T(8,128)(2,1)S(1)}, u32[]{:S(2)}, u32[]{:S(2)}) collective-permute-start(bf16[128,512]{1,0:T(8,128)(2,1)S(1)} %get-tuple-element.22), channel_id=1, source_target_pairs={{0,16},{8,24},{16,0},{24,8},{1,17},{9,25},{17,1},{25,9},{2,18},{10... | collective-permute-start | bytes 393224 | tf_op jit(solution)/shard_map/ppermute | solution.py:19
  190.5 4.5 %collective-permute-start.12 = (bf16[128,512]{1,0:T(8,128)(2,1)S(1)}, bf16[128,512]{1,0:T(8,128)(2,1)S(1)}, u32[]{:S(2)}, u32[]{:S(2)}) collective-permute-start(bf16[128,512]{1,0:T(8,128)(2,1)S(1)} %get-tuple-element.23), channel_id=1, source_target_pairs={{0,24},{8,0},{16,8},{24,16},{1,25},{9,1},{17,9},{25,17},{2,26},{10... | collective-permute-start | bytes 393224 | tf_op jit(solution)/shard_map/ppermute | solution.py:19
  195.0 0.0 collective-permute-done.10.b1
  195.0 2.3 collective-permute-done.11.b2
  197.3 1.9 collective-permute-done.12.b3
  199.2 0.7 shard_map.111.cols
  199.9 0.0 all-to-all-done.3.gds
  200.0 1.7 shard_map.112
  201.7 5.2 %all-to-all-start.4 = ((bf16[16,32,352]{2,1,0:T(8,128)(2,1)}), bf16[16,32,352]{2,1,0:T(8,128)(2,1)S(1)}, u32[]{:S(2)}, u32[]{:S(2)}) async-start(bf16[16,32,352]{2,1,0:T(8,128)(2,1)} %shard_map.112), calls=%async_computation.4 | async-start | bytes 786432 | tf_op jit(solution)/shard_map/all_to_all | solution.py:197
  206.9 0.0 collective-permute-done.9
  206.9 0.1 broadcast_select_fusion
  207.0 0.0 copy-start.9
  207.0 1.0 pad_maximum_fusion
  208.1 22.8 %all-to-all-done.4 = bf16[16,32,352]{2,1,0:T(8,128)(2,1)S(1)} async-done(((bf16[16,32,352]{2,1,0:T(8,128)(2,1)}), bf16[16,32,352]{2,1,0:T(8,128)(2,1)S(1)}, u32[]{:S(2)}, u32[]{:S(2)}) %all-to-all-start.4) | async-done | bytes 360480 | tf_op jit(solution)/shard_map/all_to_all | solution.py:197
  230.9 0.1 convert_reduce_fusion
  230.9 0.0 copy-done.9
  230.9 0.6 add.3
  (10 shorter events, 0.0 us)
Async XLA Ops:
  2.2 34.1 %all-to-all-start = ((bf16[4,96,352]{2,1,0:T(8,128)(2,1)}), bf16[4,96,352]{2,1,0:T(8,128)(2,1)}, u32[]{:S(2)}, u32[]{:S(2)}) async-start(bf16[4,96,352]{2,1,0:T(8,128)(2,1)} %broadcast_in_dim.3), calls=%async_computation | async-start | bytes 589824 | tf_op jit(solution)/shard_map/all_to_all | solution.py:24
  73.7 19.1 %all-to-all-start.1 = ((bf16[4,4,96,352]{3,2,1,0:T(8,128)(2,1)}), bf16[4,4,96,352]{3,2,1,0:T(8,128)(2,1)S(1)}, u32[]{:S(2)}, u32[]{:S(2)}) async-start(bf16[4,4,96,352]{3,2,1,0:T(8,128)(2,1)} %shard_map.104), calls=%async_computation.1 | async-start | bytes 2359296 | tf_op jit(solution)/shard_map/all_to_all | solution.py:197
  78.6 12.6 %collective-permute-start.2 = (bf16[4,96,352]{2,1,0:T(8,128)(2,1)}, bf16[4,96,352]{2,1,0:T(8,128)(2,1)S(1)}, u32[]{:S(2)}, u32[]{:S(2)}) collective-permute-start(bf16[4,96,352]{2,1,0:T(8,128)(2,1)} %all-to-all-done.piece), channel_id=1, source_target_pairs={{0,448},{32,96},{64,0},{96,160},{128,64},{160,224},{192,128},{224,... | collective-permute-start | bytes 811016 | tf_op jit(solution)/shard_map/ppermute | solution.py:211
  92.8 41.0 %all-to-all-start.2 = ((bf16[4,4,96,352]{3,2,1,0:T(8,128)(2,1)}), bf16[4,4,96,352]{3,2,1,0:T(8,128)(2,1)}, u32[]{:S(2)}, u32[]{:S(2)}) async-start(bf16[4,4,96,352]{3,2,1,0:T(8,128)(2,1)} %shard_map.105), calls=%async_computation.2 | async-start | bytes 2359296 | tf_op jit(solution)/shard_map/all_to_all | solution.py:197
  97.6 16.5 %copy-start = (bf16[128,2048]{1,0:T(8,128)(2,1)S(1)}, bf16[128,2048]{1,0:T(8,128)(2,1)}, u32[]{:S(2)}) copy-start(bf16[128,2048]{1,0:T(8,128)(2,1)} %bt.5) | copy-start | bytes 1572868
  97.7 16.5 %copy-start.2 = (bf16[128,2048]{1,0:T(8,128)(2,1)S(1)}, bf16[128,2048]{1,0:T(8,128)(2,1)}, u32[]{:S(2)}) copy-start(bf16[128,2048]{1,0:T(8,128)(2,1)} %ft.1) | copy-start | bytes 1572868
  97.7 16.5 %copy-start.3 = (bf16[128,2048]{1,0:T(8,128)(2,1)S(1)}, bf16[128,2048]{1,0:T(8,128)(2,1)}, u32[]{:S(2)}) copy-start(bf16[128,2048]{1,0:T(8,128)(2,1)} %og.1) | copy-start | bytes 1572868
  97.7 16.5 %copy-start.8 = (f32[2048]{0:T(1024)S(1)}, f32[2048]{0:T(1024)}, u32[]{:S(2)}) copy-start(f32[2048]{0:T(1024)} %param.11) | copy-start | bytes 24580
  99.2 34.7 %collective-permute-start.3 = (bf16[3,4,96,352]{3,2,1,0:T(8,128)(2,1)}, bf16[3,4,96,352]{3,2,1,0:T(8,128)(2,1)}, u32[]{:S(2)}, u32[]{:S(2)}) collective-permute-start(bf16[3,4,96,352]{3,2,1,0:T(8,128)(2,1)} %shard_map.106), channel_id=1, source_target_pairs={{0,480},{32,0},{64,32},{96,64},{128,96},{160,128},{192,160},{224,1... | collective-permute-start | bytes 2433032 | tf_op jit(solution)/shard_map/ppermute | solution.py:19
  104.4 29.4 %collective-permute-start.4 = (bf16[3,4,96,352]{3,2,1,0:T(8,128)(2,1)}, bf16[3,4,96,352]{3,2,1,0:T(8,128)(2,1)}, u32[]{:S(2)}, u32[]{:S(2)}) collective-permute-start(bf16[3,4,96,352]{3,2,1,0:T(8,128)(2,1)} %shard_map.106), channel_id=1, source_target_pairs={{0,32},{32,64},{64,96},{96,128},{128,160},{160,192},{192,224},{224... | collective-permute-start | bytes 2433032 | tf_op jit(solution)/shard_map/ppermute | solution.py:19
  108.3 22.3 %collective-permute-start = (bf16[4,96,352]{2,1,0:T(8,128)(2,1)}, bf16[4,96,352]{2,1,0:T(8,128)(2,1)S(1)}, u32[]{:S(2)}, u32[]{:S(2)}) collective-permute-start(bf16[4,96,352]{2,1,0:T(8,128)(2,1)} %all-to-all-done.piece), channel_id=1, source_target_pairs={{0,480},{32,0},{64,32},{96,64},{128,96},{160,128},{192,160},{224,1... | collective-permute-start | bytes 811016 | tf_op jit(solution)/shard_map/ppermute | solution.py:19
  111.5 21.6 %collective-permute-start.1 = (bf16[4,96,352]{2,1,0:T(8,128)(2,1)}, bf16[4,96,352]{2,1,0:T(8,128)(2,1)S(1)}, u32[]{:S(2)}, u32[]{:S(2)}) collective-permute-start(bf16[4,96,352]{2,1,0:T(8,128)(2,1)} %all-to-all-done.piece), channel_id=1, source_target_pairs={{0,32},{32,64},{64,96},{96,128},{128,160},{160,192},{192,224},{224... | collective-permute-start | bytes 811016 | tf_op jit(solution)/shard_map/ppermute | solution.py:19
  130.6 0.7 copy-start.4
  133.1 0.7 copy-start.6
  133.9 1.0 copy-start.5
  134.8 1.0 copy-start.7
  142.1 4.0 %collective-permute-start.5 = (bf16[64,4096]{1,0:T(8,128)(2,1)}, bf16[64,4096]{1,0:T(8,128)(2,1)S(1)}, u32[]{:S(2)}, u32[]{:S(2)}) collective-permute-start(bf16[64,4096]{1,0:T(8,128)(2,1)} %get-tuple-element.15), channel_id=1, source_target_pairs={{0,1},{1,0},{2,3},{3,2},{4,5},{5,4},{6,7},{7,6},{8,9},{9,8},{10,11... | collective-permute-start | bytes 1572872 | tf_op jit(solution)/shard_map/ppermute | solution.py:19
  146.1 1.0 copy-start.1
  147.8 11.4 %collective-permute-start.6 = (bf16[16,4096]{1,0:T(8,128)(2,1)S(1)}, bf16[16,4096]{1,0:T(8,128)(2,1)S(1)}, u32[]{:S(2)}, u32[]{:S(2)}) collective-permute-start(bf16[16,4096]{1,0:T(8,128)(2,1)S(1)} %get-tuple-element.17), channel_id=1, source_target_pairs={{0,2},{2,4},{4,6},{6,0},{1,3},{3,5},{5,7},{7,1},{8,10},{10,12},{12... | collective-permute-start | bytes 393224 | tf_op jit(solution)/shard_map/ppermute | solution.py:19
  151.2 9.0 %collective-permute-start.7 = (bf16[16,4096]{1,0:T(8,128)(2,1)S(1)}, bf16[16,4096]{1,0:T(8,128)(2,1)S(1)}, u32[]{:S(2)}, u32[]{:S(2)}) collective-permute-start(bf16[16,4096]{1,0:T(8,128)(2,1)S(1)} %get-tuple-element.18), channel_id=1, source_target_pairs={{0,4},{2,6},{4,0},{6,2},{1,5},{3,7},{5,1},{7,3},{8,12},{10,14},{12... | collective-permute-start | bytes 393224 | tf_op jit(solution)/shard_map/ppermute | solution.py:19
  155.9 6.9 %collective-permute-start.8 = (bf16[16,4096]{1,0:T(8,128)(2,1)S(1)}, bf16[16,4096]{1,0:T(8,128)(2,1)S(1)}, u32[]{:S(2)}, u32[]{:S(2)}) collective-permute-start(bf16[16,4096]{1,0:T(8,128)(2,1)S(1)} %get-tuple-element.19), channel_id=1, source_target_pairs={{0,6},{2,0},{4,2},{6,4},{1,7},{3,1},{5,3},{7,5},{8,14},{10,8},{12,... | collective-permute-start | bytes 393224 | tf_op jit(solution)/shard_map/ppermute | solution.py:19
  176.6 30.4 %collective-permute-start.9 = (bf16[64,4096]{1,0:T(8,128)(2,1)S(1)}, bf16[64,4096]{1,0:T(8,128)(2,1)S(1)}, u32[]{:S(2)}, u32[]{:S(2)}) collective-permute-start(bf16[64,4096]{1,0:T(8,128)(2,1)S(1)} %all_gather.3), channel_id=1, source_target_pairs={{0,1},{1,0},{2,3},{3,2},{4,5},{5,4},{6,7},{7,6},{8,9},{9,8},{10,11... | collective-permute-start | bytes 1572872 | tf_op jit(solution)/shard_map/ppermute | solution.py:19
  178.5 21.5 %all-to-all-start.3 = ((bf16[4,4,32,352]{3,2,1,0:T(8,128)(2,1)}), bf16[4,4,32,352]{3,2,1,0:T(8,128)(2,1)S(1)}, u32[]{:S(2)}, u32[]{:S(2)}) async-start(bf16[4,4,32,352]{3,2,1,0:T(8,128)(2,1)} %get-tuple-element.24), calls=%async_computation.3 | async-start | bytes 786432 | tf_op jit(solution)/shard_map/all_to_all | solution.py:197
  184.5 10.5 %collective-permute-start.10 = (bf16[128,512]{1,0:T(8,128)(2,1)S(1)}, bf16[128,512]{1,0:T(8,128)(2,1)S(1)}, u32[]{:S(2)}, u32[]{:S(2)}) collective-permute-start(bf16[128,512]{1,0:T(8,128)(2,1)S(1)} %get-tuple-element.21), channel_id=1, source_target_pairs={{0,8},{8,16},{16,24},{24,0},{1,9},{9,17},{17,25},{25,1},{2,10},{10... | collective-permute-start | bytes 393224 | tf_op jit(solution)/shard_map/ppermute | solution.py:19
  187.9 9.3 %collective-permute-start.11 = (bf16[128,512]{1,0:T(8,128)(2,1)S(1)}, bf16[128,512]{1,0:T(8,128)(2,1)S(1)}, u32[]{:S(2)}, u32[]{:S(2)}) collective-permute-start(bf16[128,512]{1,0:T(8,128)(2,1)S(1)} %get-tuple-element.22), channel_id=1, source_target_pairs={{0,16},{8,24},{16,0},{24,8},{1,17},{9,25},{17,1},{25,9},{2,18},{10... | collective-permute-start | bytes 393224 | tf_op jit(solution)/shard_map/ppermute | solution.py:19
  190.5 8.7 %collective-permute-start.12 = (bf16[128,512]{1,0:T(8,128)(2,1)S(1)}, bf16[128,512]{1,0:T(8,128)(2,1)S(1)}, u32[]{:S(2)}, u32[]{:S(2)}) collective-permute-start(bf16[128,512]{1,0:T(8,128)(2,1)S(1)} %get-tuple-element.23), channel_id=1, source_target_pairs={{0,24},{8,0},{16,8},{24,16},{1,25},{9,1},{17,9},{25,17},{2,26},{10... | collective-permute-start | bytes 393224 | tf_op jit(solution)/shard_map/ppermute | solution.py:19
  201.7 29.2 %all-to-all-start.4 = ((bf16[16,32,352]{2,1,0:T(8,128)(2,1)}), bf16[16,32,352]{2,1,0:T(8,128)(2,1)S(1)}, u32[]{:S(2)}, u32[]{:S(2)}) async-start(bf16[16,32,352]{2,1,0:T(8,128)(2,1)} %shard_map.112), calls=%async_computation.4 | async-start | bytes 786432 | tf_op jit(solution)/shard_map/all_to_all | solution.py:197
  207.0 23.9 %copy-start.9 = (f32[32,352]{1,0:T(8,128)S(1)}, f32[32,352]{1,0:T(8,128)}, u32[]{:S(2)}) copy-start(f32[32,352]{1,0:T(8,128)} %param.15) | copy-start | bytes 135172
